TPU v7x, 512 devices: a whole 4x4x16 slice. The times are simulated.
512 devices in a mesh: sp: 32 (over z, core), tp: 16 (over y, x).
Axes of the slice: x: 4, y: 4, z: 16, core: 2. Of those that a mesh axis runs over, the one named last changes fastest.
Arguments:
- b_gate: bfloat16 [8192, 1024], P('sp', 'tp'), may hold values from -6 to 6
- c_gate: bfloat16 [8192, 1024], P('sp', 'tp'), may hold values from -6 to 6
- h_in: bfloat16 [8192, 1024], P('sp', 'tp'), may hold values from -6 to 6
- docs: int32 [8192], replicated, may hold values from 0 to 15, never falling along the last dimension, each value on 1 to 1024 neighbouring positions
- conv_taps: bfloat16 [3, 1024], replicated, may hold values from -3 to 3
- out_weight: bfloat16 [1024, 4096], P(None, 'tp'), may hold values from -0.1875 to 0.1875
- residual_in: bfloat16 [8192, 4096], P('sp', 'tp'), may hold values from -52 to 52
- norm_gain: bfloat16 [4096], replicated, may hold values from 0.099609375 to 1.8984375
- expert_pick: int32 [8192, 2], P('sp'), may hold values from 0 to 31, as said below
- route_weight: float32 [8192, 2], P('sp'), may hold values from 0.5 to 2
- w_gate: bfloat16 [32, 4096, 2048], P('sp', None, 'tp'), may hold values from -0.09375 to 0.09375
- w_up: bfloat16 [32, 4096, 2048], P('sp', None, 'tp'), may hold values from -0.09375 to 0.09375
- w_down: bfloat16 [32, 2048, 4096], P('sp', None, 'tp'), may hold values from -0.125 to 0.125
Outputs:
- stream_out: bfloat16 [8192, 4096], P('sp', 'tp')
Inputs may be any that keep to these rules, and one draw needn't show every extreme that they name: `expert_pick`: each row names 2 different experts of one group; group g holds experts g * 8 up to the next group's first.
All inputs are finite; a program needn't handle non-finite values.
Results may differ from a plain program's by a relative error of at most 0.012.
Values may be sent and summed in bfloat16 or wider, within the bound.
No kernel may reach another device: no remote copies, remote signals or barrier semaphores. Data moves between devices by JAX's collectives and lax.ppermute only.
A program may use at most 64 MiB of HBM per device.

v0:
```python
import jax
import jax.numpy as jnp
from jax import lax
from jax.experimental import pallas as pl
from jax.experimental.pallas import tpu as pltpu
from jax.sharding import Mesh
from jax.sharding import PartitionSpec as P

TP = ("ty", "tx")
NORM_EPS = 1e-06
F32 = jnp.float32
BF16 = jnp.bfloat16


def dot(a, b, ca=1, cb=0):
    return lax.dot_general(a, b, (((ca,), (cb,)), ((), ())), preferred_element_type=F32)


def kernel(body, outs, *args, limit=12):
    held = [a if a.ndim == 1 else pltpu.with_memory_space_constraint(a, pltpu.VMEM) for a in args]
    vmem = pl.BlockSpec(memory_space=pltpu.VMEM)
    smem = pl.BlockSpec(memory_space=pltpu.SMEM)
    got = pl.pallas_call(
        body,
        out_shape=tuple(jax.ShapeDtypeStruct(o, BF16) for o in outs),
        in_specs=[smem if a.ndim == 1 else vmem for a in args],
        out_specs=tuple(vmem for o in outs),
        compiler_params=pltpu.CompilerParams(vmem_limit_bytes=limit << 20),
    )(*held)
    return got if len(outs) > 1 else got[0]


def iota(shape, dim):
    return lax.broadcasted_iota(jnp.int32, shape, dim)


def to_row(col, width, offset):
    rows = col.shape[0]
    hit = iota((rows, width), 0) == iota((rows, width), 1) + offset
    return jnp.sum(jnp.where(hit, col, jnp.zeros((), col.dtype)), axis=0, keepdims=True)


def to_col(row, rows, offset):
    width = row.shape[1]
    hit = iota((rows, width), 0) == iota((rows, width), 1) + offset
    return jnp.sum(jnp.where(hit, row, jnp.zeros((), row.dtype)), axis=1, keepdims=True)


def slots(pick_ref, cap):
    toks = pick_ref.shape[0]
    e0 = pick_ref[:, 0:1]
    e1 = pick_ref[:, 1:2]
    experts = iota((toks, 128), 1)
    oh0 = (experts == e0).astype(F32)
    oh1 = (experts == e1).astype(F32)
    earlier = (iota((toks, toks), 0) > iota((toks, toks), 1)).astype(F32).astype(BF16)
    count = dot(earlier, (oh0 + oh1).astype(BF16))
    s0 = jnp.sum(count * oh0, axis=1, keepdims=True).astype(jnp.int32)
    s1 = jnp.sum((count + oh0) * oh1, axis=1, keepdims=True).astype(jnp.int32)
    return jnp.where(s0 < cap, e0 * cap + s0, -1), jnp.where(s1 < cap, e1 * cap + s1, -1)


def routing_out(pick, rows, cap):
    toks = pick.shape[0]

    def body(pick_ref, ct_ref):
        t0, t1 = slots(pick_ref, cap)
        r0 = to_row(t0, toks, 0)
        r1 = to_row(t1, toks, 0)
        across = iota((rows, toks), 0)
        ct_ref[...] = jnp.logical_or(across == r0, across == r1).astype(F32).astype(BF16)

    return kernel(body, ((rows, toks),), pick)


def routing_back(pick, rows, cap):
    toks = pick.shape[0]

    def body(pick_ref, c0_ref, c1_ref):
        t0, t1 = slots(pick_ref, cap)
        lanes = iota((toks, rows), 1)
        c0_ref[...] = (lanes == t0).astype(F32).astype(BF16)
        c1_ref[...] = (lanes == t1).astype(F32).astype(BF16)

    return kernel(body, ((toks, rows), (toks, rows)), pick)


def project(conv_all, out_weight, residual, ct):
    toks, width = residual.shape
    rows = ct.shape[0]

    def body(conv_ref, w_ref, res_ref, ct_ref, stream_ref, out_ref):
        stream = (res_ref[...].astype(F32) + dot(conv_ref[...], w_ref[...], 0, 0)).astype(BF16)
        stream_ref[...] = stream
        out_ref[...] = dot(ct_ref[...], stream).astype(BF16)

    outs = ((toks, width), (rows, width))
    return kernel(body, outs, conv_all, out_weight, residual, ct)


def order_map(cap, block, splitting):
    q = iota((block, 1), 0)
    if splitting:
        core = (q >= block // 2).astype(jnp.int32)
        within = q - core * (block // 2)
        z = (within * (65536 // cap + 1)) >> 16
        source = within + z * cap + core * cap
    else:
        z = (q * (65536 // (2 * cap) + 1)) >> 16
        rest = q - z * (2 * cap)
        core = (rest >= cap).astype(jnp.int32)
        source = core * (block // 2) + z * cap + rest - core * cap
    return (iota((block, block), 1) == source).astype(F32).astype(BF16)


def split_rows(got, n_tx, cap):
    rows, width = got.shape
    half = rows // 2
    block = 8 * cap
    part = block // 2

    def body(got_ref, out_ref):
        order = order_map(cap, block, True)
        for i in range(rows // block):
            both = dot(order, got_ref[i * block : (i + 1) * block]).astype(BF16)
            for core in range(2):
                for t in range(n_tx):
                    out_ref[core * n_tx + t, i * part : (i + 1) * part] = both[
                        core * part : (core + 1) * part
                    ]

    return kernel(body, ((2 * n_tx, half, width),), got)


def pack(where, w_gate, w_up, n_ty):
    dim, hid = w_gate.shape
    feats = dim // n_ty

    def body(at_ref, wg_ref, wu_ref, *out_refs):
        for d, out_ref in enumerate(out_refs):
            to = lax.rem(at_ref[0] + (d + 1), n_ty)
            rows = pl.ds(pl.multiple_of(to * feats, feats), feats)
            out_ref[:, :hid] = wg_ref[rows, :]
            out_ref[:, hid:] = wu_ref[rows, :]

    outs = tuple((feats, 2 * hid) for _ in range(n_ty - 1))
    return kernel(body, outs, where, w_gate, w_up)


def gate_up(where, x, gain, w_gate, w_up, pieces):
    n_ty = len(pieces) + 1
    groups, half, width = x.shape
    n_tx = groups // 2
    feats = n_tx * width
    hid = w_gate.shape[1]
    rows = 2 * half

    def body(at_ref, x_ref, gain_ref, wg_ref, wu_ref, *rest):
        piece_refs, out_ref = rest[:-1], rest[-1]
        ty = at_ref[0]
        mine = pl.ds(pl.multiple_of(at_ref[0] * feats, feats), feats)
        gain_row = gain_ref[:, mine].astype(F32)
        extra = jnp.zeros((8, 2 * hid), F32)
        place = iota((8, 2 * hid), 0)
        for core in range(2):
            raw = jnp.concatenate([x_ref[core * n_tx + t] for t in range(n_tx)], axis=1).astype(F32)
            squares = jnp.sum(raw * raw, axis=1, keepdims=True)
            y = (raw * gain_row).astype(BF16)
            for k in range(2):
                row = to_row(squares, 2 * hid, k * 2 * hid)
                high = row.astype(BF16).astype(F32)
                at = core * 2 + k
                extra = jnp.where(place == at, high, extra)
                extra = jnp.where(place == at + 4, row - high, extra)
            keep = slice(core * half, (core + 1) * half)
            out_ref[ty, keep, 0:hid] = dot(y, wg_ref[mine, :]).astype(BF16)
            out_ref[ty, keep, hid : 2 * hid] = dot(y, wu_ref[mine, :]).astype(BF16)
            for d in range(1, n_ty):
                to = lax.rem(ty + (n_ty - d), n_ty)
                out_ref[to, keep, :] = dot(y, piece_refs[d - 1][...]).astype(BF16)
        for to in range(n_ty):
            out_ref[to, rows : rows + 8, :] = extra.astype(BF16)

    outs = ((n_ty, rows + 8, 2 * hid),)
    return kernel(body, outs, where, x, gain, w_gate, w_up, *pieces, limit=24)


def activate(parts, full_dim):
    n_ty, padded, both = parts.shape
    rows, hid = padded - 8, both // 2
    half = rows // 2

    def body(p_ref, out_ref):
        extra = sum(p_ref[k, rows : rows + 8, :].astype(F32) for k in range(n_ty))
        for core in range(2):
            keep = slice(core * half, (core + 1) * half)
            total = sum(p_ref[k, keep, :].astype(F32) for k in range(n_ty))
            squares = jnp.zeros((half, 1), F32)
            for k in range(2):
                at = core * 2 + k
                row = extra[at : at + 1] + extra[at + 4 : at + 5]
                squares = squares + to_col(row, half, k * both)
            total = total * lax.rsqrt(squares / full_dim + NORM_EPS)
            gate, up = total[:, :hid], total[:, hid:]
            hidden = (gate / (1.0 + jnp.exp(-gate)) * up).astype(BF16)
            for k in range(n_ty):
                out_ref[k, keep, :] = hidden

    return kernel(body, ((n_ty, rows, hid),), parts)


def down(where, hidden, w_down, pieces):
    n_ty, rows, _ = hidden.shape
    n_tx = len(pieces) + 1
    half = rows // 2
    width = w_down.shape[-1]

    def body(at_ref, h_ref, wd_ref, *rest):
        piece_refs, out_ref = rest[:-1], rest[-1]
        tx = at_ref[1]
        h = jnp.concatenate([h_ref[k] for k in range(n_ty)], axis=1)
        for d in range(n_tx):
            w = [wd_ref[b, tx] if d == 0 else piece_refs[d - 1][b] for b in range(n_ty)]
            part = dot(h, jnp.concatenate(w, axis=0)).astype(BF16)
            to = lax.rem(tx + (n_tx - d), n_tx)
            out_ref[to] = part[:half]
            out_ref[n_tx + to] = part[half:]

    outs = ((2 * n_tx, half, width),)
    return kernel(body, outs, where, hidden, w_down, *pieces, limit=24)


def join_rows(parts, cap):
    groups, half, width = parts.shape
    n_tx = groups // 2
    block = 8 * cap
    part = block // 2

    def body(p_ref, out_ref):
        order = order_map(cap, block, False)
        for i in range(2 * half // block):
            keep = slice(i * part, (i + 1) * part)
            both = [
                sum(p_ref[core * n_tx + t, keep].astype(F32) for t in range(n_tx)).astype(BF16)
                for core in range(2)
            ]
            out_ref[i * block : (i + 1) * block] = dot(
                order, jnp.concatenate(both, axis=0)
            ).astype(BF16)

    return kernel(body, ((2 * half, width),), parts)


def combine(back, c0, c1, weights, stream):
    def body(back_ref, c0_ref, c1_ref, w_ref, stream_ref, out_ref):
        rows = back_ref[...]
        feed = dot(c0_ref[...], rows) * w_ref[:, 0:1] + dot(c1_ref[...], rows) * w_ref[:, 1:2]
        out_ref[...] = (stream_ref[...].astype(F32) + feed).astype(BF16)

    return kernel(body, (stream.shape,), back, c0, c1, weights, stream)


def shifted(value, axis, steps):
    count = lax.axis_size(axis)
    return lax.ppermute(value, axis, [(i, (i + steps) % count) for i in range(count)])


def local(
    b_gate,
    c_gate,
    h_in,
    docs,
    conv_taps,
    out_weight,
    residual_in,
    norm_gain,
    expert_pick,
    route_weight,
    w_gate,
    w_up,
    w_down,
):
    toks, chans = h_in.shape
    width = residual_in.shape[1]
    full_dim = w_gate.shape[1]
    hid = w_gate.shape[2]
    n_z, n_ty, n_tx = (lax.axis_size(a) for a in ("z", "ty", "tx"))
    n_sp = 2 * n_z
    cap = 5 * toks // (2 * n_sp)
    rows = n_sp * cap
    sp_index = lax.axis_index(("z", "core"))
    ty, tx = lax.axis_index("ty"), lax.axis_index("tx")
    tp_index = ty * n_tx + tx
    where = jnp.stack([ty, tx]).astype(jnp.int32)

    product = (c_gate.astype(F32) * h_in.astype(F32)).astype(BF16)
    edge = lax.ppermute(
        product[toks - 2 :], ("z", "core"), [(i, i + 1) for i in range(n_sp - 1)]
    )
    first_pos = sp_index * toks
    padded_docs = jnp.concatenate([jnp.full((2,), -1, jnp.int32), docs], axis=0)
    near = lax.dynamic_slice_in_dim(padded_docs, first_pos, toks + 2)
    taps = lax.dynamic_slice_in_dim(conv_taps, tp_index * chans, chans, 1).astype(F32)
    extended = jnp.concatenate([edge, product], axis=0).astype(F32)
    conv_sum = taps[0][None, :] * extended[2:]
    for back in (1, 2):
        same = (near[2 - back : 2 - back + toks] == near[2:]).astype(F32)[:, None]
        conv_sum = conv_sum + taps[back][None, :] * extended[2 - back : 2 - back + toks] * same
    conv = (b_gate.astype(F32) * conv_sum).astype(BF16)
    n_tp = n_ty * n_tx
    conv_copies = jnp.broadcast_to(conv.T[None], (n_tp, chans, toks))
    conv_all = lax.all_to_all(conv_copies, TP, 0, 0, tiled=True)
    conv_all = conv_all.reshape(n_tp * chans, toks)

    packed = pack(where, w_gate[0], w_up[0], n_ty)
    gate_up_pieces = [shifted(p, "ty", d + 1) for d, p in enumerate(packed)]
    w_down4 = w_down[0].reshape(n_ty, n_tx, hid, width)
    down_pieces = []
    for d in range(1, n_tx):
        to = lax.rem(tx + d, n_tx)
        piece = lax.dynamic_index_in_dim(w_down4, to, 1, keepdims=False)
        down_pieces.append(shifted(piece, "tx", d))

    ct = routing_out(expert_pick, rows, cap)
    stream, outgoing = project(conv_all, out_weight, residual_in, ct)
    got = lax.all_to_all(
        outgoing.reshape(n_z, 2 * cap, width), "z", 0, 0, tiled=True
    ).reshape(rows, width)
    got, gate_up_pieces = lax.optimization_barrier((got, gate_up_pieces))
    split = split_rows(got, n_tx, cap)
    x = lax.all_to_all(split, ("core", "tx"), 0, 0, tiled=True)
    parts = gate_up(
        where, x, norm_gain.reshape(1, -1), w_gate[0], w_up[0], gate_up_pieces
    )
    parts = lax.all_to_all(parts, "ty", 0, 0, tiled=True)
    hidden = lax.all_to_all(activate(parts, full_dim), "ty", 0, 0, tiled=True)
    outs = lax.all_to_all(
        down(where, hidden, w_down4, down_pieces), ("core", "tx"), 0, 0, tiled=True
    )
    outs, late_pick, late_weight = lax.optimization_barrier((outs, expert_pick, route_weight))
    c0, c1 = routing_back(late_pick, rows, cap)
    back = lax.all_to_all(
        join_rows(outs, cap).reshape(n_z, 2 * cap, width), "z", 0, 0, tiled=True
    ).reshape(rows, width)
    return combine(back, c0, c1, late_weight, stream)


def solution(mesh):
    finer = Mesh(
        mesh.devices.reshape(mesh.shape["sp"] // 2, 2, 4, 4), ("z", "core", "ty", "tx")
    )
    sp = ("z", "core")
    placed = (
        P(sp, TP),
        P(sp, TP),
        P(sp, TP),
        P(),
        P(),
        P(None, TP),
        P(sp, TP),
        P(),
        P(sp, None),
        P(sp, None),
        P(sp, None, TP),
        P(sp, None, TP),
        P(sp, None, TP),
    )

    return jax.shard_map(local, mesh=finer, in_specs=placed, out_specs=P(sp, TP), check_vma=False)
```

profile of v0, /device:TPU:8, one launch (start us, length us, event | category | flops | bytes accessed | tf_op | source)
XLA Modules:
  0.0 208.1 jit_solution(3485691100178249800)
XLA Ops:
  0.0 0.8 multiply_convert_fusion
  0.8 0.1 slice.41
  0.9 1.7 collective-permute-start
  2.6 0.8 pad_dynamic-slice_fusion
  3.4 0.1 compare_convert_fusion.1
  3.5 0.8 dynamic-slice_convert_fusion
  4.2 0.0 collective-permute-done
  4.3 0.1 maximum_convert_fusion
  4.3 0.9 fusion.6
  5.2 0.8 broadcast_in_dim.2
  6.1 8.7 %all-to-all-start = ((bf16[16,64,256]{2,1,0:T(8,128)(2,1)}), bf16[16,64,256]{2,1,0:T(8,128)(2,1)S(1)}, u32[]{:S(2)}, u32[]{:S(2)}) async-start(bf16[16,64,256]{2,1,0:T(8,128)(2,1)} %broadcast_in_dim.2), calls=%async_computation | async-start | bytes 1048576 | tf_op jit(solution)/shard_map/all_to_all | solution.py:312
  14.8 0.0 copy-done.14
  14.8 0.1 copy.14.pick_ref
  14.9 0.0 copy-start
  15.0 0.0 copy-start.1
  15.0 0.7 shard_map.127.ct_ref
  15.7 9.1 %all-to-all-done = bf16[16,64,256]{2,1,0:T(8,128)(2,1)S(1)} async-done(((bf16[16,64,256]{2,1,0:T(8,128)(2,1)}), bf16[16,64,256]{2,1,0:T(8,128)(2,1)S(1)}, u32[]{:S(2)}, u32[]{:S(2)}) %all-to-all-start) | async-done | bytes 524320 | tf_op jit(solution)/shard_map/all_to_all | solution.py:312
  24.8 0.0 copy-done.10
  24.8 1.0 copy-done.3
  25.8 1.4 shard_map.128
  27.3 14.8 %all-to-all-start.1 = ((bf16[16,40,256]{2,1,0:T(8,128)(2,1)}), bf16[16,40,256]{2,1,0:T(8,128)(2,1)S(1)}, u32[]{:S(2)}, u32[]{:S(2)}) async-start(bf16[16,40,256]{2,1,0:T(8,128)(2,1)} %bitcast.7), calls=%async_computation.1 | async-start | bytes 655360 | tf_op jit(solution)/shard_map/all_to_all | solution.py:326
  42.1 0.1 pad_add_fusion.at_ref
  42.2 0.0 copy-done
  42.2 0.0 copy-done.1
  42.2 0.8 shard_map.129
  43.1 2.8 %collective-permute-start.1 = (bf16[1024,256]{1,0:T(8,128)(2,1)S(1)}, bf16[1024,256]{1,0:T(8,128)(2,1)S(1)}, u32[]{:S(2)}, u32[]{:S(2)}) collective-permute-start(bf16[1024,256]{1,0:T(8,128)(2,1)S(1)} %get-tuple-element.20), channel_id=1, source_target_pairs={{0,4},{4,8},{8,12},{12,0},{1,5},{5,9},{9,13},{13,1},{2,6},{6,10},{... | collective-permute-start | bytes 1572872 | tf_op jit(solution)/shard_map/ppermute | solution.py:265
  45.9 5.2 %collective-permute-start.2 = (bf16[1024,256]{1,0:T(8,128)(2,1)S(1)}, bf16[1024,256]{1,0:T(8,128)(2,1)S(1)}, u32[]{:S(2)}, u32[]{:S(2)}) collective-permute-start(bf16[1024,256]{1,0:T(8,128)(2,1)S(1)} %get-tuple-element.21), channel_id=1, source_target_pairs={{0,8},{4,12},{8,0},{12,4},{1,9},{5,13},{9,1},{13,5},{2,10},{6,14},... | collective-permute-start | bytes 1572872 | tf_op jit(solution)/shard_map/ppermute | solution.py:265
  51.1 2.2 %collective-permute-start.3 = (bf16[1024,256]{1,0:T(8,128)(2,1)S(1)}, bf16[1024,256]{1,0:T(8,128)(2,1)S(1)}, u32[]{:S(2)}, u32[]{:S(2)}) collective-permute-start(bf16[1024,256]{1,0:T(8,128)(2,1)S(1)} %get-tuple-element.22), channel_id=1, source_target_pairs={{0,12},{4,0},{8,4},{12,8},{1,13},{5,1},{9,5},{13,9},{2,14},{6,2},{... | collective-permute-start | bytes 1572872 | tf_op jit(solution)/shard_map/ppermute | solution.py:265
  53.3 6.6 %collective-permute-done.1.rest_0_ = bf16[1024,256]{1,0:T(8,128)(2,1)S(1)} collective-permute-done((bf16[1024,256]{1,0:T(8,128)(2,1)S(1)}, bf16[1024,256]{1,0:T(8,128)(2,1)S(1)}, u32[]{:S(2)}, u32[]{:S(2)}) %collective-permute-start.1) | collective-permute-done | bytes 524320 | tf_op jit(solution)/shard_map/ppermute | solution.py:265
  59.9 4.3 %collective-permute-done.2.rest_1_ = bf16[1024,256]{1,0:T(8,128)(2,1)S(1)} collective-permute-done((bf16[1024,256]{1,0:T(8,128)(2,1)S(1)}, bf16[1024,256]{1,0:T(8,128)(2,1)S(1)}, u32[]{:S(2)}, u32[]{:S(2)}) %collective-permute-start.2) | collective-permute-done | bytes 524320 | tf_op jit(solution)/shard_map/ppermute | solution.py:265
  64.1 0.8 copy-done.6
  64.9 7.8 %collective-permute-done.3.rest_2_ = bf16[1024,256]{1,0:T(8,128)(2,1)S(1)} collective-permute-done((bf16[1024,256]{1,0:T(8,128)(2,1)S(1)}, bf16[1024,256]{1,0:T(8,128)(2,1)S(1)}, u32[]{:S(2)}, u32[]{:S(2)}) %collective-permute-start.3) | collective-permute-done | bytes 524320 | tf_op jit(solution)/shard_map/ppermute | solution.py:265
  72.7 0.8 copy-done.8
  73.5 0.0 all-to-all-done.1
  73.5 1.3 shard_map.130
  74.8 3.6 %all-to-all-start.2 = ((bf16[8,320,256]{2,1,0:T(8,128)(2,1)}), bf16[8,320,256]{2,1,0:T(8,128)(2,1)S(1)}, u32[]{:S(2)}, u32[]{:S(2)}) async-start(bf16[8,320,256]{2,1,0:T(8,128)(2,1)} %shard_map.130), calls=%async_computation.2 | async-start | bytes 2621440 | tf_op jit(solution)/shard_map/all_to_all | solution.py:331
  78.4 0.7 reshape.24.gain_ref
  79.1 17.3 %all-to-all-done.2.x_ref = bf16[8,320,256]{2,1,0:T(8,128)(2,1)S(1)} async-done(((bf16[8,320,256]{2,1,0:T(8,128)(2,1)}), bf16[8,320,256]{2,1,0:T(8,128)(2,1)S(1)}, u32[]{:S(2)}, u32[]{:S(2)}) %all-to-all-start.2) | async-done | bytes 1310752 | tf_op jit(solution)/shard_map/all_to_all | solution.py:331
  96.4 1.0 copy-done.5
  97.4 1.0 copy-done.7
  98.5 1.0 copy-done.9
  99.5 0.6 copy-done.12
  100.1 2.4 %shard_map.131 = bf16[4,648,256]{2,1,0:T(8,128)(2,1)S(1)} custom-call(s32[2]{0:T(128)S(1)} %copy-done.12, bf16[8,320,256]{2,1,0:T(8,128)(2,1)S(1)} %all-to-all-done.2.x_ref, bf16[1,4096]{1,0:T(2,128)(2,1)S(1)} %reshape.24.gain_ref, bf16[4096,128]{1,0:T(8,128)(2,1)S(1)} %bitcast.25, bf16[4096,128]{1,0:T(8,128)(2,1)S(1)} %bitcast.27, ...), custom_call_target="tpu_custom_call" | custom-call | tf_op jit(solution)/shard_map/pallas_call | solution.py:23
  102.5 22.5 %all_to_all.35.p_ref = bf16[4,648,256]{2,1,0:T(8,128)(2,1)S(1)} all-to-all(bf16[4,648,256]{2,1,0:T(8,128)(2,1)S(1)} %shard_map.131), channel_id=1, replica_groups=mesh['z'=16,'core'=2,'ty'=4,'tx'=4] {'ty'}, dimensions={0} | all-to-all | bytes 2654208 | tf_op jit(solution)/shard_map/all_to_all | solution.py:335
  125.0 1.2 shard_map.132
  126.2 5.0 %all-to-all-start.4 = ((bf16[4,640,128]{2,1,0:T(8,128)(2,1)}), bf16[4,640,128]{2,1,0:T(8,128)(2,1)S(1)}, u32[]{:S(2)}, u32[]{:S(2)}) async-start(bf16[4,640,128]{2,1,0:T(8,128)(2,1)} %shard_map.132), calls=%async_computation.4 | async-start | bytes 1310720 | tf_op jit(solution)/shard_map/all_to_all | solution.py:336
  131.3 0.1 dynamic-slice_bitcast_fusion
  131.3 2.8 %collective-permute-start.4 = (bf16[4,128,256]{2,1,0:T(8,128)(2,1)S(1)}, bf16[4,128,256]{2,1,0:T(8,128)(2,1)S(1)}, u32[]{:S(2)}, u32[]{:S(2)}) collective-permute-start(bf16[4,128,256]{2,1,0:T(8,128)(2,1)S(1)} %get-tuple-element.35), channel_id=1, source_target_pairs={{0,1},{1,2},{2,3},{3,0},{4,5},{5,6},{6,7},{7,4},{8,9},{9,10},{10,1... | collective-permute-start | bytes 786440 | tf_op jit(solution)/shard_map/ppermute | solution.py:265
  134.1 3.7 %collective-permute-start.5 = (bf16[4,128,256]{2,1,0:T(8,128)(2,1)S(1)}, bf16[4,128,256]{2,1,0:T(8,128)(2,1)S(1)}, u32[]{:S(2)}, u32[]{:S(2)}) collective-permute-start(bf16[4,128,256]{2,1,0:T(8,128)(2,1)S(1)} %get-tuple-element.34), channel_id=1, source_target_pairs={{0,2},{1,3},{2,0},{3,1},{4,6},{5,7},{6,4},{7,5},{8,10},{9,11},{10,... | collective-permute-start | bytes 786440 | tf_op jit(solution)/shard_map/ppermute | solution.py:265
  137.8 2.8 %collective-permute-start.6 = (bf16[4,128,256]{2,1,0:T(8,128)(2,1)S(1)}, bf16[4,128,256]{2,1,0:T(8,128)(2,1)S(1)}, u32[]{:S(2)}, u32[]{:S(2)}) collective-permute-start(bf16[4,128,256]{2,1,0:T(8,128)(2,1)S(1)} %get-tuple-element.33), channel_id=1, source_target_pairs={{0,3},{1,0},{2,1},{3,2},{4,7},{5,4},{6,5},{7,6},{8,11},{9,8},{10,9... | collective-permute-start | bytes 786440 | tf_op jit(solution)/shard_map/ppermute | solution.py:265
  140.6 6.4 %collective-permute-done.4.rest_0_ = bf16[4,128,256]{2,1,0:T(8,128)(2,1)S(1)} collective-permute-done((bf16[4,128,256]{2,1,0:T(8,128)(2,1)S(1)}, bf16[4,128,256]{2,1,0:T(8,128)(2,1)S(1)}, u32[]{:S(2)}, u32[]{:S(2)}) %collective-permute-start.4) | collective-permute-done | bytes 262176 | tf_op jit(solution)/shard_map/ppermute | solution.py:265
  147.1 0.0 collective-permute-done.5.rest_1_
  147.1 2.5 %collective-permute-done.6.rest_2_ = bf16[4,128,256]{2,1,0:T(8,128)(2,1)S(1)} collective-permute-done((bf16[4,128,256]{2,1,0:T(8,128)(2,1)S(1)}, bf16[4,128,256]{2,1,0:T(8,128)(2,1)S(1)}, u32[]{:S(2)}, u32[]{:S(2)}) %collective-permute-start.6) | collective-permute-done | bytes 262176 | tf_op jit(solution)/shard_map/ppermute | solution.py:265
  149.6 0.0 all-to-all-done.4.h_ref
  149.6 0.0 copy-done.13
  149.6 1.4 shard_map.133
  151.0 21.8 %all_to_all.36.p_ref = bf16[8,320,256]{2,1,0:T(8,128)(2,1)S(1)} all-to-all(bf16[8,320,256]{2,1,0:T(8,128)(2,1)S(1)} %shard_map.133), channel_id=1, replica_groups=mesh['z'=16,'core'=2,'ty'=4,'tx'=4] {'core','tx'}, dimensions={0} | all-to-all | bytes 2621440 | tf_op jit(solution)/shard_map/all_to_all | solution.py:337
  172.8 1.1 shard_map.134
  173.9 11.7 %all-to-all-start.6 = ((bf16[16,40,256]{2,1,0:T(8,128)(2,1)}), bf16[16,40,256]{2,1,0:T(8,128)(2,1)S(1)}, u32[]{:S(2)}, u32[]{:S(2)}) async-start(bf16[16,40,256]{2,1,0:T(8,128)(2,1)} %bitcast.15), calls=%async_computation.6 | async-start | bytes 655360 | tf_op jit(solution)/shard_map/all_to_all | solution.py:342
  185.7 0.1 copy.15.pick_ref
  185.8 0.5 shard_map.135
  186.4 0.1 copy.16.w_ref
  186.5 20.6 %all-to-all-done.6 = bf16[16,40,256]{2,1,0:T(8,128)(2,1)S(1)} async-done(((bf16[16,40,256]{2,1,0:T(8,128)(2,1)}), bf16[16,40,256]{2,1,0:T(8,128)(2,1)S(1)}, u32[]{:S(2)}, u32[]{:S(2)}) %all-to-all-start.6) | async-done | bytes 327712 | tf_op jit(solution)/shard_map/all_to_all | solution.py:342
  207.1 1.0 shard_map.136
  (21 shorter events, 0.0 us)
Async XLA Ops:
  0.0 14.8 %copy-start.14 = (s32[256,2]{0,1:T(2,128)S(1)}, s32[256,2]{0,1:T(2,128)}, u32[]{:S(2)}) copy-start(s32[256,2]{0,1:T(2,128)} %param.21) | copy-start | bytes 6148
  0.9 3.4 %collective-permute-start = (bf16[2,64]{0,1:T(8,128)(2,1)S(1)}, bf16[2,64]{0,1:T(8,128)(2,1)S(1)}, u32[]{:S(2)}, u32[]{:S(2)}) collective-permute-start(bf16[2,64]{0,1:T(8,128)(2,1)S(1)} %slice.41), channel_id=1, source_target_pairs={{0,16},{16,32},{32,48},{48,64},{64,80},{80,96},{96,112},{112,128},... | collective-permute-start | bytes 776 | tf_op jit(solution)/shard_map/ppermute | solution.py:297
  4.2 20.6 %copy-start.10 = (bf16[256,256]{1,0:T(8,128)(2,1)S(1)}, bf16[256,256]{1,0:T(8,128)(2,1)}, u32[]{:S(2)}) copy-start(bf16[256,256]{1,0:T(8,128)(2,1)} %res_ref.1) | copy-start | bytes 393220
  6.1 18.7 %all-to-all-start = ((bf16[16,64,256]{2,1,0:T(8,128)(2,1)}), bf16[16,64,256]{2,1,0:T(8,128)(2,1)S(1)}, u32[]{:S(2)}, u32[]{:S(2)}) async-start(bf16[16,64,256]{2,1,0:T(8,128)(2,1)} %broadcast_in_dim.2), calls=%async_computation | async-start | bytes 1048576 | tf_op jit(solution)/shard_map/all_to_all | solution.py:312
  14.9 27.3 %copy-start = (bf16[1,4096,128]{2,1,0:T(8,128)(2,1)S(1)}, bf16[1,4096,128]{2,1,0:T(8,128)(2,1)}, u32[]{:S(2)}) copy-start(bf16[1,4096,128]{2,1,0:T(8,128)(2,1)} %param.23) | copy-start | bytes 3145732
  15.0 27.3 %copy-start.1 = (bf16[1,4096,128]{2,1,0:T(8,128)(2,1)S(1)}, bf16[1,4096,128]{2,1,0:T(8,128)(2,1)}, u32[]{:S(2)}) copy-start(bf16[1,4096,128]{2,1,0:T(8,128)(2,1)} %param.24) | copy-start | bytes 3145732
  24.8 1.0 copy-start.3
  27.3 46.2 %all-to-all-start.1 = ((bf16[16,40,256]{2,1,0:T(8,128)(2,1)}), bf16[16,40,256]{2,1,0:T(8,128)(2,1)S(1)}, u32[]{:S(2)}, u32[]{:S(2)}) async-start(bf16[16,40,256]{2,1,0:T(8,128)(2,1)} %bitcast.7), calls=%async_computation.1 | async-start | bytes 655360 | tf_op jit(solution)/shard_map/all_to_all | solution.py:326
  42.2 0.8 copy-start.11
  43.1 16.8 %collective-permute-start.1 = (bf16[1024,256]{1,0:T(8,128)(2,1)S(1)}, bf16[1024,256]{1,0:T(8,128)(2,1)S(1)}, u32[]{:S(2)}, u32[]{:S(2)}) collective-permute-start(bf16[1024,256]{1,0:T(8,128)(2,1)S(1)} %get-tuple-element.20), channel_id=1, source_target_pairs={{0,4},{4,8},{8,12},{12,0},{1,5},{5,9},{9,13},{13,1},{2,6},{6,10},{... | collective-permute-start | bytes 1572872 | tf_op jit(solution)/shard_map/ppermute | solution.py:265
  45.9 18.2 %collective-permute-start.2 = (bf16[1024,256]{1,0:T(8,128)(2,1)S(1)}, bf16[1024,256]{1,0:T(8,128)(2,1)S(1)}, u32[]{:S(2)}, u32[]{:S(2)}) collective-permute-start(bf16[1024,256]{1,0:T(8,128)(2,1)S(1)} %get-tuple-element.21), channel_id=1, source_target_pairs={{0,8},{4,12},{8,0},{12,4},{1,9},{5,13},{9,1},{13,5},{2,10},{6,14},... | collective-permute-start | bytes 1572872 | tf_op jit(solution)/shard_map/ppermute | solution.py:265
  51.1 21.6 %collective-permute-start.3 = (bf16[1024,256]{1,0:T(8,128)(2,1)S(1)}, bf16[1024,256]{1,0:T(8,128)(2,1)S(1)}, u32[]{:S(2)}, u32[]{:S(2)}) collective-permute-start(bf16[1024,256]{1,0:T(8,128)(2,1)S(1)} %get-tuple-element.22), channel_id=1, source_target_pairs={{0,12},{4,0},{8,4},{12,8},{1,13},{5,1},{9,5},{13,9},{2,14},{6,2},{... | collective-permute-start | bytes 1572872 | tf_op jit(solution)/shard_map/ppermute | solution.py:265
  59.9 15.0 %copy-start.4 = (bf16[1024,256]{1,0:T(8,128)(2,1)}, bf16[1024,256]{1,0:T(8,128)(2,1)S(1)}, u32[]{:S(2)}) copy-start(bf16[1024,256]{1,0:T(8,128)(2,1)S(1)} %collective-permute-done.1.rest_0_) | copy-start | bytes 1572868
  64.1 0.8 copy-start.6
  72.7 0.8 copy-start.8
  74.8 21.6 %all-to-all-start.2 = ((bf16[8,320,256]{2,1,0:T(8,128)(2,1)}), bf16[8,320,256]{2,1,0:T(8,128)(2,1)S(1)}, u32[]{:S(2)}, u32[]{:S(2)}) async-start(bf16[8,320,256]{2,1,0:T(8,128)(2,1)} %shard_map.130), calls=%async_computation.2 | async-start | bytes 2621440 | tf_op jit(solution)/shard_map/all_to_all | solution.py:331
  96.4 1.0 copy-start.5
  97.4 1.0 copy-start.7
  98.5 1.0 copy-start.9
  99.5 0.6 copy-start.12
  125.0 6.3 %copy-start.2 = (bf16[1,2048,256]{2,1,0:T(8,128)(2,1)S(1)}, bf16[1,2048,256]{2,1,0:T(8,128)(2,1)}, u32[]{:S(2)}) copy-start(bf16[1,2048,256]{2,1,0:T(8,128)(2,1)} %param.25) | copy-start | bytes 3145732
  126.2 23.3 %copy-start.13 = (s32[2]{0:T(128)S(1)}, s32[2]{0:T(128)}, u32[]{:S(2)}) copy-start(s32[2]{0:T(128)} %copy-done.11) | copy-start | bytes 28
  126.2 23.3 %all-to-all-start.4 = ((bf16[4,640,128]{2,1,0:T(8,128)(2,1)}), bf16[4,640,128]{2,1,0:T(8,128)(2,1)S(1)}, u32[]{:S(2)}, u32[]{:S(2)}) async-start(bf16[4,640,128]{2,1,0:T(8,128)(2,1)} %shard_map.132), calls=%async_computation.4 | async-start | bytes 1310720 | tf_op jit(solution)/shard_map/all_to_all | solution.py:336
  131.3 15.7 %collective-permute-start.4 = (bf16[4,128,256]{2,1,0:T(8,128)(2,1)S(1)}, bf16[4,128,256]{2,1,0:T(8,128)(2,1)S(1)}, u32[]{:S(2)}, u32[]{:S(2)}) collective-permute-start(bf16[4,128,256]{2,1,0:T(8,128)(2,1)S(1)} %get-tuple-element.35), channel_id=1, source_target_pairs={{0,1},{1,2},{2,3},{3,0},{4,5},{5,6},{6,7},{7,4},{8,9},{9,10},{10,1... | collective-permute-start | bytes 786440 | tf_op jit(solution)/shard_map/ppermute | solution.py:265
  134.1 13.0 %collective-permute-start.5 = (bf16[4,128,256]{2,1,0:T(8,128)(2,1)S(1)}, bf16[4,128,256]{2,1,0:T(8,128)(2,1)S(1)}, u32[]{:S(2)}, u32[]{:S(2)}) collective-permute-start(bf16[4,128,256]{2,1,0:T(8,128)(2,1)S(1)} %get-tuple-element.34), channel_id=1, source_target_pairs={{0,2},{1,3},{2,0},{3,1},{4,6},{5,7},{6,4},{7,5},{8,10},{9,11},{10,... | collective-permute-start | bytes 786440 | tf_op jit(solution)/shard_map/ppermute | solution.py:265
  137.8 11.7 %collective-permute-start.6 = (bf16[4,128,256]{2,1,0:T(8,128)(2,1)S(1)}, bf16[4,128,256]{2,1,0:T(8,128)(2,1)S(1)}, u32[]{:S(2)}, u32[]{:S(2)}) collective-permute-start(bf16[4,128,256]{2,1,0:T(8,128)(2,1)S(1)} %get-tuple-element.33), channel_id=1, source_target_pairs={{0,3},{1,0},{2,1},{3,2},{4,7},{5,4},{6,5},{7,6},{8,11},{9,8},{10,9... | collective-permute-start | bytes 786440 | tf_op jit(solution)/shard_map/ppermute | solution.py:265
  172.8 12.9 %copy-start.15 = (s32[256,2]{0,1:T(2,128)S(1)}, s32[256,2]{0,1:T(2,128)}, u32[]{:S(2)}) copy-start(s32[256,2]{0,1:T(2,128)} %param.21) | copy-start | bytes 6148
  172.8 13.6 %copy-start.16 = (f32[256,2]{0,1:T(2,128)S(1)}, f32[256,2]{0,1:T(2,128)}, u32[]{:S(2)}) copy-start(f32[256,2]{0,1:T(2,128)} %param.22) | copy-start | bytes 6148
  173.9 33.1 %all-to-all-start.6 = ((bf16[16,40,256]{2,1,0:T(8,128)(2,1)}), bf16[16,40,256]{2,1,0:T(8,128)(2,1)S(1)}, u32[]{:S(2)}, u32[]{:S(2)}) async-start(bf16[16,40,256]{2,1,0:T(8,128)(2,1)} %bitcast.15), calls=%async_computation.6 | async-start | bytes 655360 | tf_op jit(solution)/shard_map/all_to_all | solution.py:342
where the time goes:
time: 209 us; the launch traced here: 208 us
  waiting for transfers between devices  74.6 us (36%)
  starting transfers between devices  65.1 us (31%)
  blocking collectives  44.3 us (21%)
  Pallas kernels  12 us (6%)
  local copies, waits for them, and re-layouts  9.24 us (4%)
  other arithmetic  2.67 us (1%)
    ppermute x6, waiting for transfers between devices, shifted(): lax.ppermute(value, axis, [(i, (i + steps) % count) for i in range(count)])  27.6 us
    all_to_all x1, blocking collectives, local(): parts = lax.all_to_all(parts, 'ty', 0, 0, tiled=True)  22.5 us
    all_to_all x1, blocking collectives, local(): lax.all_to_all(down(where, hidden, w_down4, down_pieces), ('core', 'tx'),...  21.8 us
    all_to_all x1, waiting for transfers between devices, local(): lax.all_to_all(join_rows(outs, cap).reshape(n_z, 2 * cap, width), 'z', 0,...  20.6 us
    ppermute x6, starting transfers between devices, shifted(): lax.ppermute(value, axis, [(i, (i + steps) % count) for i in range(count)])  19.4 us
    all_to_all x1, waiting for transfers between devices, local(): x = lax.all_to_all(split, ('core', 'tx'), 0, 0, tiled=True)  17.3 us
    all_to_all x1, starting transfers between devices, local(): lax.all_to_all(outgoing.reshape(n_z, 2 * cap, width), 'z', 0, 0, tiled=True)  14.8 us
    pallas_call x10, Pallas kernels, kernel(): pl.pallas_call(body, out_shape=tuple((jax.ShapeDtypeStruct(o, BF16) for o...  12 us
  transfers between devices with their start and end apart: 12, of which 8 were waited for; matrix products, arithmetic and copies ran while one was open for 1% of the time, Pallas kernels for 1%

commit v1 on v0

--- a/solution.py
+++ b/solution.py
@@ -16,17 +16,15 @@
     return lax.dot_general(a, b, (((ca,), (cb,)), ((), ())), preferred_element_type=F32)
 
 
-def kernel(body, outs, *args, limit=12):
-    held = [a if a.ndim == 1 else pltpu.with_memory_space_constraint(a, pltpu.VMEM) for a in args]
+def kernel(body, outs, *args, limit=12, dtype=BF16):
     vmem = pl.BlockSpec(memory_space=pltpu.VMEM)
-    smem = pl.BlockSpec(memory_space=pltpu.SMEM)
     got = pl.pallas_call(
         body,
-        out_shape=tuple(jax.ShapeDtypeStruct(o, BF16) for o in outs),
-        in_specs=[smem if a.ndim == 1 else vmem for a in args],
+        out_shape=tuple(jax.ShapeDtypeStruct(o, dtype) for o in outs),
+        in_specs=[vmem for a in args],
         out_specs=tuple(vmem for o in outs),
-        compiler_params=pltpu.CompilerParams(vmem_limit_bytes=limit << 20),
-    )(*held)
+        compiler_params=pltpu.CompilerParams(vmem_limit_bytes=limit << 20 if limit else None),
+    )(*args)
     return got if len(outs) > 1 else got[0]
 
 
@@ -60,17 +58,15 @@
     return jnp.where(s0 < cap, e0 * cap + s0, -1), jnp.where(s1 < cap, e1 * cap + s1, -1)
 
 
-def routing_out(pick, rows, cap):
+def routing_out(pick, cap):
     toks = pick.shape[0]
 
-    def body(pick_ref, ct_ref):
+    def body(pick_ref, out_ref):
         t0, t1 = slots(pick_ref, cap)
-        r0 = to_row(t0, toks, 0)
-        r1 = to_row(t1, toks, 0)
-        across = iota((rows, toks), 0)
-        ct_ref[...] = jnp.logical_or(across == r0, across == r1).astype(F32).astype(BF16)
-
-    return kernel(body, ((rows, toks),), pick)
+        place = iota((8, toks), 0)
+        out_ref[...] = jnp.where(place == 0, to_row(t0, toks, 0), to_row(t1, toks, 0))
+
+    return kernel(body, ((8, toks),), pick, dtype=jnp.int32)
 
 
 def routing_back(pick, rows, cap):
@@ -85,17 +81,40 @@
     return kernel(body, ((toks, rows), (toks, rows)), pick)
 
 
-def project(conv_all, out_weight, residual, ct):
+def project(conv_all, out_weight, residual, slot_rows, rows):
     toks, width = residual.shape
-    rows = ct.shape[0]
-
-    def body(conv_ref, w_ref, res_ref, ct_ref, stream_ref, out_ref):
+
+    def body(conv_ref, w_ref, res_ref, slot_ref, stream_ref, out_ref):
         stream = (res_ref[...].astype(F32) + dot(conv_ref[...], w_ref[...], 0, 0)).astype(BF16)
         stream_ref[...] = stream
-        out_ref[...] = dot(ct_ref[...], stream).astype(BF16)
+        across = iota((rows, toks), 0)
+        hit = jnp.logical_or(across == slot_ref[0:1, :], across == slot_ref[1:2, :])
+        out_ref[...] = dot(hit.astype(F32).astype(BF16), stream).astype(BF16)
 
     outs = ((toks, width), (rows, width))
-    return kernel(body, outs, conv_all, out_weight, residual, ct)
+    return kernel(body, outs, conv_all, out_weight, residual, slot_rows)
+
+
+def convolve(b_gate, c_gate, h_in, edge, same, taps, copies):
+    chans, toks = h_in.shape
+
+    def body(b_ref, c_ref, h_ref, edge_ref, same_ref, taps_ref, out_ref):
+        product = (c_ref[...].astype(F32) * h_ref[...].astype(F32)).astype(BF16).astype(F32)
+        lanes = iota((chans, toks), 1)
+        before = [edge_ref[:, k : k + 1].astype(F32) for k in range(2)]
+        tap = [to_col(taps_ref[k : k + 1, :], chans, 0) for k in range(3)]
+        one = jnp.where(lanes == 0, before[1], pltpu.roll(product, 1, 1))
+        two = pltpu.roll(product, 2, 1)
+        two = jnp.where(lanes == 0, before[0], jnp.where(lanes == 1, before[1], two))
+        total = tap[0] * product
+        total = total + tap[1] * one * same_ref[0:1, :]
+        total = total + tap[2] * two * same_ref[1:2, :]
+        conv = (b_ref[...].astype(F32) * total).astype(BF16)
+        for k in range(copies):
+            out_ref[k] = conv
+
+    outs = ((copies, chans, toks),)
+    return kernel(body, outs, b_gate, c_gate, h_in, edge, same, taps, limit=None)
 
 
 def order_map(cap, block, splitting):
@@ -132,22 +151,23 @@
     return kernel(body, ((2 * n_tx, half, width),), got)
 
 
-def pack(where, w_gate, w_up, n_ty):
+def pack(w_gate, w_up, n_ty, steps):
     dim, hid = w_gate.shape
     feats = dim // n_ty
 
-    def body(at_ref, wg_ref, wu_ref, *out_refs):
-        for d, out_ref in enumerate(out_refs):
-            to = lax.rem(at_ref[0] + (d + 1), n_ty)
+    def body(wg_ref, wu_ref, *out_refs):
+        ty = lax.axis_index("ty")
+        for d, out_ref in zip(steps, out_refs):
+            to = lax.rem(ty + d, n_ty)
             rows = pl.ds(pl.multiple_of(to * feats, feats), feats)
             out_ref[:, :hid] = wg_ref[rows, :]
             out_ref[:, hid:] = wu_ref[rows, :]
 
-    outs = tuple((feats, 2 * hid) for _ in range(n_ty - 1))
-    return kernel(body, outs, where, w_gate, w_up)
-
-
-def gate_up(where, x, gain, w_gate, w_up, pieces):
+    outs = tuple((feats, 2 * hid) for d in steps)
+    return kernel(body, outs, w_gate, w_up)
+
+
+def gate_up(x, gain, w_gate, w_up, pieces):
     n_ty = len(pieces) + 1
     groups, half, width = x.shape
     n_tx = groups // 2
@@ -155,10 +175,10 @@
     hid = w_gate.shape[1]
     rows = 2 * half
 
-    def body(at_ref, x_ref, gain_ref, wg_ref, wu_ref, *rest):
+    def body(x_ref, gain_ref, wg_ref, wu_ref, *rest):
         piece_refs, out_ref = rest[:-1], rest[-1]
-        ty = at_ref[0]
-        mine = pl.ds(pl.multiple_of(at_ref[0] * feats, feats), feats)
+        ty = lax.axis_index("ty")
+        mine = pl.ds(pl.multiple_of(ty * feats, feats), feats)
         gain_row = gain_ref[:, mine].astype(F32)
         extra = jnp.zeros((8, 2 * hid), F32)
         place = iota((8, 2 * hid), 0)
@@ -182,7 +202,7 @@
             out_ref[to, rows : rows + 8, :] = extra.astype(BF16)
 
     outs = ((n_ty, rows + 8, 2 * hid),)
-    return kernel(body, outs, where, x, gain, w_gate, w_up, *pieces, limit=24)
+    return kernel(body, outs, x, gain, w_gate, w_up, *pieces, limit=24)
 
 
 def activate(parts, full_dim):
@@ -209,15 +229,15 @@
     return kernel(body, ((n_ty, rows, hid),), parts)
 
 
-def down(where, hidden, w_down, pieces):
+def down(hidden, w_down, pieces):
     n_ty, rows, _ = hidden.shape
     n_tx = len(pieces) + 1
     half = rows // 2
     width = w_down.shape[-1]
 
-    def body(at_ref, h_ref, wd_ref, *rest):
+    def body(h_ref, wd_ref, *rest):
         piece_refs, out_ref = rest[:-1], rest[-1]
-        tx = at_ref[1]
+        tx = lax.axis_index("tx")
         h = jnp.concatenate([h_ref[k] for k in range(n_ty)], axis=1)
         for d in range(n_tx):
             w = [wd_ref[b, tx] if d == 0 else piece_refs[d - 1][b] for b in range(n_ty)]
@@ -227,7 +247,7 @@
             out_ref[n_tx + to] = part[half:]
 
     outs = ((2 * n_tx, half, width),)
-    return kernel(body, outs, where, hidden, w_down, *pieces, limit=24)
+    return kernel(body, outs, hidden, w_down, *pieces, limit=24)
 
 
 def join_rows(parts, cap):
@@ -291,29 +311,24 @@
     sp_index = lax.axis_index(("z", "core"))
     ty, tx = lax.axis_index("ty"), lax.axis_index("tx")
     tp_index = ty * n_tx + tx
-    where = jnp.stack([ty, tx]).astype(jnp.int32)
-
-    product = (c_gate.astype(F32) * h_in.astype(F32)).astype(BF16)
-    edge = lax.ppermute(
-        product[toks - 2 :], ("z", "core"), [(i, i + 1) for i in range(n_sp - 1)]
-    )
+
+    last = slice(toks - 2, toks)
+    product = (c_gate[last].astype(F32) * h_in[last].astype(F32)).astype(BF16)
+    edge = lax.ppermute(product, ("z", "core"), [(i, i + 1) for i in range(n_sp - 1)])
     first_pos = sp_index * toks
     padded_docs = jnp.concatenate([jnp.full((2,), -1, jnp.int32), docs], axis=0)
     near = lax.dynamic_slice_in_dim(padded_docs, first_pos, toks + 2)
+    same = jnp.stack([near[1 : toks + 1], near[:toks]]) == near[None, 2:]
     taps = lax.dynamic_slice_in_dim(conv_taps, tp_index * chans, chans, 1).astype(F32)
-    extended = jnp.concatenate([edge, product], axis=0).astype(F32)
-    conv_sum = taps[0][None, :] * extended[2:]
-    for back in (1, 2):
-        same = (near[2 - back : 2 - back + toks] == near[2:]).astype(F32)[:, None]
-        conv_sum = conv_sum + taps[back][None, :] * extended[2 - back : 2 - back + toks] * same
-    conv = (b_gate.astype(F32) * conv_sum).astype(BF16)
     n_tp = n_ty * n_tx
-    conv_copies = jnp.broadcast_to(conv.T[None], (n_tp, chans, toks))
+    conv_copies = convolve(b_gate.T, c_gate.T, h_in.T, edge.T, same.astype(F32), taps, n_tp)
     conv_all = lax.all_to_all(conv_copies, TP, 0, 0, tiled=True)
     conv_all = conv_all.reshape(n_tp * chans, toks)
 
-    packed = pack(where, w_gate[0], w_up[0], n_ty)
-    gate_up_pieces = [shifted(p, "ty", d + 1) for d, p in enumerate(packed)]
+    first = pack(w_gate[0], w_up[0], n_ty, (1, 2))
+    last = pack(w_gate[0], w_up[0], n_ty, (3,))
+    gate_up_pieces = [shifted(p, "ty", d + 1) for d, p in enumerate(first)]
+    gate_up_pieces.append(shifted(last, "ty", 3))
     w_down4 = w_down[0].reshape(n_ty, n_tx, hid, width)
     down_pieces = []
     for d in range(1, n_tx):
@@ -321,21 +336,21 @@
         piece = lax.dynamic_index_in_dim(w_down4, to, 1, keepdims=False)
         down_pieces.append(shifted(piece, "tx", d))
 
-    ct = routing_out(expert_pick, rows, cap)
-    stream, outgoing = project(conv_all, out_weight, residual_in, ct)
+    slot_rows = routing_out(expert_pick, cap)
+    stream, outgoing = project(conv_all, out_weight, residual_in, slot_rows, rows)
     got = lax.all_to_all(
         outgoing.reshape(n_z, 2 * cap, width), "z", 0, 0, tiled=True
     ).reshape(rows, width)
-    got, gate_up_pieces = lax.optimization_barrier((got, gate_up_pieces))
     split = split_rows(got, n_tx, cap)
     x = lax.all_to_all(split, ("core", "tx"), 0, 0, tiled=True)
     parts = gate_up(
-        where, x, norm_gain.reshape(1, -1), w_gate[0], w_up[0], gate_up_pieces
+        x, norm_gain.reshape(1, -1), w_gate[0], w_up[0], gate_up_pieces
     )
     parts = lax.all_to_all(parts, "ty", 0, 0, tiled=True)
-    hidden = lax.all_to_all(activate(parts, full_dim), "ty", 0, 0, tiled=True)
+    hidden = activate(parts, full_dim)
+    hidden = lax.all_to_all(hidden, "ty", 0, 0, tiled=True)
     outs = lax.all_to_all(
-        down(where, hidden, w_down4, down_pieces), ("core", "tx"), 0, 0, tiled=True
+        down(hidden, w_down4, down_pieces), ("core", "tx"), 0, 0, tiled=True
     )
     outs, late_pick, late_weight = lax.optimization_barrier((outs, expert_pick, route_weight))
     c0, c1 = routing_back(late_pick, rows, cap)

time: 209 us -> 205 us (0.981)
  blocking collectives: 44.3 us -> 79 us
  waiting for transfers between devices: 74.6 us -> 55.7 us
  starting transfers between devices: 65.1 us -> 47 us
    all_to_all x1 -> x2, blocking collectives: 21.8 us -> 56.7 us  [the longest x1 34.5 us: local(): lax.all_to_all(outgoing.reshape(n_z, 2 * cap, width), 'z', 0, 0, tiled=True)]
    all_to_all x1, waiting for transfers between devices: 17.3 us -> 0.01 us  [local(): x = lax.all_to_all(split, ('core', 'tx'), 0, 0, tiled=True)]
    all_to_all x2 -> x1, starting transfers between devices: 19.9 us -> 4.91 us  [local(): hidden = lax.all_to_all(hidden, 'ty', 0, 0, tiled=True)]
    all_to_all x1, starting transfers between devices: 11.7 us -> 5.88 us  [local(): lax.all_to_all(join_rows(outs, cap).reshape(n_z, 2 * cap, width), 'z', 0,...]
    ppermute x6, starting transfers between devices: 19.4 us -> 22 us  [shifted(): lax.ppermute(value, axis, [(i, (i + steps) % count) for i in range(count)])]
    pallas_call x10 -> x12, Pallas kernels: 12 us -> 11.2 us  [kernel(): pl.pallas_call(body, out_shape=tuple((jax.ShapeDtypeStruct(o, dtype) for...]
    unnamed x35 -> x33, local copies, waits for them, and re-layouts: 6.5 us -> 6.32 us
  transfers between devices with their start and end apart: 12 -> 11, of which waited for: 8 -> 7; matrix products, arithmetic and copies ran while one was open for 1% -> 2% of each run, Pallas kernels for 1% -> 1%
where the time goes in v1:
time: 205 us; the launch traced here: 203 us
  blocking collectives  79 us (39%)
  waiting for transfers between devices  55.7 us (27%)
  starting transfers between devices  47 us (23%)
  Pallas kernels  11.2 us (5%)
  local copies, waits for them, and re-layouts  7.5 us (4%)
  other arithmetic  2.83 us (1%)
    all_to_all x1, blocking collectives, local(): lax.all_to_all(outgoing.reshape(n_z, 2 * cap, width), 'z', 0, 0, tiled=True)  34.5 us
    ppermute x6, waiting for transfers between devices, shifted(): lax.ppermute(value, axis, [(i, (i + steps) % count) for i in range(count)])  25.8 us
    all_to_all x1, blocking collectives, local(): parts = lax.all_to_all(parts, 'ty', 0, 0, tiled=True)  22.3 us
    all_to_all x1, blocking collectives, local(): lax.all_to_all(down(hidden, w_down4, down_pieces), ('core', 'tx'), 0, 0,...  22.2 us
    ppermute x6, starting transfers between devices, shifted(): lax.ppermute(value, axis, [(i, (i + steps) % count) for i in range(count)])  22 us
    all_to_all x1, waiting for transfers between devices, local(): lax.all_to_all(join_rows(outs, cap).reshape(n_z, 2 * cap, width), 'z', 0,...  20.6 us
    pallas_call x12, Pallas kernels, kernel(): pl.pallas_call(body, out_shape=tuple((jax.ShapeDtypeStruct(o, dtype) for...  11.2 us
    all_to_all x1, waiting for transfers between devices, local(): conv_all = lax.all_to_all(conv_copies, TP, 0, 0, tiled=True)  9.34 us
  transfers between devices with their start and end apart: 11, of which 7 were waited for; matrix products, arithmetic and copies ran while one was open for 2% of the time, Pallas kernels for 1%

profile of v1, /device:TPU:8, one launch (start us, length us, event | category | flops | bytes accessed | tf_op | source)
XLA Modules:
  0.0 203.5 jit_solution(17481196687163307031)
XLA Ops:
  0.0 0.0 copy-start.12
  0.0 0.9 multiply_convert_fusion
  0.9 1.7 collective-permute-start
  2.7 0.8 pad_dynamic-slice_fusion
  3.4 0.1 fusion
  3.5 0.6 compare_convert_fusion.same_ref
  4.1 1.3 dynamic-slice_convert_fusion.taps_ref
  5.5 0.0 collective-permute-done
  5.5 0.6 copy-done.11
  6.1 1.8 shard_map.127
  7.8 8.7 %all-to-all-start = ((bf16[16,64,256]{2,1,0:T(8,128)(2,1)}), bf16[16,64,256]{2,1,0:T(8,128)(2,1)S(1)}, u32[]{:S(2)}, u32[]{:S(2)}) async-start(bf16[16,64,256]{2,1,0:T(8,128)(2,1)} %shard_map.127), calls=%async_computation | async-start | bytes 1048576 | tf_op jit(solution)/shard_map/all_to_all | solution.py:325
  16.6 0.0 copy-done.12
  16.6 0.1 copy.19.pick_ref
  16.7 0.5 shard_map.128.slot_ref
  17.2 9.3 %all-to-all-done = bf16[16,64,256]{2,1,0:T(8,128)(2,1)S(1)} async-done(((bf16[16,64,256]{2,1,0:T(8,128)(2,1)}), bf16[16,64,256]{2,1,0:T(8,128)(2,1)S(1)}, u32[]{:S(2)}, u32[]{:S(2)}) %all-to-all-start) | async-done | bytes 524320 | tf_op jit(solution)/shard_map/all_to_all | solution.py:325
  26.6 0.0 copy-done.9
  26.6 0.0 copy-done.10
  26.6 0.7 shard_map.129
  27.3 34.5 %all_to_all.35 = bf16[16,40,256]{2,1,0:T(8,128)(2,1)S(1)} all-to-all(bf16[16,40,256]{2,1,0:T(8,128)(2,1)S(1)} %bitcast.31), channel_id=1, replica_groups=mesh['z'=16,'core'=2,'ty'=4,'tx'=4] {'z'}, dimensions={0} | all-to-all | bytes 655360 | tf_op jit(solution)/shard_map/all_to_all | solution.py:341
  61.8 1.3 shard_map.130
  63.1 3.7 %all-to-all-start.2 = ((bf16[8,320,256]{2,1,0:T(8,128)(2,1)}), bf16[8,320,256]{2,1,0:T(8,128)(2,1)S(1)}, u32[]{:S(2)}, u32[]{:S(2)}) async-start(bf16[8,320,256]{2,1,0:T(8,128)(2,1)} %shard_map.130), calls=%async_computation.2 | async-start | bytes 2621440 | tf_op jit(solution)/shard_map/all_to_all | solution.py:345
  66.8 0.0 copy-done
  66.8 0.0 copy-done.1
  66.8 0.2 shard_map.131
  67.0 3.2 %collective-permute-start.1 = (bf16[1024,256]{1,0:T(8,128)(2,1)S(1)}, bf16[1024,256]{1,0:T(8,128)(2,1)S(1)}, u32[]{:S(2)}, u32[]{:S(2)}) collective-permute-start(bf16[1024,256]{1,0:T(8,128)(2,1)S(1)} %get-tuple-element.15), channel_id=1, source_target_pairs={{0,4},{4,8},{8,12},{12,0},{1,5},{5,9},{9,13},{13,1},{2,6},{6,10},{... | collective-permute-start | bytes 1572872 | tf_op jit(solution)/shard_map/ppermute | solution.py:285
  70.2 0.0 copy-start.14
  70.2 5.2 %collective-permute-start.2 = (bf16[1024,256]{1,0:T(8,128)(2,1)S(1)}, bf16[1024,256]{1,0:T(8,128)(2,1)S(1)}, u32[]{:S(2)}, u32[]{:S(2)}) collective-permute-start(bf16[1024,256]{1,0:T(8,128)(2,1)S(1)} %get-tuple-element.16), channel_id=1, source_target_pairs={{0,8},{4,12},{8,0},{12,4},{1,9},{5,13},{9,1},{13,5},{2,10},{6,14},... | collective-permute-start | bytes 1572872 | tf_op jit(solution)/shard_map/ppermute | solution.py:285
  75.4 0.1 shard_map.132
  75.5 2.2 %collective-permute-start.3 = (bf16[1024,256]{1,0:T(8,128)(2,1)S(1)}, bf16[1024,256]{1,0:T(8,128)(2,1)S(1)}, u32[]{:S(2)}, u32[]{:S(2)}) collective-permute-start(bf16[1024,256]{1,0:T(8,128)(2,1)S(1)} %shard_map.132), channel_id=1, source_target_pairs={{0,12},{4,0},{8,4},{12,8},{1,13},{5,1},{9,5},{13,9},{2,14},{6,2},{... | collective-permute-start | bytes 1572872 | tf_op jit(solution)/shard_map/ppermute | solution.py:285
  77.7 0.0 copy-done.14
  77.7 6.5 %collective-permute-done.1.rest_0_ = bf16[1024,256]{1,0:T(8,128)(2,1)S(1)} collective-permute-done((bf16[1024,256]{1,0:T(8,128)(2,1)S(1)}, bf16[1024,256]{1,0:T(8,128)(2,1)S(1)}, u32[]{:S(2)}, u32[]{:S(2)}) %collective-permute-start.1) | collective-permute-done | bytes 524320 | tf_op jit(solution)/shard_map/ppermute | solution.py:285
  84.2 0.8 copy-done.3
  85.0 3.5 %collective-permute-done.2.rest_1_ = bf16[1024,256]{1,0:T(8,128)(2,1)S(1)} collective-permute-done((bf16[1024,256]{1,0:T(8,128)(2,1)S(1)}, bf16[1024,256]{1,0:T(8,128)(2,1)S(1)}, u32[]{:S(2)}, u32[]{:S(2)}) %collective-permute-start.2) | collective-permute-done | bytes 524320 | tf_op jit(solution)/shard_map/ppermute | solution.py:285
  88.5 0.8 copy-done.5
  89.3 9.6 %collective-permute-done.3.rest_2_ = bf16[1024,256]{1,0:T(8,128)(2,1)S(1)} collective-permute-done((bf16[1024,256]{1,0:T(8,128)(2,1)S(1)}, bf16[1024,256]{1,0:T(8,128)(2,1)S(1)}, u32[]{:S(2)}, u32[]{:S(2)}) %collective-permute-start.3) | collective-permute-done | bytes 524320 | tf_op jit(solution)/shard_map/ppermute | solution.py:285
  98.9 0.8 copy-done.7
  99.6 0.0 all-to-all-done.2.x_ref
  99.7 1.0 copy-done.4
  100.7 1.0 copy-done.6
  101.7 1.0 copy-done.8
  102.8 1.9 shard_map.133
  104.6 22.3 %all_to_all.36.p_ref = bf16[4,648,256]{2,1,0:T(8,128)(2,1)S(1)} all-to-all(bf16[4,648,256]{2,1,0:T(8,128)(2,1)S(1)} %shard_map.133), channel_id=1, replica_groups=mesh['z'=16,'core'=2,'ty'=4,'tx'=4] {'ty'}, dimensions={0} | all-to-all | bytes 2654208 | tf_op jit(solution)/shard_map/all_to_all | solution.py:349
  126.9 1.2 shard_map.134
  128.1 4.9 %all-to-all-start.4 = ((bf16[4,640,128]{2,1,0:T(8,128)(2,1)}), bf16[4,640,128]{2,1,0:T(8,128)(2,1)S(1)}, u32[]{:S(2)}, u32[]{:S(2)}) async-start(bf16[4,640,128]{2,1,0:T(8,128)(2,1)} %shard_map.134), calls=%async_computation.4 | async-start | bytes 1310720 | tf_op jit(solution)/shard_map/all_to_all | solution.py:351
  133.0 0.0 copy-done.2
  133.0 0.1 dynamic-slice_bitcast_fusion
  133.1 3.5 %collective-permute-start.4 = (bf16[4,128,256]{2,1,0:T(8,128)(2,1)S(1)}, bf16[4,128,256]{2,1,0:T(8,128)(2,1)S(1)}, u32[]{:S(2)}, u32[]{:S(2)}) collective-permute-start(bf16[4,128,256]{2,1,0:T(8,128)(2,1)S(1)} %get-tuple-element.25), channel_id=1, source_target_pairs={{0,1},{1,2},{2,3},{3,0},{4,5},{5,6},{6,7},{7,4},{8,9},{9,10},{10,1... | collective-permute-start | bytes 786440 | tf_op jit(solution)/shard_map/ppermute | solution.py:285
  136.7 4.6 %collective-permute-start.5 = (bf16[4,128,256]{2,1,0:T(8,128)(2,1)S(1)}, bf16[4,128,256]{2,1,0:T(8,128)(2,1)S(1)}, u32[]{:S(2)}, u32[]{:S(2)}) collective-permute-start(bf16[4,128,256]{2,1,0:T(8,128)(2,1)S(1)} %get-tuple-element.24), channel_id=1, source_target_pairs={{0,2},{1,3},{2,0},{3,1},{4,6},{5,7},{6,4},{7,5},{8,10},{9,11},{10,... | collective-permute-start | bytes 786440 | tf_op jit(solution)/shard_map/ppermute | solution.py:285
  141.3 3.4 %collective-permute-start.6 = (bf16[4,128,256]{2,1,0:T(8,128)(2,1)S(1)}, bf16[4,128,256]{2,1,0:T(8,128)(2,1)S(1)}, u32[]{:S(2)}, u32[]{:S(2)}) collective-permute-start(bf16[4,128,256]{2,1,0:T(8,128)(2,1)S(1)} %get-tuple-element.23), channel_id=1, source_target_pairs={{0,3},{1,0},{2,1},{3,2},{4,7},{5,4},{6,5},{7,6},{8,11},{9,8},{10,9... | collective-permute-start | bytes 786440 | tf_op jit(solution)/shard_map/ppermute | solution.py:285
  144.6 0.0 collective-permute-done.4.rest_0_
  144.6 4.8 %collective-permute-done.5.rest_1_ = bf16[4,128,256]{2,1,0:T(8,128)(2,1)S(1)} collective-permute-done((bf16[4,128,256]{2,1,0:T(8,128)(2,1)S(1)}, bf16[4,128,256]{2,1,0:T(8,128)(2,1)S(1)}, u32[]{:S(2)}, u32[]{:S(2)}) %collective-permute-start.5) | collective-permute-done | bytes 262176 | tf_op jit(solution)/shard_map/ppermute | solution.py:285
  149.4 1.5 collective-permute-done.6.rest_2_
  151.0 0.0 all-to-all-done.4.h_ref
  151.0 0.8 shard_map.135
  151.8 22.2 %all_to_all.37.p_ref = bf16[8,320,256]{2,1,0:T(8,128)(2,1)S(1)} all-to-all(bf16[8,320,256]{2,1,0:T(8,128)(2,1)S(1)} %shard_map.135), channel_id=1, replica_groups=mesh['z'=16,'core'=2,'ty'=4,'tx'=4] {'core','tx'}, dimensions={0} | all-to-all | bytes 2621440 | tf_op jit(solution)/shard_map/all_to_all | solution.py:352
  174.1 1.1 shard_map.136
  175.2 5.9 %all-to-all-start.6 = ((bf16[16,40,256]{2,1,0:T(8,128)(2,1)}), bf16[16,40,256]{2,1,0:T(8,128)(2,1)S(1)}, u32[]{:S(2)}, u32[]{:S(2)}) async-start(bf16[16,40,256]{2,1,0:T(8,128)(2,1)} %bitcast.15), calls=%async_computation.6 | async-start | bytes 655360 | tf_op jit(solution)/shard_map/all_to_all | solution.py:357
  181.1 0.0 copy-done.13
  181.1 0.1 copy.20.pick_ref
  181.2 0.5 shard_map.137
  181.7 0.0 copy-done.15
  181.8 0.1 copy.21.w_ref
  181.9 20.6 %all-to-all-done.6 = bf16[16,40,256]{2,1,0:T(8,128)(2,1)S(1)} async-done(((bf16[16,40,256]{2,1,0:T(8,128)(2,1)}), bf16[16,40,256]{2,1,0:T(8,128)(2,1)S(1)}, u32[]{:S(2)}, u32[]{:S(2)}) %all-to-all-start.6) | async-done | bytes 327712 | tf_op jit(solution)/shard_map/all_to_all | solution.py:357
  202.4 1.0 shard_map.138
  (15 shorter events, 0.0 us)
Async XLA Ops:
  0.0 16.6 %copy-start.12 = (s32[256,2]{0,1:T(2,128)S(1)}, s32[256,2]{0,1:T(2,128)}, u32[]{:S(2)}) copy-start(s32[256,2]{0,1:T(2,128)} %param.21) | copy-start | bytes 6148
  0.0 26.6 %copy-start.9 = (bf16[1024,256]{1,0:T(8,128)(2,1)S(1)}, bf16[1024,256]{1,0:T(8,128)(2,1)}, u32[]{:S(2)}) copy-start(bf16[1024,256]{1,0:T(8,128)(2,1)} %w_ref.1) | copy-start | bytes 1572868
  0.0 26.6 %copy-start.10 = (bf16[256,256]{1,0:T(8,128)(2,1)S(1)}, bf16[256,256]{1,0:T(8,128)(2,1)}, u32[]{:S(2)}) copy-start(bf16[256,256]{1,0:T(8,128)(2,1)} %res_ref.1) | copy-start | bytes 393220
  0.9 4.6 %collective-permute-start = (bf16[2,64]{0,1:T(8,128)(2,1)S(1)}, bf16[2,64]{0,1:T(8,128)(2,1)S(1)}, u32[]{:S(2)}, u32[]{:S(2)}) collective-permute-start(bf16[2,64]{0,1:T(8,128)(2,1)S(1)} %multiply_convert_fusion), channel_id=1, source_target_pairs={{0,16},{16,32},{32,48},{48,64},{64,80},{80,96},{96,112},{112,128},... | collective-permute-start | bytes 776 | tf_op jit(solution)/shard_map/ppermute | solution.py:317
  5.5 0.6 copy-start.11
  7.8 18.7 %all-to-all-start = ((bf16[16,64,256]{2,1,0:T(8,128)(2,1)}), bf16[16,64,256]{2,1,0:T(8,128)(2,1)S(1)}, u32[]{:S(2)}, u32[]{:S(2)}) async-start(bf16[16,64,256]{2,1,0:T(8,128)(2,1)} %shard_map.127), calls=%async_computation | async-start | bytes 1048576 | tf_op jit(solution)/shard_map/all_to_all | solution.py:325
  63.1 3.7 %copy-start = (bf16[1,4096,128]{2,1,0:T(8,128)(2,1)S(1)}, bf16[1,4096,128]{2,1,0:T(8,128)(2,1)}, u32[]{:S(2)}) copy-start(bf16[1,4096,128]{2,1,0:T(8,128)(2,1)} %param.23) | copy-start | bytes 3145732
  63.1 3.7 %copy-start.1 = (bf16[1,4096,128]{2,1,0:T(8,128)(2,1)S(1)}, bf16[1,4096,128]{2,1,0:T(8,128)(2,1)}, u32[]{:S(2)}) copy-start(bf16[1,4096,128]{2,1,0:T(8,128)(2,1)} %param.24) | copy-start | bytes 3145732
  63.1 36.6 %all-to-all-start.2 = ((bf16[8,320,256]{2,1,0:T(8,128)(2,1)}), bf16[8,320,256]{2,1,0:T(8,128)(2,1)S(1)}, u32[]{:S(2)}, u32[]{:S(2)}) async-start(bf16[8,320,256]{2,1,0:T(8,128)(2,1)} %shard_map.130), calls=%async_computation.2 | async-start | bytes 2621440 | tf_op jit(solution)/shard_map/all_to_all | solution.py:345
  67.0 17.2 %collective-permute-start.1 = (bf16[1024,256]{1,0:T(8,128)(2,1)S(1)}, bf16[1024,256]{1,0:T(8,128)(2,1)S(1)}, u32[]{:S(2)}, u32[]{:S(2)}) collective-permute-start(bf16[1024,256]{1,0:T(8,128)(2,1)S(1)} %get-tuple-element.15), channel_id=1, source_target_pairs={{0,4},{4,8},{8,12},{12,0},{1,5},{5,9},{9,13},{13,1},{2,6},{6,10},{... | collective-permute-start | bytes 1572872 | tf_op jit(solution)/shard_map/ppermute | solution.py:285
  70.2 7.5 %copy-start.14 = (bf16[4096]{0:T(1024)(128)(2,1)S(1)}, bf16[4096]{0:T(1024)(128)(2,1)}, u32[]{:S(2)}) copy-start(bf16[4096]{0:T(1024)(128)(2,1)} %param.20) | copy-start | bytes 24580
  70.2 18.2 %collective-permute-start.2 = (bf16[1024,256]{1,0:T(8,128)(2,1)S(1)}, bf16[1024,256]{1,0:T(8,128)(2,1)S(1)}, u32[]{:S(2)}, u32[]{:S(2)}) collective-permute-start(bf16[1024,256]{1,0:T(8,128)(2,1)S(1)} %get-tuple-element.16), channel_id=1, source_target_pairs={{0,8},{4,12},{8,0},{12,4},{1,9},{5,13},{9,1},{13,5},{2,10},{6,14},... | collective-permute-start | bytes 1572872 | tf_op jit(solution)/shard_map/ppermute | solution.py:285
  75.5 23.3 %collective-permute-start.3 = (bf16[1024,256]{1,0:T(8,128)(2,1)S(1)}, bf16[1024,256]{1,0:T(8,128)(2,1)S(1)}, u32[]{:S(2)}, u32[]{:S(2)}) collective-permute-start(bf16[1024,256]{1,0:T(8,128)(2,1)S(1)} %shard_map.132), channel_id=1, source_target_pairs={{0,12},{4,0},{8,4},{12,8},{1,13},{5,1},{9,5},{13,9},{2,14},{6,2},{... | collective-permute-start | bytes 1572872 | tf_op jit(solution)/shard_map/ppermute | solution.py:285
  84.2 0.8 copy-start.3
  88.5 0.8 copy-start.5
  98.8 0.8 copy-start.7
  99.6 1.0 copy-start.4
  100.7 1.0 copy-start.6
  101.7 1.0 copy-start.8
  126.9 6.1 %copy-start.2 = (bf16[1,2048,256]{2,1,0:T(8,128)(2,1)S(1)}, bf16[1,2048,256]{2,1,0:T(8,128)(2,1)}, u32[]{:S(2)}) copy-start(bf16[1,2048,256]{2,1,0:T(8,128)(2,1)} %param.25) | copy-start | bytes 3145732
  128.1 22.8 %all-to-all-start.4 = ((bf16[4,640,128]{2,1,0:T(8,128)(2,1)}), bf16[4,640,128]{2,1,0:T(8,128)(2,1)S(1)}, u32[]{:S(2)}, u32[]{:S(2)}) async-start(bf16[4,640,128]{2,1,0:T(8,128)(2,1)} %shard_map.134), calls=%async_computation.4 | async-start | bytes 1310720 | tf_op jit(solution)/shard_map/all_to_all | solution.py:351
  133.1 11.5 %collective-permute-start.4 = (bf16[4,128,256]{2,1,0:T(8,128)(2,1)S(1)}, bf16[4,128,256]{2,1,0:T(8,128)(2,1)S(1)}, u32[]{:S(2)}, u32[]{:S(2)}) collective-permute-start(bf16[4,128,256]{2,1,0:T(8,128)(2,1)S(1)} %get-tuple-element.25), channel_id=1, source_target_pairs={{0,1},{1,2},{2,3},{3,0},{4,5},{5,6},{6,7},{7,4},{8,9},{9,10},{10,1... | collective-permute-start | bytes 786440 | tf_op jit(solution)/shard_map/ppermute | solution.py:285
  136.7 12.8 %collective-permute-start.5 = (bf16[4,128,256]{2,1,0:T(8,128)(2,1)S(1)}, bf16[4,128,256]{2,1,0:T(8,128)(2,1)S(1)}, u32[]{:S(2)}, u32[]{:S(2)}) collective-permute-start(bf16[4,128,256]{2,1,0:T(8,128)(2,1)S(1)} %get-tuple-element.24), channel_id=1, source_target_pairs={{0,2},{1,3},{2,0},{3,1},{4,6},{5,7},{6,4},{7,5},{8,10},{9,11},{10,... | collective-permute-start | bytes 786440 | tf_op jit(solution)/shard_map/ppermute | solution.py:285
  141.3 9.7 %collective-permute-start.6 = (bf16[4,128,256]{2,1,0:T(8,128)(2,1)S(1)}, bf16[4,128,256]{2,1,0:T(8,128)(2,1)S(1)}, u32[]{:S(2)}, u32[]{:S(2)}) collective-permute-start(bf16[4,128,256]{2,1,0:T(8,128)(2,1)S(1)} %get-tuple-element.23), channel_id=1, source_target_pairs={{0,3},{1,0},{2,1},{3,2},{4,7},{5,4},{6,5},{7,6},{8,11},{9,8},{10,9... | collective-permute-start | bytes 786440 | tf_op jit(solution)/shard_map/ppermute | solution.py:285
  174.1 7.0 %copy-start.13 = (s32[256,2]{0,1:T(2,128)S(1)}, s32[256,2]{0,1:T(2,128)}, u32[]{:S(2)}) copy-start(s32[256,2]{0,1:T(2,128)} %param.21) | copy-start | bytes 6148
  174.1 7.7 %copy-start.15 = (f32[256,2]{0,1:T(2,128)S(1)}, f32[256,2]{0,1:T(2,128)}, u32[]{:S(2)}) copy-start(f32[256,2]{0,1:T(2,128)} %param.22) | copy-start | bytes 6148
  175.2 27.3 %all-to-all-start.6 = ((bf16[16,40,256]{2,1,0:T(8,128)(2,1)}), bf16[16,40,256]{2,1,0:T(8,128)(2,1)S(1)}, u32[]{:S(2)}, u32[]{:S(2)}) async-start(bf16[16,40,256]{2,1,0:T(8,128)(2,1)} %bitcast.15), calls=%async_computation.6 | async-start | bytes 655360 | tf_op jit(solution)/shard_map/all_to_all | solution.py:357

commit v2 on v1

--- a/solution.py
+++ b/solution.py
@@ -95,26 +95,40 @@
     return kernel(body, outs, conv_all, out_weight, residual, slot_rows)
 
 
-def convolve(b_gate, c_gate, h_in, edge, same, taps, copies):
+def convolve(b_gate, c_gate, h_in, edge, docs, taps, copies):
     chans, toks = h_in.shape
-
-    def body(b_ref, c_ref, h_ref, edge_ref, same_ref, taps_ref, out_ref):
+    lane = docs.shape[1]
+    per = toks // lane
+
+    def body(b_ref, c_ref, h_ref, edge_ref, docs_ref, taps_ref, out_ref):
+        sp = lax.axis_index("z") * 2 + lax.axis_index("core")
+        tp = lax.axis_index("ty") * lax.axis_size("tx") + lax.axis_index("tx")
+        own = jnp.concatenate([docs_ref[pl.ds(sp * per + k, 1), :] for k in range(per)], axis=1)
+        prior = docs_ref[pl.ds(jnp.maximum(sp * per - 1, 0), 1), :]
+        prior = jnp.where(sp > 0, prior, -1)
+        at = iota((1, toks), 1)
+        back1 = jnp.where(at == 0, prior[:, lane - 1 :], pltpu.roll(own, 1, 1))
+        back2 = jnp.where(at == 1, prior[:, lane - 1 :], pltpu.roll(own, 2, 1))
+        back2 = jnp.where(at == 0, prior[:, lane - 2 : lane - 1], back2)
+        all_taps = taps_ref[...].astype(F32)
+        first = lax.rem(all_taps.shape[1] - tp * chans, all_taps.shape[1])
+        near = pltpu.roll(jnp.concatenate([all_taps, jnp.zeros((5, all_taps.shape[1]), F32)]), first, 1)
+        tap = [to_col(near[k : k + 1, :chans], chans, 0) for k in range(3)]
         product = (c_ref[...].astype(F32) * h_ref[...].astype(F32)).astype(BF16).astype(F32)
         lanes = iota((chans, toks), 1)
         before = [edge_ref[:, k : k + 1].astype(F32) for k in range(2)]
-        tap = [to_col(taps_ref[k : k + 1, :], chans, 0) for k in range(3)]
         one = jnp.where(lanes == 0, before[1], pltpu.roll(product, 1, 1))
         two = pltpu.roll(product, 2, 1)
         two = jnp.where(lanes == 0, before[0], jnp.where(lanes == 1, before[1], two))
         total = tap[0] * product
-        total = total + tap[1] * one * same_ref[0:1, :]
-        total = total + tap[2] * two * same_ref[1:2, :]
+        total = total + tap[1] * one * (back1 == own).astype(F32)
+        total = total + tap[2] * two * (back2 == own).astype(F32)
         conv = (b_ref[...].astype(F32) * total).astype(BF16)
         for k in range(copies):
             out_ref[k] = conv
 
     outs = ((copies, chans, toks),)
-    return kernel(body, outs, b_gate, c_gate, h_in, edge, same, taps, limit=None)
+    return kernel(body, outs, b_gate, c_gate, h_in, edge, docs, taps, limit=None)
 
 
 def order_map(cap, block, splitting):
@@ -176,12 +190,18 @@
     rows = 2 * half
 
     def body(x_ref, gain_ref, wg_ref, wu_ref, *rest):
-        piece_refs, out_ref = rest[:-1], rest[-1]
+        piece_refs, out_ref, held, sems = rest[: n_ty - 1], rest[-3], rest[-2], rest[-1]
+        moves = [
+            pltpu.make_async_copy(ref, held.at[d], sems.at[d]) for d, ref in enumerate(piece_refs)
+        ]
+        for move in moves:
+            move.start()
         ty = lax.axis_index("ty")
         mine = pl.ds(pl.multiple_of(ty * feats, feats), feats)
         gain_row = gain_ref[:, mine].astype(F32)
         extra = jnp.zeros((8, 2 * hid), F32)
         place = iota((8, 2 * hid), 0)
+        scaled = []
         for core in range(2):
             raw = jnp.concatenate([x_ref[core * n_tx + t] for t in range(n_tx)], axis=1).astype(F32)
             squares = jnp.sum(raw * raw, axis=1, keepdims=True)
@@ -195,14 +215,30 @@
             keep = slice(core * half, (core + 1) * half)
             out_ref[ty, keep, 0:hid] = dot(y, wg_ref[mine, :]).astype(BF16)
             out_ref[ty, keep, hid : 2 * hid] = dot(y, wu_ref[mine, :]).astype(BF16)
-            for d in range(1, n_ty):
-                to = lax.rem(ty + (n_ty - d), n_ty)
-                out_ref[to, keep, :] = dot(y, piece_refs[d - 1][...]).astype(BF16)
+            scaled.append(y)
+        for d in range(1, n_ty):
+            to = lax.rem(ty + (n_ty - d), n_ty)
+            moves[d - 1].wait()
+            for core in range(2):
+                keep = slice(core * half, (core + 1) * half)
+                out_ref[to, keep, :] = dot(scaled[core], held[d - 1]).astype(BF16)
         for to in range(n_ty):
             out_ref[to, rows : rows + 8, :] = extra.astype(BF16)
 
-    outs = ((n_ty, rows + 8, 2 * hid),)
-    return kernel(body, outs, x, gain, w_gate, w_up, *pieces, limit=24)
+    vmem = pl.BlockSpec(memory_space=pltpu.VMEM)
+    anywhere = pl.BlockSpec(memory_space=pltpu.HBM)
+    return pl.pallas_call(
+        body,
+        out_shape=jax.ShapeDtypeStruct((n_ty, rows + 8, 2 * hid), BF16),
+        in_specs=[vmem] * 4 + [anywhere] * (n_ty - 1),
+        out_specs=vmem,
+        scratch_shapes=[
+            pltpu.VMEM((n_ty - 1, feats, 2 * hid), BF16),
+            pltpu.SemaphoreType.DMA((n_ty - 1,)),
+        ],
+        compiler_params=pltpu.CompilerParams(vmem_limit_bytes=24 << 20),
+        name="gate_up",
+    )(x, gain, w_gate, w_up, *[pltpu.with_memory_space_constraint(p, pltpu.HBM) for p in pieces])
 
 
 def activate(parts, full_dim):
@@ -308,20 +344,15 @@
     n_sp = 2 * n_z
     cap = 5 * toks // (2 * n_sp)
     rows = n_sp * cap
-    sp_index = lax.axis_index(("z", "core"))
-    ty, tx = lax.axis_index("ty"), lax.axis_index("tx")
-    tp_index = ty * n_tx + tx
+    tx = lax.axis_index("tx")
 
     last = slice(toks - 2, toks)
     product = (c_gate[last].astype(F32) * h_in[last].astype(F32)).astype(BF16)
     edge = lax.ppermute(product, ("z", "core"), [(i, i + 1) for i in range(n_sp - 1)])
-    first_pos = sp_index * toks
-    padded_docs = jnp.concatenate([jnp.full((2,), -1, jnp.int32), docs], axis=0)
-    near = lax.dynamic_slice_in_dim(padded_docs, first_pos, toks + 2)
-    same = jnp.stack([near[1 : toks + 1], near[:toks]]) == near[None, 2:]
-    taps = lax.dynamic_slice_in_dim(conv_taps, tp_index * chans, chans, 1).astype(F32)
     n_tp = n_ty * n_tx
-    conv_copies = convolve(b_gate.T, c_gate.T, h_in.T, edge.T, same.astype(F32), taps, n_tp)
+    conv_copies = convolve(
+        b_gate.T, c_gate.T, h_in.T, edge.T, docs.reshape(-1, 128), conv_taps, n_tp
+    )
     conv_all = lax.all_to_all(conv_copies, TP, 0, 0, tiled=True)
     conv_all = conv_all.reshape(n_tp * chans, toks)
 
@@ -343,9 +374,7 @@
     ).reshape(rows, width)
     split = split_rows(got, n_tx, cap)
     x = lax.all_to_all(split, ("core", "tx"), 0, 0, tiled=True)
-    parts = gate_up(
-        x, norm_gain.reshape(1, -1), w_gate[0], w_up[0], gate_up_pieces
-    )
+    parts = gate_up(x, norm_gain.reshape(1, -1), w_gate[0], w_up[0], gate_up_pieces)
     parts = lax.all_to_all(parts, "ty", 0, 0, tiled=True)
     hidden = activate(parts, full_dim)
     hidden = lax.all_to_all(hidden, "ty", 0, 0, tiled=True)

time: 205 us -> 200 us (0.976)
  local copies, waits for them, and re-layouts: 7.5 us -> 1.9 us
    unnamed x33 -> x25, local copies, waits for them, and re-layouts: 6.32 us -> 1.57 us
    pallas_call x0 -> x1, Pallas kernels: none -> 3.18 us  [gate_up(): pl.pallas_call(body, out_shape=jax.ShapeDtypeStruct((n_ty, rows + 8, 2 *...]
    pallas_call x12 -> x11, Pallas kernels: 11.2 us -> 9.5 us  [kernel(): pl.pallas_call(body, out_shape=tuple((jax.ShapeDtypeStruct(o, dtype) for...]
  transfers between devices with their start and end apart: 11 -> 11, of which waited for: 7 -> 8; matrix products, arithmetic and copies ran while one was open for 2% -> 0% of each run, Pallas kernels for 1% -> 1%
where the time goes in v2:
time: 200 us
  blocking collectives  79 us (40%)
  waiting for transfers between devices  57.5 us (29%)
  starting transfers between devices  47.4 us (24%)
  Pallas kernels  12.7 us (6%)
    all_to_all x1, blocking collectives, local(): lax.all_to_all(outgoing.reshape(n_z, 2 * cap, width), 'z', 0, 0, tiled=True)  34.5 us
    ppermute x6, waiting for transfers between devices, shifted(): lax.ppermute(value, axis, [(i, (i + steps) % count) for i in range(count)])  26.8 us
    all_to_all x1, blocking collectives, local(): parts = lax.all_to_all(parts, 'ty', 0, 0, tiled=True)  22.3 us
    ppermute x6, starting transfers between devices, shifted(): lax.ppermute(value, axis, [(i, (i + steps) % count) for i in range(count)])  22.2 us
    all_to_all x1, blocking collectives, local(): lax.all_to_all(down(hidden, w_down4, down_pieces), ('core', 'tx'), 0, 0,...  22.2 us
    all_to_all x1, waiting for transfers between devices, local(): lax.all_to_all(join_rows(outs, cap).reshape(n_z, 2 * cap, width), 'z', 0,...  20.6 us
    pallas_call x11, Pallas kernels, kernel(): pl.pallas_call(body, out_shape=tuple((jax.ShapeDtypeStruct(o, dtype) for...  9.5 us
    all_to_all x1, waiting for transfers between devices, local(): conv_all = lax.all_to_all(conv_copies, TP, 0, 0, tiled=True)  9.36 us
  transfers between devices with their start and end apart: 11, of which 8 were waited for; matrix products, arithmetic and copies ran while one was open for 0% of the time, Pallas kernels for 1%

profile of v2, /device:TPU:8, one launch (start us, length us, event | category | flops | bytes accessed | tf_op | source)
XLA Modules:
  0.0 199.6 jit_solution(6287791225243505350)
XLA Ops:
  0.0 0.0 copy-start.8
  0.0 0.0 copy-start.3
  0.0 0.9 multiply_convert_fusion
  0.9 1.7 collective-permute-start
  2.6 0.8 collective-permute-done
  3.5 0.0 copy-start.7
  3.5 0.6 copy-done.7
  4.1 1.9 shard_map.127
  6.0 8.7 %all-to-all-start = ((bf16[16,64,256]{2,1,0:T(8,128)(2,1)}), bf16[16,64,256]{2,1,0:T(8,128)(2,1)S(1)}, u32[]{:S(2)}, u32[]{:S(2)}) async-start(bf16[16,64,256]{2,1,0:T(8,128)(2,1)} %shard_map.127), calls=%async_computation | async-start | bytes 1048576 | tf_op jit(solution)/shard_map/all_to_all | solution.py:356
  14.7 0.0 copy-done.8
  14.7 0.1 copy.19.pick_ref
  14.8 0.5 shard_map.128.slot_ref
  15.4 9.4 %all-to-all-done = bf16[16,64,256]{2,1,0:T(8,128)(2,1)S(1)} async-done(((bf16[16,64,256]{2,1,0:T(8,128)(2,1)}), bf16[16,64,256]{2,1,0:T(8,128)(2,1)S(1)}, u32[]{:S(2)}, u32[]{:S(2)}) %all-to-all-start) | async-done | bytes 524320 | tf_op jit(solution)/shard_map/all_to_all | solution.py:356
  24.7 0.0 copy-done.3
  24.7 0.0 copy-done.4
  24.7 0.7 shard_map.129
  25.4 34.5 %all_to_all.35 = bf16[16,40,256]{2,1,0:T(8,128)(2,1)S(1)} all-to-all(bf16[16,40,256]{2,1,0:T(8,128)(2,1)S(1)} %bitcast.30), channel_id=1, replica_groups=mesh['z'=16,'core'=2,'ty'=4,'tx'=4] {'z'}, dimensions={0} | all-to-all | bytes 655360 | tf_op jit(solution)/shard_map/all_to_all | solution.py:372
  60.0 1.3 shard_map.130
  61.3 0.0 copy-start
  61.3 0.0 copy-start.1
  61.3 3.9 %all-to-all-start.2 = ((bf16[8,320,256]{2,1,0:T(8,128)(2,1)}), bf16[8,320,256]{2,1,0:T(8,128)(2,1)S(1)}, u32[]{:S(2)}, u32[]{:S(2)}) async-start(bf16[8,320,256]{2,1,0:T(8,128)(2,1)} %shard_map.130), calls=%async_computation.2 | async-start | bytes 2621440 | tf_op jit(solution)/shard_map/all_to_all | solution.py:376
  65.2 0.0 copy-done
  65.2 0.0 copy-done.1
  65.2 0.2 shard_map.131
  65.4 3.4 %collective-permute-start.1 = (bf16[1024,256]{1,0:T(8,128)(2,1)S(1)}, bf16[1024,256]{1,0:T(8,128)(2,1)S(1)}, u32[]{:S(2)}, u32[]{:S(2)}) collective-permute-start(bf16[1024,256]{1,0:T(8,128)(2,1)S(1)} %get-tuple-element.15), channel_id=1, source_target_pairs={{0,4},{4,8},{8,12},{12,0},{1,5},{5,9},{9,13},{13,1},{2,6},{6,10},{... | collective-permute-start | bytes 1572872 | tf_op jit(solution)/shard_map/ppermute | solution.py:321
  68.8 0.0 copy-start.10
  68.8 5.2 %collective-permute-start.2 = (bf16[1024,256]{1,0:T(8,128)(2,1)S(1)}, bf16[1024,256]{1,0:T(8,128)(2,1)S(1)}, u32[]{:S(2)}, u32[]{:S(2)}) collective-permute-start(bf16[1024,256]{1,0:T(8,128)(2,1)S(1)} %get-tuple-element.16), channel_id=1, source_target_pairs={{0,8},{4,12},{8,0},{12,4},{1,9},{5,13},{9,1},{13,5},{2,10},{6,14},... | collective-permute-start | bytes 1572872 | tf_op jit(solution)/shard_map/ppermute | solution.py:321
  74.0 0.1 shard_map.132
  74.1 2.2 %collective-permute-start.3 = (bf16[1024,256]{1,0:T(8,128)(2,1)S(1)}, bf16[1024,256]{1,0:T(8,128)(2,1)}, u32[]{:S(2)}, u32[]{:S(2)}) collective-permute-start(bf16[1024,256]{1,0:T(8,128)(2,1)S(1)} %shard_map.132), channel_id=1, source_target_pairs={{0,12},{4,0},{8,4},{12,8},{1,13},{5,1},{9,5},{13,9},{2,14},{6,2},{... | collective-permute-start | bytes 1572872 | tf_op jit(solution)/shard_map/ppermute | solution.py:321
  76.3 0.0 copy-done.10
  76.3 6.5 %collective-permute-done.1.rest_0_ = bf16[1024,256]{1,0:T(8,128)(2,1)S(1)} collective-permute-done((bf16[1024,256]{1,0:T(8,128)(2,1)S(1)}, bf16[1024,256]{1,0:T(8,128)(2,1)S(1)}, u32[]{:S(2)}, u32[]{:S(2)}) %collective-permute-start.1) | collective-permute-done | bytes 524320 | tf_op jit(solution)/shard_map/ppermute | solution.py:321
  82.8 0.0 copy-start.5
  82.8 4.3 %collective-permute-done.2.rest_1_ = bf16[1024,256]{1,0:T(8,128)(2,1)S(1)} collective-permute-done((bf16[1024,256]{1,0:T(8,128)(2,1)S(1)}, bf16[1024,256]{1,0:T(8,128)(2,1)S(1)}, u32[]{:S(2)}, u32[]{:S(2)}) %collective-permute-start.2) | collective-permute-done | bytes 524320 | tf_op jit(solution)/shard_map/ppermute | solution.py:321
  87.1 0.0 copy-done.5
  87.1 0.0 copy-start.6
  87.1 0.8 copy-done.6
  87.9 9.7 %collective-permute-done.3.rest_2_ = bf16[1024,256]{1,0:T(8,128)(2,1)} collective-permute-done((bf16[1024,256]{1,0:T(8,128)(2,1)S(1)}, bf16[1024,256]{1,0:T(8,128)(2,1)}, u32[]{:S(2)}, u32[]{:S(2)}) %collective-permute-start.3) | collective-permute-done | bytes 524320 | tf_op jit(solution)/shard_map/ppermute | solution.py:321
  97.6 0.0 all-to-all-done.2.x_ref
  97.6 3.2 %gate_up.1 = bf16[4,648,256]{2,1,0:T(8,128)(2,1)S(1)} custom-call(bf16[8,320,256]{2,1,0:T(8,128)(2,1)S(1)} %all-to-all-done.2.x_ref, bf16[1,4096]{1,0:T(2,128)(2,1)S(1)} %reshape.25.gain_ref, bf16[4096,128]{1,0:T(8,128)(2,1)S(1)} %bitcast.21, bf16[4096,128]{1,0:T(8,128)(2,1)S(1)} %bitcast.24, bf16[1024,256]{1,0:T(8,128)(2,1)} %copy-done.5, ...), custom_call_target="tpu_custom_call" | custom-call | tf_op jit(solution)/shard_map/gate_up/pallas_call | solution.py:230
  100.8 22.3 %all_to_all.36.p_ref = bf16[4,648,256]{2,1,0:T(8,128)(2,1)S(1)} all-to-all(bf16[4,648,256]{2,1,0:T(8,128)(2,1)S(1)} %gate_up.1), channel_id=1, replica_groups=mesh['z'=16,'core'=2,'ty'=4,'tx'=4] {'ty'}, dimensions={0} | all-to-all | bytes 2654208 | tf_op jit(solution)/shard_map/all_to_all | solution.py:378
  123.1 0.0 copy-start.2
  123.1 1.2 shard_map.133
  124.3 4.9 %all-to-all-start.4 = ((bf16[4,640,128]{2,1,0:T(8,128)(2,1)}), bf16[4,640,128]{2,1,0:T(8,128)(2,1)S(1)}, u32[]{:S(2)}, u32[]{:S(2)}) async-start(bf16[4,640,128]{2,1,0:T(8,128)(2,1)} %shard_map.133), calls=%async_computation.4 | async-start | bytes 1310720 | tf_op jit(solution)/shard_map/all_to_all | solution.py:380
  129.2 0.0 copy-done.2
  129.2 0.1 dynamic-slice_bitcast_fusion
  129.2 3.5 %collective-permute-start.4 = (bf16[4,128,256]{2,1,0:T(8,128)(2,1)S(1)}, bf16[4,128,256]{2,1,0:T(8,128)(2,1)S(1)}, u32[]{:S(2)}, u32[]{:S(2)}) collective-permute-start(bf16[4,128,256]{2,1,0:T(8,128)(2,1)S(1)} %get-tuple-element.25), channel_id=1, source_target_pairs={{0,1},{1,2},{2,3},{3,0},{4,5},{5,6},{6,7},{7,4},{8,9},{9,10},{10,1... | collective-permute-start | bytes 786440 | tf_op jit(solution)/shard_map/ppermute | solution.py:321
  132.8 4.6 %collective-permute-start.5 = (bf16[4,128,256]{2,1,0:T(8,128)(2,1)S(1)}, bf16[4,128,256]{2,1,0:T(8,128)(2,1)S(1)}, u32[]{:S(2)}, u32[]{:S(2)}) collective-permute-start(bf16[4,128,256]{2,1,0:T(8,128)(2,1)S(1)} %get-tuple-element.24), channel_id=1, source_target_pairs={{0,2},{1,3},{2,0},{3,1},{4,6},{5,7},{6,4},{7,5},{8,10},{9,11},{10,... | collective-permute-start | bytes 786440 | tf_op jit(solution)/shard_map/ppermute | solution.py:321
  137.4 3.4 %collective-permute-start.6 = (bf16[4,128,256]{2,1,0:T(8,128)(2,1)S(1)}, bf16[4,128,256]{2,1,0:T(8,128)(2,1)S(1)}, u32[]{:S(2)}, u32[]{:S(2)}) collective-permute-start(bf16[4,128,256]{2,1,0:T(8,128)(2,1)S(1)} %get-tuple-element.23), channel_id=1, source_target_pairs={{0,3},{1,0},{2,1},{3,2},{4,7},{5,4},{6,5},{7,6},{8,11},{9,8},{10,9... | collective-permute-start | bytes 786440 | tf_op jit(solution)/shard_map/ppermute | solution.py:321
  140.8 0.0 collective-permute-done.4.rest_0_
  140.8 4.8 %collective-permute-done.5.rest_1_ = bf16[4,128,256]{2,1,0:T(8,128)(2,1)S(1)} collective-permute-done((bf16[4,128,256]{2,1,0:T(8,128)(2,1)S(1)}, bf16[4,128,256]{2,1,0:T(8,128)(2,1)S(1)}, u32[]{:S(2)}, u32[]{:S(2)}) %collective-permute-start.5) | collective-permute-done | bytes 262176 | tf_op jit(solution)/shard_map/ppermute | solution.py:321
  145.6 1.5 collective-permute-done.6.rest_2_
  147.1 0.0 all-to-all-done.4.h_ref
  147.1 0.8 shard_map.134
  148.0 22.2 %all_to_all.37.p_ref = bf16[8,320,256]{2,1,0:T(8,128)(2,1)S(1)} all-to-all(bf16[8,320,256]{2,1,0:T(8,128)(2,1)S(1)} %shard_map.134), channel_id=1, replica_groups=mesh['z'=16,'core'=2,'ty'=4,'tx'=4] {'core','tx'}, dimensions={0} | all-to-all | bytes 2621440 | tf_op jit(solution)/shard_map/all_to_all | solution.py:381
  170.2 0.0 copy-start.9
  170.2 1.1 shard_map.135
  171.3 5.8 %all-to-all-start.6 = ((bf16[16,40,256]{2,1,0:T(8,128)(2,1)}), bf16[16,40,256]{2,1,0:T(8,128)(2,1)S(1)}, u32[]{:S(2)}, u32[]{:S(2)}) async-start(bf16[16,40,256]{2,1,0:T(8,128)(2,1)} %bitcast.14), calls=%async_computation.6 | async-start | bytes 655360 | tf_op jit(solution)/shard_map/all_to_all | solution.py:386
  177.1 0.0 copy-done.9
  177.2 0.1 copy.20.pick_ref
  177.3 0.5 shard_map.136
  177.8 0.0 copy-done.11
  177.8 0.1 copy.21.w_ref
  178.0 20.6 %all-to-all-done.6 = bf16[16,40,256]{2,1,0:T(8,128)(2,1)S(1)} async-done(((bf16[16,40,256]{2,1,0:T(8,128)(2,1)}), bf16[16,40,256]{2,1,0:T(8,128)(2,1)S(1)}, u32[]{:S(2)}, u32[]{:S(2)}) %all-to-all-start.6) | async-done | bytes 327712 | tf_op jit(solution)/shard_map/all_to_all | solution.py:386
  198.5 1.0 shard_map.137
  (3 shorter events, 0.0 us)
Async XLA Ops:
  0.0 14.7 %copy-start.8 = (s32[256,2]{0,1:T(2,128)S(1)}, s32[256,2]{0,1:T(2,128)}, u32[]{:S(2)}) copy-start(s32[256,2]{0,1:T(2,128)} %param.21) | copy-start | bytes 6148
  0.0 24.7 %copy-start.3 = (bf16[1024,256]{1,0:T(8,128)(2,1)S(1)}, bf16[1024,256]{1,0:T(8,128)(2,1)}, u32[]{:S(2)}) copy-start(bf16[1024,256]{1,0:T(8,128)(2,1)} %w_ref.1) | copy-start | bytes 1572868
  0.0 24.7 %copy-start.4 = (bf16[256,256]{1,0:T(8,128)(2,1)S(1)}, bf16[256,256]{1,0:T(8,128)(2,1)}, u32[]{:S(2)}) copy-start(bf16[256,256]{1,0:T(8,128)(2,1)} %res_ref.1) | copy-start | bytes 393220
  0.9 2.6 %collective-permute-start = (bf16[2,64]{0,1:T(8,128)(2,1)S(1)}, bf16[2,64]{0,1:T(8,128)(2,1)S(1)}, u32[]{:S(2)}, u32[]{:S(2)}) collective-permute-start(bf16[2,64]{0,1:T(8,128)(2,1)S(1)} %multiply_convert_fusion), channel_id=1, source_target_pairs={{0,16},{16,32},{32,48},{48,64},{64,80},{80,96},{96,112},{112,128},... | collective-permute-start | bytes 776 | tf_op jit(solution)/shard_map/ppermute | solution.py:351
  3.5 0.6 copy-start.7
  6.0 18.7 %all-to-all-start = ((bf16[16,64,256]{2,1,0:T(8,128)(2,1)}), bf16[16,64,256]{2,1,0:T(8,128)(2,1)S(1)}, u32[]{:S(2)}, u32[]{:S(2)}) async-start(bf16[16,64,256]{2,1,0:T(8,128)(2,1)} %shard_map.127), calls=%async_computation | async-start | bytes 1048576 | tf_op jit(solution)/shard_map/all_to_all | solution.py:356
  61.3 3.9 %copy-start = (bf16[1,4096,128]{2,1,0:T(8,128)(2,1)S(1)}, bf16[1,4096,128]{2,1,0:T(8,128)(2,1)}, u32[]{:S(2)}) copy-start(bf16[1,4096,128]{2,1,0:T(8,128)(2,1)} %param.23) | copy-start | bytes 3145732
  61.3 3.9 %copy-start.1 = (bf16[1,4096,128]{2,1,0:T(8,128)(2,1)S(1)}, bf16[1,4096,128]{2,1,0:T(8,128)(2,1)}, u32[]{:S(2)}) copy-start(bf16[1,4096,128]{2,1,0:T(8,128)(2,1)} %param.24) | copy-start | bytes 3145732
  61.3 36.3 %all-to-all-start.2 = ((bf16[8,320,256]{2,1,0:T(8,128)(2,1)}), bf16[8,320,256]{2,1,0:T(8,128)(2,1)S(1)}, u32[]{:S(2)}, u32[]{:S(2)}) async-start(bf16[8,320,256]{2,1,0:T(8,128)(2,1)} %shard_map.130), calls=%async_computation.2 | async-start | bytes 2621440 | tf_op jit(solution)/shard_map/all_to_all | solution.py:376
  65.4 17.4 %collective-permute-start.1 = (bf16[1024,256]{1,0:T(8,128)(2,1)S(1)}, bf16[1024,256]{1,0:T(8,128)(2,1)S(1)}, u32[]{:S(2)}, u32[]{:S(2)}) collective-permute-start(bf16[1024,256]{1,0:T(8,128)(2,1)S(1)} %get-tuple-element.15), channel_id=1, source_target_pairs={{0,4},{4,8},{8,12},{12,0},{1,5},{5,9},{9,13},{13,1},{2,6},{6,10},{... | collective-permute-start | bytes 1572872 | tf_op jit(solution)/shard_map/ppermute | solution.py:321
  68.8 7.5 %copy-start.10 = (bf16[4096]{0:T(1024)(128)(2,1)S(1)}, bf16[4096]{0:T(1024)(128)(2,1)}, u32[]{:S(2)}) copy-start(bf16[4096]{0:T(1024)(128)(2,1)} %param.20) | copy-start | bytes 24580
  68.8 18.2 %collective-permute-start.2 = (bf16[1024,256]{1,0:T(8,128)(2,1)S(1)}, bf16[1024,256]{1,0:T(8,128)(2,1)S(1)}, u32[]{:S(2)}, u32[]{:S(2)}) collective-permute-start(bf16[1024,256]{1,0:T(8,128)(2,1)S(1)} %get-tuple-element.16), channel_id=1, source_target_pairs={{0,8},{4,12},{8,0},{12,4},{1,9},{5,13},{9,1},{13,5},{2,10},{6,14},... | collective-permute-start | bytes 1572872 | tf_op jit(solution)/shard_map/ppermute | solution.py:321
  74.1 23.4 %collective-permute-start.3 = (bf16[1024,256]{1,0:T(8,128)(2,1)S(1)}, bf16[1024,256]{1,0:T(8,128)(2,1)}, u32[]{:S(2)}, u32[]{:S(2)}) collective-permute-start(bf16[1024,256]{1,0:T(8,128)(2,1)S(1)} %shard_map.132), channel_id=1, source_target_pairs={{0,12},{4,0},{8,4},{12,8},{1,13},{5,1},{9,5},{13,9},{2,14},{6,2},{... | collective-permute-start | bytes 1572872 | tf_op jit(solution)/shard_map/ppermute | solution.py:321
  82.8 4.3 %copy-start.5 = (bf16[1024,256]{1,0:T(8,128)(2,1)}, bf16[1024,256]{1,0:T(8,128)(2,1)S(1)}, u32[]{:S(2)}) copy-start(bf16[1024,256]{1,0:T(8,128)(2,1)S(1)} %collective-permute-done.1.rest_0_) | copy-start | bytes 1572868
  87.1 0.8 copy-start.6
  123.1 6.1 %copy-start.2 = (bf16[1,2048,256]{2,1,0:T(8,128)(2,1)S(1)}, bf16[1,2048,256]{2,1,0:T(8,128)(2,1)}, u32[]{:S(2)}) copy-start(bf16[1,2048,256]{2,1,0:T(8,128)(2,1)} %param.25) | copy-start | bytes 3145732
  124.3 22.8 %all-to-all-start.4 = ((bf16[4,640,128]{2,1,0:T(8,128)(2,1)}), bf16[4,640,128]{2,1,0:T(8,128)(2,1)S(1)}, u32[]{:S(2)}, u32[]{:S(2)}) async-start(bf16[4,640,128]{2,1,0:T(8,128)(2,1)} %shard_map.133), calls=%async_computation.4 | async-start | bytes 1310720 | tf_op jit(solution)/shard_map/all_to_all | solution.py:380
  129.2 11.5 %collective-permute-start.4 = (bf16[4,128,256]{2,1,0:T(8,128)(2,1)S(1)}, bf16[4,128,256]{2,1,0:T(8,128)(2,1)S(1)}, u32[]{:S(2)}, u32[]{:S(2)}) collective-permute-start(bf16[4,128,256]{2,1,0:T(8,128)(2,1)S(1)} %get-tuple-element.25), channel_id=1, source_target_pairs={{0,1},{1,2},{2,3},{3,0},{4,5},{5,6},{6,7},{7,4},{8,9},{9,10},{10,1... | collective-permute-start | bytes 786440 | tf_op jit(solution)/shard_map/ppermute | solution.py:321
  132.8 12.8 %collective-permute-start.5 = (bf16[4,128,256]{2,1,0:T(8,128)(2,1)S(1)}, bf16[4,128,256]{2,1,0:T(8,128)(2,1)S(1)}, u32[]{:S(2)}, u32[]{:S(2)}) collective-permute-start(bf16[4,128,256]{2,1,0:T(8,128)(2,1)S(1)} %get-tuple-element.24), channel_id=1, source_target_pairs={{0,2},{1,3},{2,0},{3,1},{4,6},{5,7},{6,4},{7,5},{8,10},{9,11},{10,... | collective-permute-start | bytes 786440 | tf_op jit(solution)/shard_map/ppermute | solution.py:321
  137.4 9.7 %collective-permute-start.6 = (bf16[4,128,256]{2,1,0:T(8,128)(2,1)S(1)}, bf16[4,128,256]{2,1,0:T(8,128)(2,1)S(1)}, u32[]{:S(2)}, u32[]{:S(2)}) collective-permute-start(bf16[4,128,256]{2,1,0:T(8,128)(2,1)S(1)} %get-tuple-element.23), channel_id=1, source_target_pairs={{0,3},{1,0},{2,1},{3,2},{4,7},{5,4},{6,5},{7,6},{8,11},{9,8},{10,9... | collective-permute-start | bytes 786440 | tf_op jit(solution)/shard_map/ppermute | solution.py:321
  170.2 7.0 %copy-start.9 = (s32[256,2]{0,1:T(2,128)S(1)}, s32[256,2]{0,1:T(2,128)}, u32[]{:S(2)}) copy-start(s32[256,2]{0,1:T(2,128)} %param.21) | copy-start | bytes 6148
  170.2 7.7 %copy-start.11 = (f32[256,2]{0,1:T(2,128)S(1)}, f32[256,2]{0,1:T(2,128)}, u32[]{:S(2)}) copy-start(f32[256,2]{0,1:T(2,128)} %param.22) | copy-start | bytes 6148
  171.3 27.2 %all-to-all-start.6 = ((bf16[16,40,256]{2,1,0:T(8,128)(2,1)}), bf16[16,40,256]{2,1,0:T(8,128)(2,1)S(1)}, u32[]{:S(2)}, u32[]{:S(2)}) async-start(bf16[16,40,256]{2,1,0:T(8,128)(2,1)} %bitcast.14), calls=%async_computation.6 | async-start | bytes 655360 | tf_op jit(solution)/shard_map/all_to_all | solution.py:386

commit v3 on v2

--- a/solution.py
+++ b/solution.py
@@ -69,18 +69,6 @@
     return kernel(body, ((8, toks),), pick, dtype=jnp.int32)
 
 
-def routing_back(pick, rows, cap):
-    toks = pick.shape[0]
-
-    def body(pick_ref, c0_ref, c1_ref):
-        t0, t1 = slots(pick_ref, cap)
-        lanes = iota((toks, rows), 1)
-        c0_ref[...] = (lanes == t0).astype(F32).astype(BF16)
-        c1_ref[...] = (lanes == t1).astype(F32).astype(BF16)
-
-    return kernel(body, ((toks, rows), (toks, rows)), pick)
-
-
 def project(conv_all, out_weight, residual, slot_rows, rows):
     toks, width = residual.shape
 
@@ -95,12 +83,13 @@
     return kernel(body, outs, conv_all, out_weight, residual, slot_rows)
 
 
-def convolve(b_gate, c_gate, h_in, edge, docs, taps, copies):
+def convolve_head(b_gate, c_gate, h_in, docs, taps):
     chans, toks = h_in.shape
     lane = docs.shape[1]
     per = toks // lane
 
-    def body(b_ref, c_ref, h_ref, edge_ref, docs_ref, taps_ref, out_ref):
+    def body(b_ref, c_ref, h_ref, docs_ref, taps_ref, total_ref, factor_ref, gate_ref):
+        gate_ref[...] = b_ref[...].astype(F32)
         sp = lax.axis_index("z") * 2 + lax.axis_index("core")
         tp = lax.axis_index("ty") * lax.axis_size("tx") + lax.axis_index("tx")
         own = jnp.concatenate([docs_ref[pl.ds(sp * per + k, 1), :] for k in range(per)], axis=1)
@@ -110,25 +99,43 @@
         back1 = jnp.where(at == 0, prior[:, lane - 1 :], pltpu.roll(own, 1, 1))
         back2 = jnp.where(at == 1, prior[:, lane - 1 :], pltpu.roll(own, 2, 1))
         back2 = jnp.where(at == 0, prior[:, lane - 2 : lane - 1], back2)
+        same1 = (back1 == own).astype(F32)
+        same2 = (back2 == own).astype(F32)
         all_taps = taps_ref[...].astype(F32)
-        first = lax.rem(all_taps.shape[1] - tp * chans, all_taps.shape[1])
-        near = pltpu.roll(jnp.concatenate([all_taps, jnp.zeros((5, all_taps.shape[1]), F32)]), first, 1)
+        length = all_taps.shape[1]
+        first = lax.rem(length - tp * chans, length)
+        near = pltpu.roll(jnp.concatenate([all_taps, jnp.zeros((5, length), F32)]), first, 1)
         tap = [to_col(near[k : k + 1, :chans], chans, 0) for k in range(3)]
         product = (c_ref[...].astype(F32) * h_ref[...].astype(F32)).astype(BF16).astype(F32)
         lanes = iota((chans, toks), 1)
+        one = jnp.where(lanes >= 1, pltpu.roll(product, 1, 1), 0.0)
+        two = jnp.where(lanes >= 2, pltpu.roll(product, 2, 1), 0.0)
+        total_ref[...] = tap[0] * product + tap[1] * one * same1 + tap[2] * two * same2
+        place = iota((chans, lane), 1)
+        factor = jnp.where(place == 0, tap[1] * same1[:, 0:1], tap[2] * same2[:, 0:1])
+        factor_ref[...] = jnp.where(place == 2, tap[2] * same2[:, 1:2], factor)
+
+    outs = ((chans, toks), (chans, lane), (chans, toks))
+    return kernel(body, outs, b_gate, c_gate, h_in, docs, taps, dtype=F32)
+
+
+def convolve(total, factor, gate, edge, copies):
+    chans, toks = gate.shape
+
+    def body(total_ref, factor_ref, gate_ref, edge_ref, out_ref):
         before = [edge_ref[:, k : k + 1].astype(F32) for k in range(2)]
-        one = jnp.where(lanes == 0, before[1], pltpu.roll(product, 1, 1))
-        two = pltpu.roll(product, 2, 1)
-        two = jnp.where(lanes == 0, before[0], jnp.where(lanes == 1, before[1], two))
-        total = tap[0] * product
-        total = total + tap[1] * one * (back1 == own).astype(F32)
-        total = total + tap[2] * two * (back2 == own).astype(F32)
-        conv = (b_ref[...].astype(F32) * total).astype(BF16)
+        at0, at1, at2 = (factor_ref[:, k : k + 1] for k in range(3))
+        lanes = iota((chans, toks), 1)
+        whole = total_ref[...]
+        whole = whole + jnp.where(lanes == 0, at0 * before[1], 0.0)
+        whole = whole + jnp.where(
+            lanes == 0, at1 * before[0], jnp.where(lanes == 1, at2 * before[1], 0.0)
+        )
+        conv = (gate_ref[...] * whole).astype(BF16)
         for k in range(copies):
             out_ref[k] = conv
 
-    outs = ((copies, chans, toks),)
-    return kernel(body, outs, b_gate, c_gate, h_in, edge, docs, taps, limit=None)
+    return kernel(body, ((copies, chans, toks),), total, factor, gate, edge)
 
 
 def order_map(cap, block, splitting):
@@ -198,7 +205,8 @@
             move.start()
         ty = lax.axis_index("ty")
         mine = pl.ds(pl.multiple_of(ty * feats, feats), feats)
-        gain_row = gain_ref[:, mine].astype(F32)
+        gain_rows = gain_ref[pl.ds(pl.multiple_of(ty * (feats // 128), 8), feats // 128), :].astype(F32)
+        gain_row = jnp.concatenate([gain_rows[k : k + 1] for k in range(feats // 128)], axis=1)
         extra = jnp.zeros((8, 2 * hid), F32)
         place = iota((8, 2 * hid), 0)
         scaled = []
@@ -266,24 +274,42 @@
 
 
 def down(hidden, w_down, pieces):
-    n_ty, rows, _ = hidden.shape
+    n_ty, rows, hid = hidden.shape
     n_tx = len(pieces) + 1
     half = rows // 2
     width = w_down.shape[-1]
 
     def body(h_ref, wd_ref, *rest):
-        piece_refs, out_ref = rest[:-1], rest[-1]
+        piece_refs, out_ref, held, sems = rest[: n_tx - 1], rest[-3], rest[-2], rest[-1]
+        moves = [
+            pltpu.make_async_copy(ref, held.at[d], sems.at[d]) for d, ref in enumerate(piece_refs)
+        ]
+        for move in moves:
+            move.start()
         tx = lax.axis_index("tx")
         h = jnp.concatenate([h_ref[k] for k in range(n_ty)], axis=1)
         for d in range(n_tx):
-            w = [wd_ref[b, tx] if d == 0 else piece_refs[d - 1][b] for b in range(n_ty)]
+            if d:
+                moves[d - 1].wait()
+            w = [wd_ref[b, tx] if d == 0 else held[d - 1, b] for b in range(n_ty)]
             part = dot(h, jnp.concatenate(w, axis=0)).astype(BF16)
             to = lax.rem(tx + (n_tx - d), n_tx)
             out_ref[to] = part[:half]
             out_ref[n_tx + to] = part[half:]
 
-    outs = ((2 * n_tx, half, width),)
-    return kernel(body, outs, hidden, w_down, *pieces, limit=24)
+    vmem = pl.BlockSpec(memory_space=pltpu.VMEM)
+    return pl.pallas_call(
+        body,
+        out_shape=jax.ShapeDtypeStruct((2 * n_tx, half, width), BF16),
+        in_specs=[vmem] * 2 + [pl.BlockSpec(memory_space=pltpu.HBM)] * (n_tx - 1),
+        out_specs=vmem,
+        scratch_shapes=[
+            pltpu.VMEM((n_tx - 1, n_ty, hid, width), BF16),
+            pltpu.SemaphoreType.DMA((n_tx - 1,)),
+        ],
+        compiler_params=pltpu.CompilerParams(vmem_limit_bytes=24 << 20),
+        name="down",
+    )(hidden, w_down, *[pltpu.with_memory_space_constraint(p, pltpu.HBM) for p in pieces])
 
 
 def join_rows(parts, cap):
@@ -307,13 +333,22 @@
     return kernel(body, ((2 * half, width),), parts)
 
 
-def combine(back, c0, c1, weights, stream):
-    def body(back_ref, c0_ref, c1_ref, w_ref, stream_ref, out_ref):
-        rows = back_ref[...]
-        feed = dot(c0_ref[...], rows) * w_ref[:, 0:1] + dot(c1_ref[...], rows) * w_ref[:, 1:2]
-        out_ref[...] = (stream_ref[...].astype(F32) + feed).astype(BF16)
-
-    return kernel(body, (stream.shape,), back, c0, c1, weights, stream)
+def combine(back, slot_rows, weights, stream):
+    toks = stream.shape[0]
+    rows = back.shape[0]
+
+    def body(back_ref, slot_ref, w_ref, stream_ref, out_ref):
+        got = back_ref[...]
+        lanes = iota((toks, rows), 1)
+        total = stream_ref[...].astype(F32)
+        feed = jnp.zeros(total.shape, F32)
+        for k in range(2):
+            slot = to_col(slot_ref[k : k + 1, :], toks, 0)
+            picked = dot((lanes == slot).astype(F32).astype(BF16), got)
+            feed = feed + picked * to_col(w_ref[k : k + 1, :], toks, 0)
+        out_ref[...] = (total + feed).astype(BF16)
+
+    return kernel(body, (stream.shape,), back, slot_rows, weights, stream)
 
 
 def shifted(value, axis, steps):
@@ -350,9 +385,8 @@
     product = (c_gate[last].astype(F32) * h_in[last].astype(F32)).astype(BF16)
     edge = lax.ppermute(product, ("z", "core"), [(i, i + 1) for i in range(n_sp - 1)])
     n_tp = n_ty * n_tx
-    conv_copies = convolve(
-        b_gate.T, c_gate.T, h_in.T, edge.T, docs.reshape(-1, 128), conv_taps, n_tp
-    )
+    head = convolve_head(b_gate.T, c_gate.T, h_in.T, docs.reshape(-1, 128), conv_taps)
+    conv_copies = convolve(*head, edge.T, n_tp)
     conv_all = lax.all_to_all(conv_copies, TP, 0, 0, tiled=True)
     conv_all = conv_all.reshape(n_tp * chans, toks)
 
@@ -374,19 +408,17 @@
     ).reshape(rows, width)
     split = split_rows(got, n_tx, cap)
     x = lax.all_to_all(split, ("core", "tx"), 0, 0, tiled=True)
-    parts = gate_up(x, norm_gain.reshape(1, -1), w_gate[0], w_up[0], gate_up_pieces)
+    parts = gate_up(x, norm_gain.reshape(-1, 128), w_gate[0], w_up[0], gate_up_pieces)
     parts = lax.all_to_all(parts, "ty", 0, 0, tiled=True)
     hidden = activate(parts, full_dim)
     hidden = lax.all_to_all(hidden, "ty", 0, 0, tiled=True)
     outs = lax.all_to_all(
         down(hidden, w_down4, down_pieces), ("core", "tx"), 0, 0, tiled=True
     )
-    outs, late_pick, late_weight = lax.optimization_barrier((outs, expert_pick, route_weight))
-    c0, c1 = routing_back(late_pick, rows, cap)
     back = lax.all_to_all(
         join_rows(outs, cap).reshape(n_z, 2 * cap, width), "z", 0, 0, tiled=True
     ).reshape(rows, width)
-    return combine(back, c0, c1, late_weight, stream)
+    return combine(back, slot_rows, route_weight.T, stream)
 
 
 def solution(mesh):

time: 200 us -> 205 us (1.025)
  blocking collectives: 79 us -> 107 us
  waiting for transfers between devices: 57.5 us -> 36.1 us
  starting transfers between devices: 47.4 us -> 41.3 us
  local copies, waits for them, and re-layouts: 1.9 us -> 5.44 us
    all_to_all x0 -> x1, blocking collectives: none -> 27.3 us  [local(): lax.all_to_all(join_rows(outs, cap).reshape(n_z, 2 * cap, width), 'z', 0,...]
    all_to_all x1 -> x0, waiting for transfers between devices: 20.6 us -> none  [local(): lax.all_to_all(join_rows(outs, cap).reshape(n_z, 2 * cap, width), 'z', 0,...]
    all_to_all x1 -> x0, starting transfers between devices: 5.85 us -> none  [local(): lax.all_to_all(join_rows(outs, cap).reshape(n_z, 2 * cap, width), 'z', 0,...]
    unnamed x25 -> x37, local copies, waits for them, and re-layouts: 1.57 us -> 5.39 us
    pallas_call x0 -> x1, Pallas kernels: none -> 2.81 us  [down(): pl.pallas_call(body, out_shape=jax.ShapeDtypeStruct((2 * n_tx, half, widt...]
    pallas_call x11 -> x10, Pallas kernels: 9.5 us -> 6.89 us  [kernel(): pl.pallas_call(body, out_shape=tuple((jax.ShapeDtypeStruct(o, dtype) for...]
  transfers between devices with their start and end apart: 11 -> 10, of which waited for: 8 -> 6; matrix products, arithmetic and copies ran while one was open for 0% -> 0% of each run, Pallas kernels for 1% -> 1%
where the time goes in v3:
time: 205 us; the launch traced here: 204 us
  blocking collectives  107 us (52%)
  starting transfers between devices  41.3 us (20%)
  waiting for transfers between devices  36.1 us (18%)
  Pallas kernels  12.9 us (6%)
  local copies, waits for them, and re-layouts  5.44 us (3%)
    all_to_all x1, blocking collectives, local(): lax.all_to_all(outgoing.reshape(n_z, 2 * cap, width), 'z', 0, 0, tiled=True)  34.9 us
    all_to_all x1, blocking collectives, local(): lax.all_to_all(join_rows(outs, cap).reshape(n_z, 2 * cap, width), 'z', 0,...  27.3 us
    ppermute x6, waiting for transfers between devices, shifted(): lax.ppermute(value, axis, [(i, (i + steps) % count) for i in range(count)])  26.8 us
    all_to_all x1, blocking collectives, local(): parts = lax.all_to_all(parts, 'ty', 0, 0, tiled=True)  22.3 us
    all_to_all x1, blocking collectives, local(): lax.all_to_all(down(hidden, w_down4, down_pieces), ('core', 'tx'), 0, 0,...  22.2 us
    ppermute x6, starting transfers between devices, shifted(): lax.ppermute(value, axis, [(i, (i + steps) % count) for i in range(count)])  22.2 us
    all_to_all x1, waiting for transfers between devices, local(): conv_all = lax.all_to_all(conv_copies, TP, 0, 0, tiled=True)  9.33 us
    all_to_all x1, starting transfers between devices, local(): conv_all = lax.all_to_all(conv_copies, TP, 0, 0, tiled=True)  8.73 us
  transfers between devices with their start and end apart: 10, of which 6 were waited for; matrix products, arithmetic and copies ran while one was open for 0% of the time, Pallas kernels for 1%

profile of v3, /device:TPU:8, one launch (start us, length us, event | category | flops | bytes accessed | tf_op | source)
XLA Modules:
  0.0 203.6 jit_solution(1007596397312320765)
XLA Ops:
  0.0 0.0 copy-start.3
  0.0 0.0 copy-start.4
  0.0 0.9 multiply_convert_fusion
  0.9 1.7 collective-permute-start
  2.6 0.0 copy-start.5
  2.6 0.7 copy-done.5
  3.4 0.0 copy-start.6
  3.4 0.8 copy-done.6
  4.2 0.0 copy-start.7
  4.2 0.8 copy-done.7
  4.9 0.8 copy-done.8
  5.7 0.7 copy-done.10
  6.4 0.3 shard_map.127
  6.7 0.0 collective-permute-done
  6.7 1.0 shard_map.128
  7.7 8.7 %all-to-all-start = ((bf16[16,64,256]{2,1,0:T(8,128)(2,1)}), bf16[16,64,256]{2,1,0:T(8,128)(2,1)S(1)}, u32[]{:S(2)}, u32[]{:S(2)}) async-start(bf16[16,64,256]{2,1,0:T(8,128)(2,1)} %shard_map.128), calls=%async_computation | async-start | bytes 1048576 | tf_op jit(solution)/shard_map/all_to_all | solution.py:390
  16.4 0.0 copy-done.17
  16.4 0.1 copy.17.pick_ref
  16.6 0.5 shard_map.129.slot_ref
  17.1 9.3 %all-to-all-done = bf16[16,64,256]{2,1,0:T(8,128)(2,1)S(1)} async-done(((bf16[16,64,256]{2,1,0:T(8,128)(2,1)}), bf16[16,64,256]{2,1,0:T(8,128)(2,1)S(1)}, u32[]{:S(2)}, u32[]{:S(2)}) %all-to-all-start) | async-done | bytes 524320 | tf_op jit(solution)/shard_map/all_to_all | solution.py:390
  26.4 0.0 copy-done.3
  26.4 0.0 copy-done.4
  26.4 0.7 shard_map.130
  27.1 34.9 %all_to_all.35 = bf16[16,40,256]{2,1,0:T(8,128)(2,1)S(1)} all-to-all(bf16[16,40,256]{2,1,0:T(8,128)(2,1)S(1)} %bitcast.33), channel_id=1, replica_groups=mesh['z'=16,'core'=2,'ty'=4,'tx'=4] {'z'}, dimensions={0} | all-to-all | bytes 655360 | tf_op jit(solution)/shard_map/all_to_all | solution.py:406
  62.1 1.3 shard_map.131
  63.4 3.7 %all-to-all-start.2 = ((bf16[8,320,256]{2,1,0:T(8,128)(2,1)}), bf16[8,320,256]{2,1,0:T(8,128)(2,1)S(1)}, u32[]{:S(2)}, u32[]{:S(2)}) async-start(bf16[8,320,256]{2,1,0:T(8,128)(2,1)} %shard_map.131), calls=%async_computation.2 | async-start | bytes 2621440 | tf_op jit(solution)/shard_map/all_to_all | solution.py:410
  67.1 0.0 copy-done
  67.1 0.0 copy-done.1
  67.1 0.2 shard_map.132
  67.3 3.3 %collective-permute-start.1 = (bf16[1024,256]{1,0:T(8,128)(2,1)S(1)}, bf16[1024,256]{1,0:T(8,128)(2,1)S(1)}, u32[]{:S(2)}, u32[]{:S(2)}) collective-permute-start(bf16[1024,256]{1,0:T(8,128)(2,1)S(1)} %get-tuple-element.16), channel_id=1, source_target_pairs={{0,4},{4,8},{8,12},{12,0},{1,5},{5,9},{9,13},{13,1},{2,6},{6,10},{... | collective-permute-start | bytes 1572872 | tf_op jit(solution)/shard_map/ppermute | solution.py:356
  70.7 0.0 copy-start.9
  70.7 5.2 %collective-permute-start.2 = (bf16[1024,256]{1,0:T(8,128)(2,1)S(1)}, bf16[1024,256]{1,0:T(8,128)(2,1)S(1)}, u32[]{:S(2)}, u32[]{:S(2)}) collective-permute-start(bf16[1024,256]{1,0:T(8,128)(2,1)S(1)} %get-tuple-element.17), channel_id=1, source_target_pairs={{0,8},{4,12},{8,0},{12,4},{1,9},{5,13},{9,1},{13,5},{2,10},{6,14},... | collective-permute-start | bytes 1572872 | tf_op jit(solution)/shard_map/ppermute | solution.py:356
  75.9 0.1 shard_map.133
  76.0 2.2 %collective-permute-start.3 = (bf16[1024,256]{1,0:T(8,128)(2,1)S(1)}, bf16[1024,256]{1,0:T(8,128)(2,1)}, u32[]{:S(2)}, u32[]{:S(2)}) collective-permute-start(bf16[1024,256]{1,0:T(8,128)(2,1)S(1)} %shard_map.133), channel_id=1, source_target_pairs={{0,12},{4,0},{8,4},{12,8},{1,13},{5,1},{9,5},{13,9},{2,14},{6,2},{... | collective-permute-start | bytes 1572872 | tf_op jit(solution)/shard_map/ppermute | solution.py:356
  78.2 6.5 %collective-permute-done.1.rest_0_ = bf16[1024,256]{1,0:T(8,128)(2,1)S(1)} collective-permute-done((bf16[1024,256]{1,0:T(8,128)(2,1)S(1)}, bf16[1024,256]{1,0:T(8,128)(2,1)S(1)}, u32[]{:S(2)}, u32[]{:S(2)}) %collective-permute-start.1) | collective-permute-done | bytes 524320 | tf_op jit(solution)/shard_map/ppermute | solution.py:356
  84.6 4.3 %collective-permute-done.2.rest_1_ = bf16[1024,256]{1,0:T(8,128)(2,1)S(1)} collective-permute-done((bf16[1024,256]{1,0:T(8,128)(2,1)S(1)}, bf16[1024,256]{1,0:T(8,128)(2,1)S(1)}, u32[]{:S(2)}, u32[]{:S(2)}) %collective-permute-start.2) | collective-permute-done | bytes 524320 | tf_op jit(solution)/shard_map/ppermute | solution.py:356
  88.9 0.0 copy-done.12
  88.9 0.8 copy-done.13
  89.7 9.7 %collective-permute-done.3.rest_2_ = bf16[1024,256]{1,0:T(8,128)(2,1)} collective-permute-done((bf16[1024,256]{1,0:T(8,128)(2,1)S(1)}, bf16[1024,256]{1,0:T(8,128)(2,1)}, u32[]{:S(2)}, u32[]{:S(2)}) %collective-permute-start.3) | collective-permute-done | bytes 524320 | tf_op jit(solution)/shard_map/ppermute | solution.py:356
  99.4 0.0 all-to-all-done.2.x_ref
  99.4 0.0 copy-done.9
  99.4 3.2 %gate_up.1 = bf16[4,648,256]{2,1,0:T(8,128)(2,1)S(1)} custom-call(bf16[8,320,256]{2,1,0:T(8,128)(2,1)S(1)} %all-to-all-done.2.x_ref, bf16[32,128]{1,0:T(8,128)(2,1)S(1)} %bitcast.39, bf16[4096,128]{1,0:T(8,128)(2,1)S(1)} %bitcast.23, bf16[4096,128]{1,0:T(8,128)(2,1)S(1)} %bitcast.26, bf16[1024,256]{1,0:T(8,128)(2,1)} %copy-done.12, ...), custom_call_target="tpu_custom_call" | custom-call | tf_op jit(solution)/shard_map/gate_up/pallas_call | solution.py:238
  102.6 22.3 %all_to_all.36.p_ref = bf16[4,648,256]{2,1,0:T(8,128)(2,1)S(1)} all-to-all(bf16[4,648,256]{2,1,0:T(8,128)(2,1)S(1)} %gate_up.1), channel_id=1, replica_groups=mesh['z'=16,'core'=2,'ty'=4,'tx'=4] {'ty'}, dimensions={0} | all-to-all | bytes 2654208 | tf_op jit(solution)/shard_map/all_to_all | solution.py:412
  124.9 1.2 shard_map.134
  126.1 4.9 %all-to-all-start.4 = ((bf16[4,640,128]{2,1,0:T(8,128)(2,1)}), bf16[4,640,128]{2,1,0:T(8,128)(2,1)S(1)}, u32[]{:S(2)}, u32[]{:S(2)}) async-start(bf16[4,640,128]{2,1,0:T(8,128)(2,1)} %shard_map.134), calls=%async_computation.4 | async-start | bytes 1310720 | tf_op jit(solution)/shard_map/all_to_all | solution.py:414
  131.0 0.0 copy-done.2
  131.0 0.1 dynamic-slice_bitcast_fusion
  131.1 3.5 %collective-permute-start.4 = (bf16[4,128,256]{2,1,0:T(8,128)(2,1)S(1)}, bf16[4,128,256]{2,1,0:T(8,128)(2,1)S(1)}, u32[]{:S(2)}, u32[]{:S(2)}) collective-permute-start(bf16[4,128,256]{2,1,0:T(8,128)(2,1)S(1)} %get-tuple-element.21), channel_id=1, source_target_pairs={{0,1},{1,2},{2,3},{3,0},{4,5},{5,6},{6,7},{7,4},{8,9},{9,10},{10,1... | collective-permute-start | bytes 786440 | tf_op jit(solution)/shard_map/ppermute | solution.py:356
  134.6 4.6 %collective-permute-start.5 = (bf16[4,128,256]{2,1,0:T(8,128)(2,1)S(1)}, bf16[4,128,256]{2,1,0:T(8,128)(2,1)S(1)}, u32[]{:S(2)}, u32[]{:S(2)}) collective-permute-start(bf16[4,128,256]{2,1,0:T(8,128)(2,1)S(1)} %get-tuple-element.20), channel_id=1, source_target_pairs={{0,2},{1,3},{2,0},{3,1},{4,6},{5,7},{6,4},{7,5},{8,10},{9,11},{10,... | collective-permute-start | bytes 786440 | tf_op jit(solution)/shard_map/ppermute | solution.py:356
  139.2 3.4 %collective-permute-start.6 = (bf16[4,128,256]{2,1,0:T(8,128)(2,1)S(1)}, bf16[4,128,256]{2,1,0:T(8,128)(2,1)S(1)}, u32[]{:S(2)}, u32[]{:S(2)}) collective-permute-start(bf16[4,128,256]{2,1,0:T(8,128)(2,1)S(1)} %get-tuple-element.19), channel_id=1, source_target_pairs={{0,3},{1,0},{2,1},{3,2},{4,7},{5,4},{6,5},{7,6},{8,11},{9,8},{10,9... | collective-permute-start | bytes 786440 | tf_op jit(solution)/shard_map/ppermute | solution.py:356
  142.6 0.0 collective-permute-done.4.rest_0_
  142.6 0.0 copy-start.14
  142.6 4.8 %collective-permute-done.5.rest_1_ = bf16[4,128,256]{2,1,0:T(8,128)(2,1)S(1)} collective-permute-done((bf16[4,128,256]{2,1,0:T(8,128)(2,1)S(1)}, bf16[4,128,256]{2,1,0:T(8,128)(2,1)S(1)}, u32[]{:S(2)}, u32[]{:S(2)}) %collective-permute-start.5) | collective-permute-done | bytes 262176 | tf_op jit(solution)/shard_map/ppermute | solution.py:356
  147.4 1.5 collective-permute-done.6.rest_2_
  149.0 0.0 all-to-all-done.4.h_ref
  149.0 0.0 copy-done.14
  149.0 0.0 copy-done.15
  149.0 0.7 copy-done.16
  149.7 2.8 %down.1 = bf16[8,320,256]{2,1,0:T(8,128)(2,1)S(1)} custom-call(bf16[4,640,128]{2,1,0:T(8,128)(2,1)S(1)} %all-to-all-done.4.h_ref, bf16[4,4,128,256]{3,2,1,0:T(8,128)(2,1)S(1)} %bitcast.28, bf16[4,128,256]{2,1,0:T(8,128)(2,1)} %copy-done.14, bf16[4,128,256]{2,1,0:T(8,128)(2,1)} %copy-done.15, bf16[4,128,256]{2,1,0:T(8,128)(2,1)} %copy-done.16), custom_call_target="tpu_custom_call" | custom-call | tf_op jit(solution)/shard_map/down/pallas_call | solution.py:301
  152.5 22.2 %all_to_all.37.p_ref = bf16[8,320,256]{2,1,0:T(8,128)(2,1)S(1)} all-to-all(bf16[8,320,256]{2,1,0:T(8,128)(2,1)S(1)} %down.1), channel_id=1, replica_groups=mesh['z'=16,'core'=2,'ty'=4,'tx'=4] {'core','tx'}, dimensions={0} | all-to-all | bytes 2621440 | tf_op jit(solution)/shard_map/all_to_all | solution.py:415
  174.7 0.4 shard_map.135
  175.1 27.3 %all_to_all.38 = bf16[16,40,256]{2,1,0:T(8,128)(2,1)S(1)} all-to-all(bf16[16,40,256]{2,1,0:T(8,128)(2,1)S(1)} %bitcast.32), channel_id=1, replica_groups=mesh['z'=16,'core'=2,'ty'=4,'tx'=4] {'z'}, dimensions={0} | all-to-all | bytes 655360 | tf_op jit(solution)/shard_map/all_to_all | solution.py:418
  202.4 0.0 copy-done.11
  202.4 1.2 shard_map.136
  (11 shorter events, 0.0 us)
Async XLA Ops:
  0.0 26.4 %copy-start.3 = (bf16[1024,256]{1,0:T(8,128)(2,1)S(1)}, bf16[1024,256]{1,0:T(8,128)(2,1)}, u32[]{:S(2)}) copy-start(bf16[1024,256]{1,0:T(8,128)(2,1)} %w_ref.1) | copy-start | bytes 1572868
  0.0 26.4 %copy-start.4 = (bf16[256,256]{1,0:T(8,128)(2,1)S(1)}, bf16[256,256]{1,0:T(8,128)(2,1)}, u32[]{:S(2)}) copy-start(bf16[256,256]{1,0:T(8,128)(2,1)} %res_ref.1) | copy-start | bytes 393220
  0.9 5.8 %collective-permute-start = (bf16[2,64]{0,1:T(8,128)(2,1)S(1)}, bf16[2,64]{0,1:T(8,128)(2,1)S(1)}, u32[]{:S(2)}, u32[]{:S(2)}) collective-permute-start(bf16[2,64]{0,1:T(8,128)(2,1)S(1)} %multiply_convert_fusion), channel_id=1, source_target_pairs={{0,16},{16,32},{32,48},{48,64},{64,80},{80,96},{96,112},{112,128},... | collective-permute-start | bytes 776 | tf_op jit(solution)/shard_map/ppermute | solution.py:386
  2.6 0.8 copy-start.5
  3.4 0.8 copy-start.6
  4.2 0.8 copy-start.7
  4.9 0.8 copy-start.8
  5.7 0.7 copy-start.10
  6.4 10.1 %copy-start.17 = (s32[256,2]{0,1:T(2,128)S(1)}, s32[256,2]{0,1:T(2,128)}, u32[]{:S(2)}) copy-start(s32[256,2]{0,1:T(2,128)} %param.21) | copy-start | bytes 6148
  7.7 18.7 %all-to-all-start = ((bf16[16,64,256]{2,1,0:T(8,128)(2,1)}), bf16[16,64,256]{2,1,0:T(8,128)(2,1)S(1)}, u32[]{:S(2)}, u32[]{:S(2)}) async-start(bf16[16,64,256]{2,1,0:T(8,128)(2,1)} %shard_map.128), calls=%async_computation | async-start | bytes 1048576 | tf_op jit(solution)/shard_map/all_to_all | solution.py:390
  63.4 3.7 %copy-start = (bf16[1,4096,128]{2,1,0:T(8,128)(2,1)S(1)}, bf16[1,4096,128]{2,1,0:T(8,128)(2,1)}, u32[]{:S(2)}) copy-start(bf16[1,4096,128]{2,1,0:T(8,128)(2,1)} %param.23) | copy-start | bytes 3145732
  63.4 3.7 %copy-start.1 = (bf16[1,4096,128]{2,1,0:T(8,128)(2,1)S(1)}, bf16[1,4096,128]{2,1,0:T(8,128)(2,1)}, u32[]{:S(2)}) copy-start(bf16[1,4096,128]{2,1,0:T(8,128)(2,1)} %param.24) | copy-start | bytes 3145732
  63.4 36.0 %all-to-all-start.2 = ((bf16[8,320,256]{2,1,0:T(8,128)(2,1)}), bf16[8,320,256]{2,1,0:T(8,128)(2,1)S(1)}, u32[]{:S(2)}, u32[]{:S(2)}) async-start(bf16[8,320,256]{2,1,0:T(8,128)(2,1)} %shard_map.131), calls=%async_computation.2 | async-start | bytes 2621440 | tf_op jit(solution)/shard_map/all_to_all | solution.py:410
  67.3 17.3 %collective-permute-start.1 = (bf16[1024,256]{1,0:T(8,128)(2,1)S(1)}, bf16[1024,256]{1,0:T(8,128)(2,1)S(1)}, u32[]{:S(2)}, u32[]{:S(2)}) collective-permute-start(bf16[1024,256]{1,0:T(8,128)(2,1)S(1)} %get-tuple-element.16), channel_id=1, source_target_pairs={{0,4},{4,8},{8,12},{12,0},{1,5},{5,9},{9,13},{13,1},{2,6},{6,10},{... | collective-permute-start | bytes 1572872 | tf_op jit(solution)/shard_map/ppermute | solution.py:356
  70.7 28.8 %copy-start.9 = (bf16[4096]{0:T(1024)(128)(2,1)S(1)}, bf16[4096]{0:T(1024)(128)(2,1)}, u32[]{:S(2)}) copy-start(bf16[4096]{0:T(1024)(128)(2,1)} %param.20) | copy-start | bytes 24580
  70.7 18.2 %collective-permute-start.2 = (bf16[1024,256]{1,0:T(8,128)(2,1)S(1)}, bf16[1024,256]{1,0:T(8,128)(2,1)S(1)}, u32[]{:S(2)}, u32[]{:S(2)}) collective-permute-start(bf16[1024,256]{1,0:T(8,128)(2,1)S(1)} %get-tuple-element.17), channel_id=1, source_target_pairs={{0,8},{4,12},{8,0},{12,4},{1,9},{5,13},{9,1},{13,5},{2,10},{6,14},... | collective-permute-start | bytes 1572872 | tf_op jit(solution)/shard_map/ppermute | solution.py:356
  76.0 23.4 %collective-permute-start.3 = (bf16[1024,256]{1,0:T(8,128)(2,1)S(1)}, bf16[1024,256]{1,0:T(8,128)(2,1)}, u32[]{:S(2)}, u32[]{:S(2)}) collective-permute-start(bf16[1024,256]{1,0:T(8,128)(2,1)S(1)} %shard_map.133), channel_id=1, source_target_pairs={{0,12},{4,0},{8,4},{12,8},{1,13},{5,1},{9,5},{13,9},{2,14},{6,2},{... | collective-permute-start | bytes 1572872 | tf_op jit(solution)/shard_map/ppermute | solution.py:356
  84.6 4.3 %copy-start.12 = (bf16[1024,256]{1,0:T(8,128)(2,1)}, bf16[1024,256]{1,0:T(8,128)(2,1)S(1)}, u32[]{:S(2)}) copy-start(bf16[1024,256]{1,0:T(8,128)(2,1)S(1)} %collective-permute-done.1.rest_0_) | copy-start | bytes 1572868
  88.9 0.8 copy-start.13
  124.9 6.1 %copy-start.2 = (bf16[1,2048,256]{2,1,0:T(8,128)(2,1)S(1)}, bf16[1,2048,256]{2,1,0:T(8,128)(2,1)}, u32[]{:S(2)}) copy-start(bf16[1,2048,256]{2,1,0:T(8,128)(2,1)} %param.25) | copy-start | bytes 3145732
  126.1 22.8 %all-to-all-start.4 = ((bf16[4,640,128]{2,1,0:T(8,128)(2,1)}), bf16[4,640,128]{2,1,0:T(8,128)(2,1)S(1)}, u32[]{:S(2)}, u32[]{:S(2)}) async-start(bf16[4,640,128]{2,1,0:T(8,128)(2,1)} %shard_map.134), calls=%async_computation.4 | async-start | bytes 1310720 | tf_op jit(solution)/shard_map/all_to_all | solution.py:414
  131.1 11.5 %collective-permute-start.4 = (bf16[4,128,256]{2,1,0:T(8,128)(2,1)S(1)}, bf16[4,128,256]{2,1,0:T(8,128)(2,1)S(1)}, u32[]{:S(2)}, u32[]{:S(2)}) collective-permute-start(bf16[4,128,256]{2,1,0:T(8,128)(2,1)S(1)} %get-tuple-element.21), channel_id=1, source_target_pairs={{0,1},{1,2},{2,3},{3,0},{4,5},{5,6},{6,7},{7,4},{8,9},{9,10},{10,1... | collective-permute-start | bytes 786440 | tf_op jit(solution)/shard_map/ppermute | solution.py:356
  134.6 12.8 %collective-permute-start.5 = (bf16[4,128,256]{2,1,0:T(8,128)(2,1)S(1)}, bf16[4,128,256]{2,1,0:T(8,128)(2,1)S(1)}, u32[]{:S(2)}, u32[]{:S(2)}) collective-permute-start(bf16[4,128,256]{2,1,0:T(8,128)(2,1)S(1)} %get-tuple-element.20), channel_id=1, source_target_pairs={{0,2},{1,3},{2,0},{3,1},{4,6},{5,7},{6,4},{7,5},{8,10},{9,11},{10,... | collective-permute-start | bytes 786440 | tf_op jit(solution)/shard_map/ppermute | solution.py:356
  139.2 9.7 %collective-permute-start.6 = (bf16[4,128,256]{2,1,0:T(8,128)(2,1)S(1)}, bf16[4,128,256]{2,1,0:T(8,128)(2,1)S(1)}, u32[]{:S(2)}, u32[]{:S(2)}) collective-permute-start(bf16[4,128,256]{2,1,0:T(8,128)(2,1)S(1)} %get-tuple-element.19), channel_id=1, source_target_pairs={{0,3},{1,0},{2,1},{3,2},{4,7},{5,4},{6,5},{7,6},{8,11},{9,8},{10,9... | collective-permute-start | bytes 786440 | tf_op jit(solution)/shard_map/ppermute | solution.py:356
  142.6 6.3 %copy-start.14 = (bf16[4,128,256]{2,1,0:T(8,128)(2,1)}, bf16[4,128,256]{2,1,0:T(8,128)(2,1)S(1)}, u32[]{:S(2)}) copy-start(bf16[4,128,256]{2,1,0:T(8,128)(2,1)S(1)} %collective-permute-done.4.rest_0_) | copy-start | bytes 786436
  147.4 1.6 copy-start.15
  148.9 0.7 copy-start.16
  174.7 27.7 %copy-start.11 = (f32[256,2]{0,1:T(2,128)S(1)}, f32[256,2]{0,1:T(2,128)}, u32[]{:S(2)}) copy-start(f32[256,2]{0,1:T(2,128)} %param.22) | copy-start | bytes 6148

commit v4 on v3

--- a/solution.py
+++ b/solution.py
@@ -88,7 +88,14 @@
     lane = docs.shape[1]
     per = toks // lane
 
-    def body(b_ref, c_ref, h_ref, docs_ref, taps_ref, total_ref, factor_ref, gate_ref):
+    def body(*refs):
+        given, (total_ref, factor_ref, gate_ref), held = refs[:5], refs[5:8], refs[8:13]
+        moves = [pltpu.make_async_copy(g, k, refs[13].at[i]) for i, (g, k) in enumerate(zip(given, held))]
+        for move in moves:
+            move.start()
+        for move in moves:
+            move.wait()
+        b_ref, c_ref, h_ref, docs_ref, taps_ref = held
         gate_ref[...] = b_ref[...].astype(F32)
         sp = lax.axis_index("z") * 2 + lax.axis_index("core")
         tp = lax.axis_index("ty") * lax.axis_size("tx") + lax.axis_index("tx")
@@ -116,7 +123,17 @@
         factor_ref[...] = jnp.where(place == 2, tap[2] * same2[:, 1:2], factor)
 
     outs = ((chans, toks), (chans, lane), (chans, toks))
-    return kernel(body, outs, b_gate, c_gate, h_in, docs, taps, dtype=F32)
+    args = (b_gate, c_gate, h_in, docs, taps)
+    vmem = pl.BlockSpec(memory_space=pltpu.VMEM)
+    return pl.pallas_call(
+        body,
+        out_shape=tuple(jax.ShapeDtypeStruct(o, F32) for o in outs),
+        in_specs=[pl.BlockSpec(memory_space=pltpu.HBM)] * len(args),
+        out_specs=(vmem,) * len(outs),
+        scratch_shapes=[*[pltpu.VMEM(a.shape, a.dtype) for a in args], pltpu.SemaphoreType.DMA((len(args),))],
+        compiler_params=pltpu.CompilerParams(vmem_limit_bytes=12 << 20),
+        name="convolve_head",
+    )(*[pltpu.with_memory_space_constraint(a, pltpu.HBM) for a in args])
 
 
 def convolve(total, factor, gate, edge, copies):
@@ -176,16 +193,33 @@
     dim, hid = w_gate.shape
     feats = dim // n_ty
 
-    def body(wg_ref, wu_ref, *out_refs):
+    def body(wg_ref, wu_ref, *rest):
+        out_refs, sems = rest[:-1], rest[-1]
         ty = lax.axis_index("ty")
-        for d, out_ref in zip(steps, out_refs):
+        moves = []
+        for k, d in enumerate(steps):
             to = lax.rem(ty + d, n_ty)
             rows = pl.ds(pl.multiple_of(to * feats, feats), feats)
-            out_ref[:, :hid] = wg_ref[rows, :]
-            out_ref[:, hid:] = wu_ref[rows, :]
-
-    outs = tuple((feats, 2 * hid) for d in steps)
-    return kernel(body, outs, w_gate, w_up)
+            for j, w_ref in enumerate((wg_ref, wu_ref)):
+                lanes = pl.ds(j * hid, hid)
+                moves.append(
+                    pltpu.make_async_copy(
+                        w_ref.at[rows, :], out_refs[k].at[:, lanes], sems.at[2 * k + j]
+                    )
+                )
+        for move in moves:
+            move.start()
+        for move in moves:
+            move.wait()
+
+    return pl.pallas_call(
+        body,
+        out_shape=tuple(jax.ShapeDtypeStruct((feats, 2 * hid), BF16) for d in steps),
+        in_specs=[pl.BlockSpec(memory_space=pltpu.HBM)] * 2,
+        out_specs=tuple(pl.BlockSpec(memory_space=pl.ANY) for d in steps),
+        scratch_shapes=[pltpu.SemaphoreType.DMA((2 * len(steps),))],
+        compiler_params=pltpu.CompilerParams(vmem_limit_bytes=12 << 20),
+    )(*[pltpu.with_memory_space_constraint(w, pltpu.HBM) for w in (w_gate, w_up)])
 
 
 def gate_up(x, gain, w_gate, w_up, pieces):
@@ -274,42 +308,24 @@
 
 
 def down(hidden, w_down, pieces):
-    n_ty, rows, hid = hidden.shape
+    n_ty, rows, _ = hidden.shape
     n_tx = len(pieces) + 1
     half = rows // 2
     width = w_down.shape[-1]
 
     def body(h_ref, wd_ref, *rest):
-        piece_refs, out_ref, held, sems = rest[: n_tx - 1], rest[-3], rest[-2], rest[-1]
-        moves = [
-            pltpu.make_async_copy(ref, held.at[d], sems.at[d]) for d, ref in enumerate(piece_refs)
-        ]
-        for move in moves:
-            move.start()
+        piece_refs, out_ref = rest[:-1], rest[-1]
         tx = lax.axis_index("tx")
         h = jnp.concatenate([h_ref[k] for k in range(n_ty)], axis=1)
         for d in range(n_tx):
-            if d:
-                moves[d - 1].wait()
-            w = [wd_ref[b, tx] if d == 0 else held[d - 1, b] for b in range(n_ty)]
+            w = [wd_ref[b, tx] if d == 0 else piece_refs[d - 1][b] for b in range(n_ty)]
             part = dot(h, jnp.concatenate(w, axis=0)).astype(BF16)
             to = lax.rem(tx + (n_tx - d), n_tx)
             out_ref[to] = part[:half]
             out_ref[n_tx + to] = part[half:]
 
-    vmem = pl.BlockSpec(memory_space=pltpu.VMEM)
-    return pl.pallas_call(
-        body,
-        out_shape=jax.ShapeDtypeStruct((2 * n_tx, half, width), BF16),
-        in_specs=[vmem] * 2 + [pl.BlockSpec(memory_space=pltpu.HBM)] * (n_tx - 1),
-        out_specs=vmem,
-        scratch_shapes=[
-            pltpu.VMEM((n_tx - 1, n_ty, hid, width), BF16),
-            pltpu.SemaphoreType.DMA((n_tx - 1,)),
-        ],
-        compiler_params=pltpu.CompilerParams(vmem_limit_bytes=24 << 20),
-        name="down",
-    )(hidden, w_down, *[pltpu.with_memory_space_constraint(p, pltpu.HBM) for p in pieces])
+    outs = ((2 * n_tx, half, width),)
+    return kernel(body, outs, hidden, w_down, *pieces, limit=24)
 
 
 def join_rows(parts, cap):
@@ -391,7 +407,7 @@
     conv_all = conv_all.reshape(n_tp * chans, toks)
 
     first = pack(w_gate[0], w_up[0], n_ty, (1, 2))
-    last = pack(w_gate[0], w_up[0], n_ty, (3,))
+    (last,) = pack(w_gate[0], w_up[0], n_ty, (3,))
     gate_up_pieces = [shifted(p, "ty", d + 1) for d, p in enumerate(first)]
     gate_up_pieces.append(shifted(last, "ty", 3))
     w_down4 = w_down[0].reshape(n_ty, n_tx, hid, width)

time: 205 us -> 200 us (0.976)
  local copies, waits for them, and re-layouts: 5.44 us -> 1.03 us
    unnamed x37 -> x21, local copies, waits for them, and re-layouts: 5.39 us -> 0.98 us
    pallas_call x10 -> x8, Pallas kernels: 6.89 us -> 7.17 us  [kernel(): pl.pallas_call(body, out_shape=tuple((jax.ShapeDtypeStruct(o, dtype) for...]
  transfers between devices with their start and end apart: 10 -> 10, of which waited for: 6 -> 6; matrix products, arithmetic and copies ran while one was open for 0% -> 0% of each run, Pallas kernels for 1% -> 2%
where the time goes in v4:
time: 200 us; the launch traced here: 199 us
  blocking collectives  107 us (54%)
  starting transfers between devices  41 us (20%)
  waiting for transfers between devices  35.2 us (18%)
  Pallas kernels  13.8 us (7%)
    all_to_all x1, blocking collectives, local(): lax.all_to_all(outgoing.reshape(n_z, 2 * cap, width), 'z', 0, 0, tiled=True)  35.3 us
    all_to_all x1, blocking collectives, local(): lax.all_to_all(join_rows(outs, cap).reshape(n_z, 2 * cap, width), 'z', 0,...  27.4 us
    ppermute x6, waiting for transfers between devices, shifted(): lax.ppermute(value, axis, [(i, (i + steps) % count) for i in range(count)])  25.8 us
    all_to_all x1, blocking collectives, local(): parts = lax.all_to_all(parts, 'ty', 0, 0, tiled=True)  22.3 us
    all_to_all x1, blocking collectives, local(): lax.all_to_all(down(hidden, w_down4, down_pieces), ('core', 'tx'), 0, 0,...  22.2 us
    ppermute x6, starting transfers between devices, shifted(): lax.ppermute(value, axis, [(i, (i + steps) % count) for i in range(count)])  22 us
    all_to_all x1, waiting for transfers between devices, local(): conv_all = lax.all_to_all(conv_copies, TP, 0, 0, tiled=True)  9.33 us
    all_to_all x1, starting transfers between devices, local(): conv_all = lax.all_to_all(conv_copies, TP, 0, 0, tiled=True)  8.72 us
  transfers between devices with their start and end apart: 10, of which 6 were waited for; matrix products, arithmetic and copies ran while one was open for 0% of the time, Pallas kernels for 2%

profile of v4, /device:TPU:8, one launch (start us, length us, event | category | flops | bytes accessed | tf_op | source)
XLA Modules:
  0.0 199.3 jit_solution(439513936643293991)
XLA Ops:
  0.0 0.0 copy-start.9
  0.0 0.0 copy-start.3
  0.0 0.0 copy-start.4
  0.0 0.9 multiply_convert_fusion
  0.9 1.7 collective-permute-start
  2.6 1.2 convolve_head.1
  3.8 0.0 collective-permute-done
  3.8 1.0 shard_map.127
  4.8 8.7 %all-to-all-start = ((bf16[16,64,256]{2,1,0:T(8,128)(2,1)}), bf16[16,64,256]{2,1,0:T(8,128)(2,1)S(1)}, u32[]{:S(2)}, u32[]{:S(2)}) async-start(bf16[16,64,256]{2,1,0:T(8,128)(2,1)} %shard_map.127), calls=%async_computation | async-start | bytes 1048576 | tf_op jit(solution)/shard_map/all_to_all | solution.py:406
  13.6 0.0 copy-done.9
  13.6 0.1 copy.17.pick_ref
  13.7 0.5 shard_map.128.slot_ref
  14.2 9.3 %all-to-all-done = bf16[16,64,256]{2,1,0:T(8,128)(2,1)S(1)} async-done(((bf16[16,64,256]{2,1,0:T(8,128)(2,1)}), bf16[16,64,256]{2,1,0:T(8,128)(2,1)S(1)}, u32[]{:S(2)}, u32[]{:S(2)}) %all-to-all-start) | async-done | bytes 524320 | tf_op jit(solution)/shard_map/all_to_all | solution.py:406
  23.6 0.0 copy-done.3
  23.6 0.0 copy-done.4
  23.6 0.7 shard_map.129
  24.3 35.3 %all_to_all.35 = bf16[16,40,256]{2,1,0:T(8,128)(2,1)S(1)} all-to-all(bf16[16,40,256]{2,1,0:T(8,128)(2,1)S(1)} %bitcast.33), channel_id=1, replica_groups=mesh['z'=16,'core'=2,'ty'=4,'tx'=4] {'z'}, dimensions={0} | all-to-all | bytes 655360 | tf_op jit(solution)/shard_map/all_to_all | solution.py:422
  59.6 1.3 shard_map.130
  60.9 3.6 %all-to-all-start.2 = ((bf16[8,320,256]{2,1,0:T(8,128)(2,1)}), bf16[8,320,256]{2,1,0:T(8,128)(2,1)S(1)}, u32[]{:S(2)}, u32[]{:S(2)}) async-start(bf16[8,320,256]{2,1,0:T(8,128)(2,1)} %shard_map.130), calls=%async_computation.2 | async-start | bytes 2621440 | tf_op jit(solution)/shard_map/all_to_all | solution.py:426
  64.5 1.2 shard_map.131
  65.7 3.1 %collective-permute-start.1 = (bf16[1024,256]{1,0:T(8,128)(2,1)S(1)}, bf16[1024,256]{1,0:T(8,128)(2,1)S(1)}, u32[]{:S(2)}, u32[]{:S(2)}) collective-permute-start(bf16[1024,256]{1,0:T(8,128)(2,1)S(1)} %get-tuple-element.16), channel_id=1, source_target_pairs={{0,4},{4,8},{8,12},{12,0},{1,5},{5,9},{9,13},{13,1},{2,6},{6,10},{... | collective-permute-start | bytes 1572872 | tf_op jit(solution)/shard_map/ppermute | solution.py:372
  68.8 0.0 copy-start
  68.8 0.0 copy-start.1
  68.8 0.0 copy-start.5
  68.9 5.3 %collective-permute-start.2 = (bf16[1024,256]{1,0:T(8,128)(2,1)S(1)}, bf16[1024,256]{1,0:T(8,128)(2,1)S(1)}, u32[]{:S(2)}, u32[]{:S(2)}) collective-permute-start(bf16[1024,256]{1,0:T(8,128)(2,1)S(1)} %get-tuple-element.17), channel_id=1, source_target_pairs={{0,8},{4,12},{8,0},{12,4},{1,9},{5,13},{9,1},{13,5},{2,10},{6,14},... | collective-permute-start | bytes 1572872 | tf_op jit(solution)/shard_map/ppermute | solution.py:372
  74.2 1.1 shard_map.132
  75.2 2.1 %collective-permute-start.3 = (bf16[1024,256]{1,0:T(8,128)(2,1)S(1)}, bf16[1024,256]{1,0:T(8,128)(2,1)}, u32[]{:S(2)}, u32[]{:S(2)}) collective-permute-start(bf16[1024,256]{1,0:T(8,128)(2,1)S(1)} %shard_map.132), channel_id=1, source_target_pairs={{0,12},{4,0},{8,4},{12,8},{1,13},{5,1},{9,5},{13,9},{2,14},{6,2},{... | collective-permute-start | bytes 1572872 | tf_op jit(solution)/shard_map/ppermute | solution.py:372
  77.4 5.4 %collective-permute-done.1.rest_0_ = bf16[1024,256]{1,0:T(8,128)(2,1)S(1)} collective-permute-done((bf16[1024,256]{1,0:T(8,128)(2,1)S(1)}, bf16[1024,256]{1,0:T(8,128)(2,1)S(1)}, u32[]{:S(2)}, u32[]{:S(2)}) %collective-permute-start.1) | collective-permute-done | bytes 524320 | tf_op jit(solution)/shard_map/ppermute | solution.py:372
  82.8 0.0 copy-start.7
  82.8 4.5 %collective-permute-done.2.rest_1_ = bf16[1024,256]{1,0:T(8,128)(2,1)S(1)} collective-permute-done((bf16[1024,256]{1,0:T(8,128)(2,1)S(1)}, bf16[1024,256]{1,0:T(8,128)(2,1)S(1)}, u32[]{:S(2)}, u32[]{:S(2)}) %collective-permute-start.2) | collective-permute-done | bytes 524320 | tf_op jit(solution)/shard_map/ppermute | solution.py:372
  87.2 0.0 copy-done.7
  87.2 0.0 copy-start.8
  87.2 0.8 copy-done.8
  88.0 9.7 %collective-permute-done.3.rest_2_ = bf16[1024,256]{1,0:T(8,128)(2,1)} collective-permute-done((bf16[1024,256]{1,0:T(8,128)(2,1)S(1)}, bf16[1024,256]{1,0:T(8,128)(2,1)}, u32[]{:S(2)}, u32[]{:S(2)}) %collective-permute-start.3) | collective-permute-done | bytes 524320 | tf_op jit(solution)/shard_map/ppermute | solution.py:372
  97.7 0.0 all-to-all-done.2.x_ref
  97.7 0.0 copy-done
  97.7 0.0 copy-done.1
  97.7 0.0 copy-done.5
  97.7 3.2 %gate_up.1 = bf16[4,648,256]{2,1,0:T(8,128)(2,1)S(1)} custom-call(bf16[8,320,256]{2,1,0:T(8,128)(2,1)S(1)} %all-to-all-done.2.x_ref, bf16[32,128]{1,0:T(8,128)(2,1)S(1)} %bitcast.35, bf16[4096,128]{1,0:T(8,128)(2,1)S(1)} %bitcast.23, bf16[4096,128]{1,0:T(8,128)(2,1)S(1)} %bitcast.26, bf16[1024,256]{1,0:T(8,128)(2,1)} %copy-done.7, ...), custom_call_target="tpu_custom_call" | custom-call | tf_op jit(solution)/shard_map/gate_up/pallas_call | solution.py:272
  100.9 22.3 %all_to_all.36.p_ref = bf16[4,648,256]{2,1,0:T(8,128)(2,1)S(1)} all-to-all(bf16[4,648,256]{2,1,0:T(8,128)(2,1)S(1)} %gate_up.1), channel_id=1, replica_groups=mesh['z'=16,'core'=2,'ty'=4,'tx'=4] {'ty'}, dimensions={0} | all-to-all | bytes 2654208 | tf_op jit(solution)/shard_map/all_to_all | solution.py:428
  123.2 0.0 copy-start.2
  123.2 1.2 shard_map.133
  124.4 4.9 %all-to-all-start.4 = ((bf16[4,640,128]{2,1,0:T(8,128)(2,1)}), bf16[4,640,128]{2,1,0:T(8,128)(2,1)S(1)}, u32[]{:S(2)}, u32[]{:S(2)}) async-start(bf16[4,640,128]{2,1,0:T(8,128)(2,1)} %shard_map.133), calls=%async_computation.4 | async-start | bytes 1310720 | tf_op jit(solution)/shard_map/all_to_all | solution.py:430
  129.3 0.0 copy-done.2
  129.3 0.1 dynamic-slice_bitcast_fusion
  129.4 3.5 %collective-permute-start.4 = (bf16[4,128,256]{2,1,0:T(8,128)(2,1)S(1)}, bf16[4,128,256]{2,1,0:T(8,128)(2,1)S(1)}, u32[]{:S(2)}, u32[]{:S(2)}) collective-permute-start(bf16[4,128,256]{2,1,0:T(8,128)(2,1)S(1)} %get-tuple-element.21), channel_id=1, source_target_pairs={{0,1},{1,2},{2,3},{3,0},{4,5},{5,6},{6,7},{7,4},{8,9},{9,10},{10,1... | collective-permute-start | bytes 786440 | tf_op jit(solution)/shard_map/ppermute | solution.py:372
  132.9 4.6 %collective-permute-start.5 = (bf16[4,128,256]{2,1,0:T(8,128)(2,1)S(1)}, bf16[4,128,256]{2,1,0:T(8,128)(2,1)S(1)}, u32[]{:S(2)}, u32[]{:S(2)}) collective-permute-start(bf16[4,128,256]{2,1,0:T(8,128)(2,1)S(1)} %get-tuple-element.20), channel_id=1, source_target_pairs={{0,2},{1,3},{2,0},{3,1},{4,6},{5,7},{6,4},{7,5},{8,10},{9,11},{10,... | collective-permute-start | bytes 786440 | tf_op jit(solution)/shard_map/ppermute | solution.py:372
  137.6 3.4 %collective-permute-start.6 = (bf16[4,128,256]{2,1,0:T(8,128)(2,1)S(1)}, bf16[4,128,256]{2,1,0:T(8,128)(2,1)S(1)}, u32[]{:S(2)}, u32[]{:S(2)}) collective-permute-start(bf16[4,128,256]{2,1,0:T(8,128)(2,1)S(1)} %get-tuple-element.19), channel_id=1, source_target_pairs={{0,3},{1,0},{2,1},{3,2},{4,7},{5,4},{6,5},{7,6},{8,11},{9,8},{10,9... | collective-permute-start | bytes 786440 | tf_op jit(solution)/shard_map/ppermute | solution.py:372
  140.9 0.0 collective-permute-done.4.rest_0_
  140.9 4.8 %collective-permute-done.5.rest_1_ = bf16[4,128,256]{2,1,0:T(8,128)(2,1)S(1)} collective-permute-done((bf16[4,128,256]{2,1,0:T(8,128)(2,1)S(1)}, bf16[4,128,256]{2,1,0:T(8,128)(2,1)S(1)}, u32[]{:S(2)}, u32[]{:S(2)}) %collective-permute-start.5) | collective-permute-done | bytes 262176 | tf_op jit(solution)/shard_map/ppermute | solution.py:372
  145.7 1.5 collective-permute-done.6.rest_2_
  147.3 0.0 all-to-all-done.4.h_ref
  147.3 0.9 shard_map.134
  148.1 22.2 %all_to_all.37.p_ref = bf16[8,320,256]{2,1,0:T(8,128)(2,1)S(1)} all-to-all(bf16[8,320,256]{2,1,0:T(8,128)(2,1)S(1)} %shard_map.134), channel_id=1, replica_groups=mesh['z'=16,'core'=2,'ty'=4,'tx'=4] {'core','tx'}, dimensions={0} | all-to-all | bytes 2621440 | tf_op jit(solution)/shard_map/all_to_all | solution.py:431
  170.3 0.0 copy-start.6
  170.3 0.4 shard_map.135
  170.7 27.4 %all_to_all.38 = bf16[16,40,256]{2,1,0:T(8,128)(2,1)S(1)} all-to-all(bf16[16,40,256]{2,1,0:T(8,128)(2,1)S(1)} %bitcast.32), channel_id=1, replica_groups=mesh['z'=16,'core'=2,'ty'=4,'tx'=4] {'z'}, dimensions={0} | all-to-all | bytes 655360 | tf_op jit(solution)/shard_map/all_to_all | solution.py:434
  198.1 0.0 copy-done.6
  198.1 1.2 shard_map.136
Async XLA Ops:
  0.0 13.6 %copy-start.9 = (s32[256,2]{0,1:T(2,128)S(1)}, s32[256,2]{0,1:T(2,128)}, u32[]{:S(2)}) copy-start(s32[256,2]{0,1:T(2,128)} %param.21) | copy-start | bytes 6148
  0.0 23.6 %copy-start.3 = (bf16[1024,256]{1,0:T(8,128)(2,1)S(1)}, bf16[1024,256]{1,0:T(8,128)(2,1)}, u32[]{:S(2)}) copy-start(bf16[1024,256]{1,0:T(8,128)(2,1)} %w_ref.1) | copy-start | bytes 1572868
  0.0 23.6 %copy-start.4 = (bf16[256,256]{1,0:T(8,128)(2,1)S(1)}, bf16[256,256]{1,0:T(8,128)(2,1)}, u32[]{:S(2)}) copy-start(bf16[256,256]{1,0:T(8,128)(2,1)} %res_ref.1) | copy-start | bytes 393220
  0.9 2.9 %collective-permute-start = (bf16[2,64]{0,1:T(8,128)(2,1)S(1)}, bf16[2,64]{0,1:T(8,128)(2,1)S(1)}, u32[]{:S(2)}, u32[]{:S(2)}) collective-permute-start(bf16[2,64]{0,1:T(8,128)(2,1)S(1)} %multiply_convert_fusion), channel_id=1, source_target_pairs={{0,16},{16,32},{32,48},{48,64},{64,80},{80,96},{96,112},{112,128},... | collective-permute-start | bytes 776 | tf_op jit(solution)/shard_map/ppermute | solution.py:402
  4.8 18.7 %all-to-all-start = ((bf16[16,64,256]{2,1,0:T(8,128)(2,1)}), bf16[16,64,256]{2,1,0:T(8,128)(2,1)S(1)}, u32[]{:S(2)}, u32[]{:S(2)}) async-start(bf16[16,64,256]{2,1,0:T(8,128)(2,1)} %shard_map.127), calls=%async_computation | async-start | bytes 1048576 | tf_op jit(solution)/shard_map/all_to_all | solution.py:406
  60.9 36.8 %all-to-all-start.2 = ((bf16[8,320,256]{2,1,0:T(8,128)(2,1)}), bf16[8,320,256]{2,1,0:T(8,128)(2,1)S(1)}, u32[]{:S(2)}, u32[]{:S(2)}) async-start(bf16[8,320,256]{2,1,0:T(8,128)(2,1)} %shard_map.130), calls=%async_computation.2 | async-start | bytes 2621440 | tf_op jit(solution)/shard_map/all_to_all | solution.py:426
  65.7 17.1 %collective-permute-start.1 = (bf16[1024,256]{1,0:T(8,128)(2,1)S(1)}, bf16[1024,256]{1,0:T(8,128)(2,1)S(1)}, u32[]{:S(2)}, u32[]{:S(2)}) collective-permute-start(bf16[1024,256]{1,0:T(8,128)(2,1)S(1)} %get-tuple-element.16), channel_id=1, source_target_pairs={{0,4},{4,8},{8,12},{12,0},{1,5},{5,9},{9,13},{13,1},{2,6},{6,10},{... | collective-permute-start | bytes 1572872 | tf_op jit(solution)/shard_map/ppermute | solution.py:372
  68.8 28.9 %copy-start = (bf16[1,4096,128]{2,1,0:T(8,128)(2,1)S(1)}, bf16[1,4096,128]{2,1,0:T(8,128)(2,1)}, u32[]{:S(2)}) copy-start(bf16[1,4096,128]{2,1,0:T(8,128)(2,1)} %param.23) | copy-start | bytes 3145732
  68.8 28.9 %copy-start.1 = (bf16[1,4096,128]{2,1,0:T(8,128)(2,1)S(1)}, bf16[1,4096,128]{2,1,0:T(8,128)(2,1)}, u32[]{:S(2)}) copy-start(bf16[1,4096,128]{2,1,0:T(8,128)(2,1)} %param.24) | copy-start | bytes 3145732
  68.8 28.9 %copy-start.5 = (bf16[4096]{0:T(1024)(128)(2,1)S(1)}, bf16[4096]{0:T(1024)(128)(2,1)}, u32[]{:S(2)}) copy-start(bf16[4096]{0:T(1024)(128)(2,1)} %param.20) | copy-start | bytes 24580
  68.9 18.4 %collective-permute-start.2 = (bf16[1024,256]{1,0:T(8,128)(2,1)S(1)}, bf16[1024,256]{1,0:T(8,128)(2,1)S(1)}, u32[]{:S(2)}, u32[]{:S(2)}) collective-permute-start(bf16[1024,256]{1,0:T(8,128)(2,1)S(1)} %get-tuple-element.17), channel_id=1, source_target_pairs={{0,8},{4,12},{8,0},{12,4},{1,9},{5,13},{9,1},{13,5},{2,10},{6,14},... | collective-permute-start | bytes 1572872 | tf_op jit(solution)/shard_map/ppermute | solution.py:372
  75.2 22.5 %collective-permute-start.3 = (bf16[1024,256]{1,0:T(8,128)(2,1)S(1)}, bf16[1024,256]{1,0:T(8,128)(2,1)}, u32[]{:S(2)}, u32[]{:S(2)}) collective-permute-start(bf16[1024,256]{1,0:T(8,128)(2,1)S(1)} %shard_map.132), channel_id=1, source_target_pairs={{0,12},{4,0},{8,4},{12,8},{1,13},{5,1},{9,5},{13,9},{2,14},{6,2},{... | collective-permute-start | bytes 1572872 | tf_op jit(solution)/shard_map/ppermute | solution.py:372
  82.8 4.5 %copy-start.7 = (bf16[1024,256]{1,0:T(8,128)(2,1)}, bf16[1024,256]{1,0:T(8,128)(2,1)S(1)}, u32[]{:S(2)}) copy-start(bf16[1024,256]{1,0:T(8,128)(2,1)S(1)} %collective-permute-done.1.rest_0_) | copy-start | bytes 1572868
  87.2 0.8 copy-start.8
  123.2 6.1 %copy-start.2 = (bf16[1,2048,256]{2,1,0:T(8,128)(2,1)S(1)}, bf16[1,2048,256]{2,1,0:T(8,128)(2,1)}, u32[]{:S(2)}) copy-start(bf16[1,2048,256]{2,1,0:T(8,128)(2,1)} %param.25) | copy-start | bytes 3145732
  124.4 22.8 %all-to-all-start.4 = ((bf16[4,640,128]{2,1,0:T(8,128)(2,1)}), bf16[4,640,128]{2,1,0:T(8,128)(2,1)S(1)}, u32[]{:S(2)}, u32[]{:S(2)}) async-start(bf16[4,640,128]{2,1,0:T(8,128)(2,1)} %shard_map.133), calls=%async_computation.4 | async-start | bytes 1310720 | tf_op jit(solution)/shard_map/all_to_all | solution.py:430
  129.4 11.5 %collective-permute-start.4 = (bf16[4,128,256]{2,1,0:T(8,128)(2,1)S(1)}, bf16[4,128,256]{2,1,0:T(8,128)(2,1)S(1)}, u32[]{:S(2)}, u32[]{:S(2)}) collective-permute-start(bf16[4,128,256]{2,1,0:T(8,128)(2,1)S(1)} %get-tuple-element.21), channel_id=1, source_target_pairs={{0,1},{1,2},{2,3},{3,0},{4,5},{5,6},{6,7},{7,4},{8,9},{9,10},{10,1... | collective-permute-start | bytes 786440 | tf_op jit(solution)/shard_map/ppermute | solution.py:372
  132.9 12.8 %collective-permute-start.5 = (bf16[4,128,256]{2,1,0:T(8,128)(2,1)S(1)}, bf16[4,128,256]{2,1,0:T(8,128)(2,1)S(1)}, u32[]{:S(2)}, u32[]{:S(2)}) collective-permute-start(bf16[4,128,256]{2,1,0:T(8,128)(2,1)S(1)} %get-tuple-element.20), channel_id=1, source_target_pairs={{0,2},{1,3},{2,0},{3,1},{4,6},{5,7},{6,4},{7,5},{8,10},{9,11},{10,... | collective-permute-start | bytes 786440 | tf_op jit(solution)/shard_map/ppermute | solution.py:372
  137.6 9.7 %collective-permute-start.6 = (bf16[4,128,256]{2,1,0:T(8,128)(2,1)S(1)}, bf16[4,128,256]{2,1,0:T(8,128)(2,1)S(1)}, u32[]{:S(2)}, u32[]{:S(2)}) collective-permute-start(bf16[4,128,256]{2,1,0:T(8,128)(2,1)S(1)} %get-tuple-element.19), channel_id=1, source_target_pairs={{0,3},{1,0},{2,1},{3,2},{4,7},{5,4},{6,5},{7,6},{8,11},{9,8},{10,9... | collective-permute-start | bytes 786440 | tf_op jit(solution)/shard_map/ppermute | solution.py:372
  170.3 27.7 %copy-start.6 = (f32[256,2]{0,1:T(2,128)S(1)}, f32[256,2]{0,1:T(2,128)}, u32[]{:S(2)}) copy-start(f32[256,2]{0,1:T(2,128)} %param.22) | copy-start | bytes 6148

commit v5 on v4

--- a/solution.py
+++ b/solution.py
@@ -216,7 +216,7 @@
         body,
         out_shape=tuple(jax.ShapeDtypeStruct((feats, 2 * hid), BF16) for d in steps),
         in_specs=[pl.BlockSpec(memory_space=pltpu.HBM)] * 2,
-        out_specs=tuple(pl.BlockSpec(memory_space=pl.ANY) for d in steps),
+        out_specs=tuple(pl.BlockSpec(memory_space=pltpu.VMEM) for d in steps),
         scratch_shapes=[pltpu.SemaphoreType.DMA((2 * len(steps),))],
         compiler_params=pltpu.CompilerParams(vmem_limit_bytes=12 << 20),
     )(*[pltpu.with_memory_space_constraint(w, pltpu.HBM) for w in (w_gate, w_up)])
@@ -255,8 +255,8 @@
                 extra = jnp.where(place == at, high, extra)
                 extra = jnp.where(place == at + 4, row - high, extra)
             keep = slice(core * half, (core + 1) * half)
-            out_ref[ty, keep, 0:hid] = dot(y, wg_ref[mine, :]).astype(BF16)
-            out_ref[ty, keep, hid : 2 * hid] = dot(y, wu_ref[mine, :]).astype(BF16)
+            own = jnp.concatenate([wg_ref[mine, :], wu_ref[mine, :]], axis=1)
+            out_ref[ty, keep, :] = dot(y, own).astype(BF16)
             scaled.append(y)
         for d in range(1, n_ty):
             to = lax.rem(ty + (n_ty - d), n_ty)

time: 200 us -> 200 us (level)
  no operation moved by 1% of the time
where the time goes in v5:
time: 200 us; the launch traced here: 199 us
  blocking collectives  107 us (54%)
  starting transfers between devices  41 us (20%)
  waiting for transfers between devices  35.2 us (18%)
  Pallas kernels  13.5 us (7%)
    all_to_all x1, blocking collectives, local(): lax.all_to_all(outgoing.reshape(n_z, 2 * cap, width), 'z', 0, 0, tiled=True)  35.3 us
    all_to_all x1, blocking collectives, local(): lax.all_to_all(join_rows(outs, cap).reshape(n_z, 2 * cap, width), 'z', 0,...  27.4 us
    ppermute x6, waiting for transfers between devices, shifted(): lax.ppermute(value, axis, [(i, (i + steps) % count) for i in range(count)])  25.8 us
    all_to_all x1, blocking collectives, local(): parts = lax.all_to_all(parts, 'ty', 0, 0, tiled=True)  22.3 us
    all_to_all x1, blocking collectives, local(): lax.all_to_all(down(hidden, w_down4, down_pieces), ('core', 'tx'), 0, 0,...  22.2 us
    ppermute x6, starting transfers between devices, shifted(): lax.ppermute(value, axis, [(i, (i + steps) % count) for i in range(count)])  22 us
    all_to_all x1, waiting for transfers between devices, local(): conv_all = lax.all_to_all(conv_copies, TP, 0, 0, tiled=True)  9.33 us
    all_to_all x1, starting transfers between devices, local(): conv_all = lax.all_to_all(conv_copies, TP, 0, 0, tiled=True)  8.72 us
  transfers between devices with their start and end apart: 10, of which 6 were waited for; matrix products, arithmetic and copies ran while one was open for 0% of the time, Pallas kernels for 2%

profile of v5, /device:TPU:8, one launch (start us, length us, event | category | flops | bytes accessed | tf_op | source)
XLA Modules:
  0.0 198.9 jit_solution(6273519156523935188)
XLA Ops:
  0.0 0.0 copy-start.9
  0.0 0.0 copy-start.3
  0.0 0.0 copy-start.4
  0.0 0.9 multiply_convert_fusion
  0.9 1.7 collective-permute-start
  2.6 1.2 convolve_head.1
  3.8 0.0 collective-permute-done
  3.8 1.0 shard_map.127
  4.8 8.7 %all-to-all-start = ((bf16[16,64,256]{2,1,0:T(8,128)(2,1)}), bf16[16,64,256]{2,1,0:T(8,128)(2,1)S(1)}, u32[]{:S(2)}, u32[]{:S(2)}) async-start(bf16[16,64,256]{2,1,0:T(8,128)(2,1)} %shard_map.127), calls=%async_computation | async-start | bytes 1048576 | tf_op jit(solution)/shard_map/all_to_all | solution.py:406
  13.6 0.0 copy-done.9
  13.6 0.1 copy.17.pick_ref
  13.7 0.5 shard_map.128.slot_ref
  14.2 9.3 %all-to-all-done = bf16[16,64,256]{2,1,0:T(8,128)(2,1)S(1)} async-done(((bf16[16,64,256]{2,1,0:T(8,128)(2,1)}), bf16[16,64,256]{2,1,0:T(8,128)(2,1)S(1)}, u32[]{:S(2)}, u32[]{:S(2)}) %all-to-all-start) | async-done | bytes 524320 | tf_op jit(solution)/shard_map/all_to_all | solution.py:406
  23.6 0.0 copy-done.3
  23.6 0.0 copy-done.4
  23.6 0.7 shard_map.129
  24.3 35.3 %all_to_all.35 = bf16[16,40,256]{2,1,0:T(8,128)(2,1)S(1)} all-to-all(bf16[16,40,256]{2,1,0:T(8,128)(2,1)S(1)} %bitcast.33), channel_id=1, replica_groups=mesh['z'=16,'core'=2,'ty'=4,'tx'=4] {'z'}, dimensions={0} | all-to-all | bytes 655360 | tf_op jit(solution)/shard_map/all_to_all | solution.py:422
  59.6 1.3 shard_map.130
  60.9 3.6 %all-to-all-start.2 = ((bf16[8,320,256]{2,1,0:T(8,128)(2,1)}), bf16[8,320,256]{2,1,0:T(8,128)(2,1)S(1)}, u32[]{:S(2)}, u32[]{:S(2)}) async-start(bf16[8,320,256]{2,1,0:T(8,128)(2,1)} %shard_map.130), calls=%async_computation.2 | async-start | bytes 2621440 | tf_op jit(solution)/shard_map/all_to_all | solution.py:426
  64.5 1.2 shard_map.131
  65.7 3.1 %collective-permute-start.1 = (bf16[1024,256]{1,0:T(8,128)(2,1)S(1)}, bf16[1024,256]{1,0:T(8,128)(2,1)S(1)}, u32[]{:S(2)}, u32[]{:S(2)}) collective-permute-start(bf16[1024,256]{1,0:T(8,128)(2,1)S(1)} %get-tuple-element.16), channel_id=1, source_target_pairs={{0,4},{4,8},{8,12},{12,0},{1,5},{5,9},{9,13},{13,1},{2,6},{6,10},{... | collective-permute-start | bytes 1572872 | tf_op jit(solution)/shard_map/ppermute | solution.py:372
  68.8 0.0 copy-start
  68.8 0.0 copy-start.1
  68.8 0.0 copy-start.5
  68.9 5.3 %collective-permute-start.2 = (bf16[1024,256]{1,0:T(8,128)(2,1)S(1)}, bf16[1024,256]{1,0:T(8,128)(2,1)S(1)}, u32[]{:S(2)}, u32[]{:S(2)}) collective-permute-start(bf16[1024,256]{1,0:T(8,128)(2,1)S(1)} %get-tuple-element.17), channel_id=1, source_target_pairs={{0,8},{4,12},{8,0},{12,4},{1,9},{5,13},{9,1},{13,5},{2,10},{6,14},... | collective-permute-start | bytes 1572872 | tf_op jit(solution)/shard_map/ppermute | solution.py:372
  74.2 1.1 shard_map.132
  75.2 2.1 %collective-permute-start.3 = (bf16[1024,256]{1,0:T(8,128)(2,1)S(1)}, bf16[1024,256]{1,0:T(8,128)(2,1)}, u32[]{:S(2)}, u32[]{:S(2)}) collective-permute-start(bf16[1024,256]{1,0:T(8,128)(2,1)S(1)} %shard_map.132), channel_id=1, source_target_pairs={{0,12},{4,0},{8,4},{12,8},{1,13},{5,1},{9,5},{13,9},{2,14},{6,2},{... | collective-permute-start | bytes 1572872 | tf_op jit(solution)/shard_map/ppermute | solution.py:372
  77.4 5.4 %collective-permute-done.1.rest_0_ = bf16[1024,256]{1,0:T(8,128)(2,1)S(1)} collective-permute-done((bf16[1024,256]{1,0:T(8,128)(2,1)S(1)}, bf16[1024,256]{1,0:T(8,128)(2,1)S(1)}, u32[]{:S(2)}, u32[]{:S(2)}) %collective-permute-start.1) | collective-permute-done | bytes 524320 | tf_op jit(solution)/shard_map/ppermute | solution.py:372
  82.8 0.0 copy-start.7
  82.8 4.5 %collective-permute-done.2.rest_1_ = bf16[1024,256]{1,0:T(8,128)(2,1)S(1)} collective-permute-done((bf16[1024,256]{1,0:T(8,128)(2,1)S(1)}, bf16[1024,256]{1,0:T(8,128)(2,1)S(1)}, u32[]{:S(2)}, u32[]{:S(2)}) %collective-permute-start.2) | collective-permute-done | bytes 524320 | tf_op jit(solution)/shard_map/ppermute | solution.py:372
  87.2 0.0 copy-done.7
  87.2 0.0 copy-start.8
  87.2 0.8 copy-done.8
  88.0 9.7 %collective-permute-done.3.rest_2_ = bf16[1024,256]{1,0:T(8,128)(2,1)} collective-permute-done((bf16[1024,256]{1,0:T(8,128)(2,1)S(1)}, bf16[1024,256]{1,0:T(8,128)(2,1)}, u32[]{:S(2)}, u32[]{:S(2)}) %collective-permute-start.3) | collective-permute-done | bytes 524320 | tf_op jit(solution)/shard_map/ppermute | solution.py:372
  97.7 0.0 all-to-all-done.2.x_ref
  97.7 0.0 copy-done
  97.7 0.0 copy-done.1
  97.7 0.0 copy-done.5
  97.7 2.9 %gate_up.1 = bf16[4,648,256]{2,1,0:T(8,128)(2,1)S(1)} custom-call(bf16[8,320,256]{2,1,0:T(8,128)(2,1)S(1)} %all-to-all-done.2.x_ref, bf16[32,128]{1,0:T(8,128)(2,1)S(1)} %bitcast.35, bf16[4096,128]{1,0:T(8,128)(2,1)S(1)} %bitcast.23, bf16[4096,128]{1,0:T(8,128)(2,1)S(1)} %bitcast.26, bf16[1024,256]{1,0:T(8,128)(2,1)} %copy-done.7, ...), custom_call_target="tpu_custom_call" | custom-call | tf_op jit(solution)/shard_map/gate_up/pallas_call | solution.py:272
  100.6 22.3 %all_to_all.36.p_ref = bf16[4,648,256]{2,1,0:T(8,128)(2,1)S(1)} all-to-all(bf16[4,648,256]{2,1,0:T(8,128)(2,1)S(1)} %gate_up.1), channel_id=1, replica_groups=mesh['z'=16,'core'=2,'ty'=4,'tx'=4] {'ty'}, dimensions={0} | all-to-all | bytes 2654208 | tf_op jit(solution)/shard_map/all_to_all | solution.py:428
  122.9 0.0 copy-start.2
  122.9 1.2 shard_map.133
  124.1 4.9 %all-to-all-start.4 = ((bf16[4,640,128]{2,1,0:T(8,128)(2,1)}), bf16[4,640,128]{2,1,0:T(8,128)(2,1)S(1)}, u32[]{:S(2)}, u32[]{:S(2)}) async-start(bf16[4,640,128]{2,1,0:T(8,128)(2,1)} %shard_map.133), calls=%async_computation.4 | async-start | bytes 1310720 | tf_op jit(solution)/shard_map/all_to_all | solution.py:430
  129.0 0.0 copy-done.2
  129.0 0.1 dynamic-slice_bitcast_fusion
  129.1 3.5 %collective-permute-start.4 = (bf16[4,128,256]{2,1,0:T(8,128)(2,1)S(1)}, bf16[4,128,256]{2,1,0:T(8,128)(2,1)S(1)}, u32[]{:S(2)}, u32[]{:S(2)}) collective-permute-start(bf16[4,128,256]{2,1,0:T(8,128)(2,1)S(1)} %get-tuple-element.21), channel_id=1, source_target_pairs={{0,1},{1,2},{2,3},{3,0},{4,5},{5,6},{6,7},{7,4},{8,9},{9,10},{10,1... | collective-permute-start | bytes 786440 | tf_op jit(solution)/shard_map/ppermute | solution.py:372
  132.6 4.6 %collective-permute-start.5 = (bf16[4,128,256]{2,1,0:T(8,128)(2,1)S(1)}, bf16[4,128,256]{2,1,0:T(8,128)(2,1)S(1)}, u32[]{:S(2)}, u32[]{:S(2)}) collective-permute-start(bf16[4,128,256]{2,1,0:T(8,128)(2,1)S(1)} %get-tuple-element.20), channel_id=1, source_target_pairs={{0,2},{1,3},{2,0},{3,1},{4,6},{5,7},{6,4},{7,5},{8,10},{9,11},{10,... | collective-permute-start | bytes 786440 | tf_op jit(solution)/shard_map/ppermute | solution.py:372
  137.2 3.4 %collective-permute-start.6 = (bf16[4,128,256]{2,1,0:T(8,128)(2,1)S(1)}, bf16[4,128,256]{2,1,0:T(8,128)(2,1)S(1)}, u32[]{:S(2)}, u32[]{:S(2)}) collective-permute-start(bf16[4,128,256]{2,1,0:T(8,128)(2,1)S(1)} %get-tuple-element.19), channel_id=1, source_target_pairs={{0,3},{1,0},{2,1},{3,2},{4,7},{5,4},{6,5},{7,6},{8,11},{9,8},{10,9... | collective-permute-start | bytes 786440 | tf_op jit(solution)/shard_map/ppermute | solution.py:372
  140.6 0.0 collective-permute-done.4.rest_0_
  140.6 4.8 %collective-permute-done.5.rest_1_ = bf16[4,128,256]{2,1,0:T(8,128)(2,1)S(1)} collective-permute-done((bf16[4,128,256]{2,1,0:T(8,128)(2,1)S(1)}, bf16[4,128,256]{2,1,0:T(8,128)(2,1)S(1)}, u32[]{:S(2)}, u32[]{:S(2)}) %collective-permute-start.5) | collective-permute-done | bytes 262176 | tf_op jit(solution)/shard_map/ppermute | solution.py:372
  145.4 1.5 collective-permute-done.6.rest_2_
  146.9 0.0 all-to-all-done.4.h_ref
  147.0 0.8 shard_map.134
  147.8 22.2 %all_to_all.37.p_ref = bf16[8,320,256]{2,1,0:T(8,128)(2,1)S(1)} all-to-all(bf16[8,320,256]{2,1,0:T(8,128)(2,1)S(1)} %shard_map.134), channel_id=1, replica_groups=mesh['z'=16,'core'=2,'ty'=4,'tx'=4] {'core','tx'}, dimensions={0} | all-to-all | bytes 2621440 | tf_op jit(solution)/shard_map/all_to_all | solution.py:431
  170.0 0.0 copy-start.6
  170.0 0.4 shard_map.135
  170.4 27.4 %all_to_all.38 = bf16[16,40,256]{2,1,0:T(8,128)(2,1)S(1)} all-to-all(bf16[16,40,256]{2,1,0:T(8,128)(2,1)S(1)} %bitcast.32), channel_id=1, replica_groups=mesh['z'=16,'core'=2,'ty'=4,'tx'=4] {'z'}, dimensions={0} | all-to-all | bytes 655360 | tf_op jit(solution)/shard_map/all_to_all | solution.py:434
  197.8 0.0 copy-done.6
  197.8 1.2 shard_map.136
Async XLA Ops:
  0.0 13.6 %copy-start.9 = (s32[256,2]{0,1:T(2,128)S(1)}, s32[256,2]{0,1:T(2,128)}, u32[]{:S(2)}) copy-start(s32[256,2]{0,1:T(2,128)} %param.21) | copy-start | bytes 6148
  0.0 23.6 %copy-start.3 = (bf16[1024,256]{1,0:T(8,128)(2,1)S(1)}, bf16[1024,256]{1,0:T(8,128)(2,1)}, u32[]{:S(2)}) copy-start(bf16[1024,256]{1,0:T(8,128)(2,1)} %w_ref.1) | copy-start | bytes 1572868
  0.0 23.6 %copy-start.4 = (bf16[256,256]{1,0:T(8,128)(2,1)S(1)}, bf16[256,256]{1,0:T(8,128)(2,1)}, u32[]{:S(2)}) copy-start(bf16[256,256]{1,0:T(8,128)(2,1)} %res_ref.1) | copy-start | bytes 393220
  0.9 2.9 %collective-permute-start = (bf16[2,64]{0,1:T(8,128)(2,1)S(1)}, bf16[2,64]{0,1:T(8,128)(2,1)S(1)}, u32[]{:S(2)}, u32[]{:S(2)}) collective-permute-start(bf16[2,64]{0,1:T(8,128)(2,1)S(1)} %multiply_convert_fusion), channel_id=1, source_target_pairs={{0,16},{16,32},{32,48},{48,64},{64,80},{80,96},{96,112},{112,128},... | collective-permute-start | bytes 776 | tf_op jit(solution)/shard_map/ppermute | solution.py:402
  4.8 18.7 %all-to-all-start = ((bf16[16,64,256]{2,1,0:T(8,128)(2,1)}), bf16[16,64,256]{2,1,0:T(8,128)(2,1)S(1)}, u32[]{:S(2)}, u32[]{:S(2)}) async-start(bf16[16,64,256]{2,1,0:T(8,128)(2,1)} %shard_map.127), calls=%async_computation | async-start | bytes 1048576 | tf_op jit(solution)/shard_map/all_to_all | solution.py:406
  60.9 36.8 %all-to-all-start.2 = ((bf16[8,320,256]{2,1,0:T(8,128)(2,1)}), bf16[8,320,256]{2,1,0:T(8,128)(2,1)S(1)}, u32[]{:S(2)}, u32[]{:S(2)}) async-start(bf16[8,320,256]{2,1,0:T(8,128)(2,1)} %shard_map.130), calls=%async_computation.2 | async-start | bytes 2621440 | tf_op jit(solution)/shard_map/all_to_all | solution.py:426
  65.7 17.1 %collective-permute-start.1 = (bf16[1024,256]{1,0:T(8,128)(2,1)S(1)}, bf16[1024,256]{1,0:T(8,128)(2,1)S(1)}, u32[]{:S(2)}, u32[]{:S(2)}) collective-permute-start(bf16[1024,256]{1,0:T(8,128)(2,1)S(1)} %get-tuple-element.16), channel_id=1, source_target_pairs={{0,4},{4,8},{8,12},{12,0},{1,5},{5,9},{9,13},{13,1},{2,6},{6,10},{... | collective-permute-start | bytes 1572872 | tf_op jit(solution)/shard_map/ppermute | solution.py:372
  68.8 28.9 %copy-start = (bf16[1,4096,128]{2,1,0:T(8,128)(2,1)S(1)}, bf16[1,4096,128]{2,1,0:T(8,128)(2,1)}, u32[]{:S(2)}) copy-start(bf16[1,4096,128]{2,1,0:T(8,128)(2,1)} %param.23) | copy-start | bytes 3145732
  68.8 28.9 %copy-start.1 = (bf16[1,4096,128]{2,1,0:T(8,128)(2,1)S(1)}, bf16[1,4096,128]{2,1,0:T(8,128)(2,1)}, u32[]{:S(2)}) copy-start(bf16[1,4096,128]{2,1,0:T(8,128)(2,1)} %param.24) | copy-start | bytes 3145732
  68.8 28.9 %copy-start.5 = (bf16[4096]{0:T(1024)(128)(2,1)S(1)}, bf16[4096]{0:T(1024)(128)(2,1)}, u32[]{:S(2)}) copy-start(bf16[4096]{0:T(1024)(128)(2,1)} %param.20) | copy-start | bytes 24580
  68.9 18.4 %collective-permute-start.2 = (bf16[1024,256]{1,0:T(8,128)(2,1)S(1)}, bf16[1024,256]{1,0:T(8,128)(2,1)S(1)}, u32[]{:S(2)}, u32[]{:S(2)}) collective-permute-start(bf16[1024,256]{1,0:T(8,128)(2,1)S(1)} %get-tuple-element.17), channel_id=1, source_target_pairs={{0,8},{4,12},{8,0},{12,4},{1,9},{5,13},{9,1},{13,5},{2,10},{6,14},... | collective-permute-start | bytes 1572872 | tf_op jit(solution)/shard_map/ppermute | solution.py:372
  75.2 22.5 %collective-permute-start.3 = (bf16[1024,256]{1,0:T(8,128)(2,1)S(1)}, bf16[1024,256]{1,0:T(8,128)(2,1)}, u32[]{:S(2)}, u32[]{:S(2)}) collective-permute-start(bf16[1024,256]{1,0:T(8,128)(2,1)S(1)} %shard_map.132), channel_id=1, source_target_pairs={{0,12},{4,0},{8,4},{12,8},{1,13},{5,1},{9,5},{13,9},{2,14},{6,2},{... | collective-permute-start | bytes 1572872 | tf_op jit(solution)/shard_map/ppermute | solution.py:372
  82.8 4.5 %copy-start.7 = (bf16[1024,256]{1,0:T(8,128)(2,1)}, bf16[1024,256]{1,0:T(8,128)(2,1)S(1)}, u32[]{:S(2)}) copy-start(bf16[1024,256]{1,0:T(8,128)(2,1)S(1)} %collective-permute-done.1.rest_0_) | copy-start | bytes 1572868
  87.2 0.8 copy-start.8
  122.9 6.1 %copy-start.2 = (bf16[1,2048,256]{2,1,0:T(8,128)(2,1)S(1)}, bf16[1,2048,256]{2,1,0:T(8,128)(2,1)}, u32[]{:S(2)}) copy-start(bf16[1,2048,256]{2,1,0:T(8,128)(2,1)} %param.25) | copy-start | bytes 3145732
  124.1 22.8 %all-to-all-start.4 = ((bf16[4,640,128]{2,1,0:T(8,128)(2,1)}), bf16[4,640,128]{2,1,0:T(8,128)(2,1)S(1)}, u32[]{:S(2)}, u32[]{:S(2)}) async-start(bf16[4,640,128]{2,1,0:T(8,128)(2,1)} %shard_map.133), calls=%async_computation.4 | async-start | bytes 1310720 | tf_op jit(solution)/shard_map/all_to_all | solution.py:430
  129.1 11.5 %collective-permute-start.4 = (bf16[4,128,256]{2,1,0:T(8,128)(2,1)S(1)}, bf16[4,128,256]{2,1,0:T(8,128)(2,1)S(1)}, u32[]{:S(2)}, u32[]{:S(2)}) collective-permute-start(bf16[4,128,256]{2,1,0:T(8,128)(2,1)S(1)} %get-tuple-element.21), channel_id=1, source_target_pairs={{0,1},{1,2},{2,3},{3,0},{4,5},{5,6},{6,7},{7,4},{8,9},{9,10},{10,1... | collective-permute-start | bytes 786440 | tf_op jit(solution)/shard_map/ppermute | solution.py:372
  132.6 12.8 %collective-permute-start.5 = (bf16[4,128,256]{2,1,0:T(8,128)(2,1)S(1)}, bf16[4,128,256]{2,1,0:T(8,128)(2,1)S(1)}, u32[]{:S(2)}, u32[]{:S(2)}) collective-permute-start(bf16[4,128,256]{2,1,0:T(8,128)(2,1)S(1)} %get-tuple-element.20), channel_id=1, source_target_pairs={{0,2},{1,3},{2,0},{3,1},{4,6},{5,7},{6,4},{7,5},{8,10},{9,11},{10,... | collective-permute-start | bytes 786440 | tf_op jit(solution)/shard_map/ppermute | solution.py:372
  137.2 9.7 %collective-permute-start.6 = (bf16[4,128,256]{2,1,0:T(8,128)(2,1)S(1)}, bf16[4,128,256]{2,1,0:T(8,128)(2,1)S(1)}, u32[]{:S(2)}, u32[]{:S(2)}) collective-permute-start(bf16[4,128,256]{2,1,0:T(8,128)(2,1)S(1)} %get-tuple-element.19), channel_id=1, source_target_pairs={{0,3},{1,0},{2,1},{3,2},{4,7},{5,4},{6,5},{7,6},{8,11},{9,8},{10,9... | collective-permute-start | bytes 786440 | tf_op jit(solution)/shard_map/ppermute | solution.py:372
  170.0 27.8 %copy-start.6 = (f32[256,2]{0,1:T(2,128)S(1)}, f32[256,2]{0,1:T(2,128)}, u32[]{:S(2)}) copy-start(f32[256,2]{0,1:T(2,128)} %param.22) | copy-start | bytes 6148

commit v6 on v5

--- a/solution.py
+++ b/solution.py
@@ -328,6 +328,29 @@
     return kernel(body, outs, hidden, w_down, *pieces, limit=24)
 
 
+def stage(pieces):
+    count = len(pieces)
+
+    def body(*refs):
+        moves = [
+            pltpu.make_async_copy(refs[d], refs[count + d], refs[-1].at[d]) for d in range(count)
+        ]
+        for move in moves:
+            move.start()
+        for move in moves:
+            move.wait()
+
+    return pl.pallas_call(
+        body,
+        out_shape=tuple(jax.ShapeDtypeStruct(p.shape, p.dtype) for p in pieces),
+        in_specs=[pl.BlockSpec(memory_space=pltpu.HBM)] * count,
+        out_specs=tuple(pl.BlockSpec(memory_space=pltpu.VMEM) for p in pieces),
+        scratch_shapes=[pltpu.SemaphoreType.DMA((count,))],
+        compiler_params=pltpu.CompilerParams(vmem_limit_bytes=12 << 20),
+        name="stage",
+    )(*[pltpu.with_memory_space_constraint(p, pltpu.HBM) for p in pieces])
+
+
 def join_rows(parts, cap):
     groups, half, width = parts.shape
     n_tx = groups // 2
@@ -429,7 +452,7 @@
     hidden = activate(parts, full_dim)
     hidden = lax.all_to_all(hidden, "ty", 0, 0, tiled=True)
     outs = lax.all_to_all(
-        down(hidden, w_down4, down_pieces), ("core", "tx"), 0, 0, tiled=True
+        down(hidden, w_down4, stage(down_pieces)), ("core", "tx"), 0, 0, tiled=True
     )
     back = lax.all_to_all(
         join_rows(outs, cap).reshape(n_z, 2 * cap, width), "z", 0, 0, tiled=True

time: 200 us -> 202 us (1.010)
  transfers between devices with their start and end apart: 10 -> 10, of which waited for: 6 -> 6; matrix products, arithmetic and copies ran while one was open for 0% -> 0% of each run, Pallas kernels for 2% -> 3%
where the time goes in v6:
time: 202 us; the launch traced here: 201 us
  blocking collectives  107 us (53%)
  starting transfers between devices  41 us (20%)
  waiting for transfers between devices  35.2 us (17%)
  Pallas kernels  14.7 us (7%)
    all_to_all x1, blocking collectives, local(): lax.all_to_all(outgoing.reshape(n_z, 2 * cap, width), 'z', 0, 0, tiled=True)  35.3 us
    all_to_all x1, blocking collectives, local(): lax.all_to_all(join_rows(outs, cap).reshape(n_z, 2 * cap, width), 'z', 0,...  27.4 us
    ppermute x6, waiting for transfers between devices, shifted(): lax.ppermute(value, axis, [(i, (i + steps) % count) for i in range(count)])  25.8 us
    all_to_all x1, blocking collectives, local(): parts = lax.all_to_all(parts, 'ty', 0, 0, tiled=True)  22.3 us
    all_to_all x1, blocking collectives, local(): lax.all_to_all(down(hidden, w_down4, stage(down_pieces)), ('core', 'tx'),...  22.2 us
    ppermute x6, starting transfers between devices, shifted(): lax.ppermute(value, axis, [(i, (i + steps) % count) for i in range(count)])  22 us
    all_to_all x1, waiting for transfers between devices, local(): conv_all = lax.all_to_all(conv_copies, TP, 0, 0, tiled=True)  9.33 us
    all_to_all x1, starting transfers between devices, local(): conv_all = lax.all_to_all(conv_copies, TP, 0, 0, tiled=True)  8.72 us
  transfers between devices with their start and end apart: 10, of which 6 were waited for; matrix products, arithmetic and copies ran while one was open for 0% of the time, Pallas kernels for 3%

profile of v6, /device:TPU:8, one launch (start us, length us, event | category | flops | bytes accessed | tf_op | source)
XLA Modules:
  0.0 200.8 jit_solution(3484988680011358782)
XLA Ops:
  0.0 0.0 copy-start.12
  0.0 0.0 copy-start.3
  0.0 0.9 multiply_convert_fusion
  0.9 1.7 collective-permute-start
  2.6 1.2 convolve_head.1
  3.8 0.0 collective-permute-done
  3.8 1.0 shard_map.127
  4.9 8.7 %all-to-all-start = ((bf16[16,64,256]{2,1,0:T(8,128)(2,1)}), bf16[16,64,256]{2,1,0:T(8,128)(2,1)S(1)}, u32[]{:S(2)}, u32[]{:S(2)}) async-start(bf16[16,64,256]{2,1,0:T(8,128)(2,1)} %shard_map.127), calls=%async_computation | async-start | bytes 1048576 | tf_op jit(solution)/shard_map/all_to_all | solution.py:429
  13.6 0.0 copy-done.12
  13.6 0.1 copy.17.pick_ref
  13.7 0.5 shard_map.128.slot_ref
  14.3 9.3 %all-to-all-done = bf16[16,64,256]{2,1,0:T(8,128)(2,1)S(1)} async-done(((bf16[16,64,256]{2,1,0:T(8,128)(2,1)}), bf16[16,64,256]{2,1,0:T(8,128)(2,1)S(1)}, u32[]{:S(2)}, u32[]{:S(2)}) %all-to-all-start) | async-done | bytes 524320 | tf_op jit(solution)/shard_map/all_to_all | solution.py:429
  23.6 0.0 copy-done.3
  23.6 0.0 copy-done.4
  23.6 0.7 shard_map.129
  24.3 35.3 %all_to_all.35 = bf16[16,40,256]{2,1,0:T(8,128)(2,1)S(1)} all-to-all(bf16[16,40,256]{2,1,0:T(8,128)(2,1)S(1)} %bitcast.33), channel_id=1, replica_groups=mesh['z'=16,'core'=2,'ty'=4,'tx'=4] {'z'}, dimensions={0} | all-to-all | bytes 655360 | tf_op jit(solution)/shard_map/all_to_all | solution.py:445
  59.6 1.3 shard_map.130
  60.9 3.6 %all-to-all-start.2 = ((bf16[8,320,256]{2,1,0:T(8,128)(2,1)}), bf16[8,320,256]{2,1,0:T(8,128)(2,1)S(1)}, u32[]{:S(2)}, u32[]{:S(2)}) async-start(bf16[8,320,256]{2,1,0:T(8,128)(2,1)} %shard_map.130), calls=%async_computation.2 | async-start | bytes 2621440 | tf_op jit(solution)/shard_map/all_to_all | solution.py:449
  64.5 1.2 shard_map.131
  65.7 3.1 %collective-permute-start.1 = (bf16[1024,256]{1,0:T(8,128)(2,1)S(1)}, bf16[1024,256]{1,0:T(8,128)(2,1)S(1)}, u32[]{:S(2)}, u32[]{:S(2)}) collective-permute-start(bf16[1024,256]{1,0:T(8,128)(2,1)S(1)} %get-tuple-element.19), channel_id=1, source_target_pairs={{0,4},{4,8},{8,12},{12,0},{1,5},{5,9},{9,13},{13,1},{2,6},{6,10},{... | collective-permute-start | bytes 1572872 | tf_op jit(solution)/shard_map/ppermute | solution.py:395
  68.9 0.0 copy-start
  68.9 0.0 copy-start.1
  68.9 0.0 copy-start.5
  68.9 5.3 %collective-permute-start.2 = (bf16[1024,256]{1,0:T(8,128)(2,1)S(1)}, bf16[1024,256]{1,0:T(8,128)(2,1)S(1)}, u32[]{:S(2)}, u32[]{:S(2)}) collective-permute-start(bf16[1024,256]{1,0:T(8,128)(2,1)S(1)} %get-tuple-element.20), channel_id=1, source_target_pairs={{0,8},{4,12},{8,0},{12,4},{1,9},{5,13},{9,1},{13,5},{2,10},{6,14},... | collective-permute-start | bytes 1572872 | tf_op jit(solution)/shard_map/ppermute | solution.py:395
  74.2 1.1 shard_map.132
  75.3 2.1 %collective-permute-start.3 = (bf16[1024,256]{1,0:T(8,128)(2,1)S(1)}, bf16[1024,256]{1,0:T(8,128)(2,1)}, u32[]{:S(2)}, u32[]{:S(2)}) collective-permute-start(bf16[1024,256]{1,0:T(8,128)(2,1)S(1)} %shard_map.132), channel_id=1, source_target_pairs={{0,12},{4,0},{8,4},{12,8},{1,13},{5,1},{9,5},{13,9},{2,14},{6,2},{... | collective-permute-start | bytes 1572872 | tf_op jit(solution)/shard_map/ppermute | solution.py:395
  77.4 5.4 %collective-permute-done.1.rest_0_ = bf16[1024,256]{1,0:T(8,128)(2,1)S(1)} collective-permute-done((bf16[1024,256]{1,0:T(8,128)(2,1)S(1)}, bf16[1024,256]{1,0:T(8,128)(2,1)S(1)}, u32[]{:S(2)}, u32[]{:S(2)}) %collective-permute-start.1) | collective-permute-done | bytes 524320 | tf_op jit(solution)/shard_map/ppermute | solution.py:395
  82.8 0.0 copy-start.7
  82.8 4.5 %collective-permute-done.2.rest_1_ = bf16[1024,256]{1,0:T(8,128)(2,1)S(1)} collective-permute-done((bf16[1024,256]{1,0:T(8,128)(2,1)S(1)}, bf16[1024,256]{1,0:T(8,128)(2,1)S(1)}, u32[]{:S(2)}, u32[]{:S(2)}) %collective-permute-start.2) | collective-permute-done | bytes 524320 | tf_op jit(solution)/shard_map/ppermute | solution.py:395
  87.3 0.0 copy-done.7
  87.3 0.0 copy-start.8
  87.3 0.8 copy-done.8
  88.1 9.7 %collective-permute-done.3.rest_2_ = bf16[1024,256]{1,0:T(8,128)(2,1)} collective-permute-done((bf16[1024,256]{1,0:T(8,128)(2,1)S(1)}, bf16[1024,256]{1,0:T(8,128)(2,1)}, u32[]{:S(2)}, u32[]{:S(2)}) %collective-permute-start.3) | collective-permute-done | bytes 524320 | tf_op jit(solution)/shard_map/ppermute | solution.py:395
  97.7 0.0 all-to-all-done.2.x_ref
  97.7 0.0 copy-done
  97.7 0.0 copy-done.1
  97.7 0.0 copy-done.5
  97.8 2.9 %gate_up.1 = bf16[4,648,256]{2,1,0:T(8,128)(2,1)S(1)} custom-call(bf16[8,320,256]{2,1,0:T(8,128)(2,1)S(1)} %all-to-all-done.2.x_ref, bf16[32,128]{1,0:T(8,128)(2,1)S(1)} %bitcast.35, bf16[4096,128]{1,0:T(8,128)(2,1)S(1)} %bitcast.23, bf16[4096,128]{1,0:T(8,128)(2,1)S(1)} %bitcast.26, bf16[1024,256]{1,0:T(8,128)(2,1)} %copy-done.7, ...), custom_call_target="tpu_custom_call" | custom-call | tf_op jit(solution)/shard_map/gate_up/pallas_call | solution.py:272
  100.6 22.3 %all_to_all.36.p_ref = bf16[4,648,256]{2,1,0:T(8,128)(2,1)S(1)} all-to-all(bf16[4,648,256]{2,1,0:T(8,128)(2,1)S(1)} %gate_up.1), channel_id=1, replica_groups=mesh['z'=16,'core'=2,'ty'=4,'tx'=4] {'ty'}, dimensions={0} | all-to-all | bytes 2654208 | tf_op jit(solution)/shard_map/all_to_all | solution.py:451
  122.9 0.0 copy-start.2
  122.9 1.2 shard_map.133
  124.1 4.9 %all-to-all-start.4 = ((bf16[4,640,128]{2,1,0:T(8,128)(2,1)}), bf16[4,640,128]{2,1,0:T(8,128)(2,1)S(1)}, u32[]{:S(2)}, u32[]{:S(2)}) async-start(bf16[4,640,128]{2,1,0:T(8,128)(2,1)} %shard_map.133), calls=%async_computation.4 | async-start | bytes 1310720 | tf_op jit(solution)/shard_map/all_to_all | solution.py:453
  129.1 0.0 copy-done.2
  129.1 0.1 dynamic-slice_bitcast_fusion
  129.1 3.5 %collective-permute-start.4 = (bf16[4,128,256]{2,1,0:T(8,128)(2,1)S(1)}, bf16[4,128,256]{2,1,0:T(8,128)(2,1)S(1)}, u32[]{:S(2)}, u32[]{:S(2)}) collective-permute-start(bf16[4,128,256]{2,1,0:T(8,128)(2,1)S(1)} %get-tuple-element.27), channel_id=1, source_target_pairs={{0,1},{1,2},{2,3},{3,0},{4,5},{5,6},{6,7},{7,4},{8,9},{9,10},{10,1... | collective-permute-start | bytes 786440 | tf_op jit(solution)/shard_map/ppermute | solution.py:395
  132.7 4.6 %collective-permute-start.5 = (bf16[4,128,256]{2,1,0:T(8,128)(2,1)S(1)}, bf16[4,128,256]{2,1,0:T(8,128)(2,1)S(1)}, u32[]{:S(2)}, u32[]{:S(2)}) collective-permute-start(bf16[4,128,256]{2,1,0:T(8,128)(2,1)S(1)} %get-tuple-element.26), channel_id=1, source_target_pairs={{0,2},{1,3},{2,0},{3,1},{4,6},{5,7},{6,4},{7,5},{8,10},{9,11},{10,... | collective-permute-start | bytes 786440 | tf_op jit(solution)/shard_map/ppermute | solution.py:395
  137.3 3.4 %collective-permute-start.6 = (bf16[4,128,256]{2,1,0:T(8,128)(2,1)S(1)}, bf16[4,128,256]{2,1,0:T(8,128)(2,1)S(1)}, u32[]{:S(2)}, u32[]{:S(2)}) collective-permute-start(bf16[4,128,256]{2,1,0:T(8,128)(2,1)S(1)} %get-tuple-element.25), channel_id=1, source_target_pairs={{0,3},{1,0},{2,1},{3,2},{4,7},{5,4},{6,5},{7,6},{8,11},{9,8},{10,9... | collective-permute-start | bytes 786440 | tf_op jit(solution)/shard_map/ppermute | solution.py:395
  140.6 0.0 collective-permute-done.4.refs_0_
  140.6 0.0 copy-start.9
  140.7 4.8 %collective-permute-done.5.refs_1_ = bf16[4,128,256]{2,1,0:T(8,128)(2,1)S(1)} collective-permute-done((bf16[4,128,256]{2,1,0:T(8,128)(2,1)S(1)}, bf16[4,128,256]{2,1,0:T(8,128)(2,1)S(1)}, u32[]{:S(2)}, u32[]{:S(2)}) %collective-permute-start.5) | collective-permute-done | bytes 262176 | tf_op jit(solution)/shard_map/ppermute | solution.py:395
  145.4 0.0 copy-start.10
  145.4 1.5 collective-permute-done.6.refs_2_
  147.0 0.0 copy-done.9
  147.0 0.0 copy-done.10
  147.0 0.0 copy-start.11
  147.0 0.7 copy-done.11
  147.7 1.1 stage.1
  148.8 0.0 all-to-all-done.4.h_ref
  148.8 0.8 shard_map.134
  149.7 22.2 %all_to_all.37.p_ref = bf16[8,320,256]{2,1,0:T(8,128)(2,1)S(1)} all-to-all(bf16[8,320,256]{2,1,0:T(8,128)(2,1)S(1)} %shard_map.134), channel_id=1, replica_groups=mesh['z'=16,'core'=2,'ty'=4,'tx'=4] {'core','tx'}, dimensions={0} | all-to-all | bytes 2621440 | tf_op jit(solution)/shard_map/all_to_all | solution.py:454
  171.9 0.4 shard_map.135
  172.3 27.4 %all_to_all.38 = bf16[16,40,256]{2,1,0:T(8,128)(2,1)S(1)} all-to-all(bf16[16,40,256]{2,1,0:T(8,128)(2,1)S(1)} %bitcast.32), channel_id=1, replica_groups=mesh['z'=16,'core'=2,'ty'=4,'tx'=4] {'z'}, dimensions={0} | all-to-all | bytes 655360 | tf_op jit(solution)/shard_map/all_to_all | solution.py:457
  199.6 0.0 copy-done.6
  199.6 1.2 shard_map.136
  (2 shorter events, 0.0 us)
Async XLA Ops:
  0.0 13.6 %copy-start.12 = (s32[256,2]{0,1:T(2,128)S(1)}, s32[256,2]{0,1:T(2,128)}, u32[]{:S(2)}) copy-start(s32[256,2]{0,1:T(2,128)} %param.21) | copy-start | bytes 6148
  0.0 23.6 %copy-start.3 = (bf16[1024,256]{1,0:T(8,128)(2,1)S(1)}, bf16[1024,256]{1,0:T(8,128)(2,1)}, u32[]{:S(2)}) copy-start(bf16[1024,256]{1,0:T(8,128)(2,1)} %w_ref.1) | copy-start | bytes 1572868
  0.0 23.6 %copy-start.4 = (bf16[256,256]{1,0:T(8,128)(2,1)S(1)}, bf16[256,256]{1,0:T(8,128)(2,1)}, u32[]{:S(2)}) copy-start(bf16[256,256]{1,0:T(8,128)(2,1)} %res_ref.1) | copy-start | bytes 393220
  0.9 2.9 %collective-permute-start = (bf16[2,64]{0,1:T(8,128)(2,1)S(1)}, bf16[2,64]{0,1:T(8,128)(2,1)S(1)}, u32[]{:S(2)}, u32[]{:S(2)}) collective-permute-start(bf16[2,64]{0,1:T(8,128)(2,1)S(1)} %multiply_convert_fusion), channel_id=1, source_target_pairs={{0,16},{16,32},{32,48},{48,64},{64,80},{80,96},{96,112},{112,128},... | collective-permute-start | bytes 776 | tf_op jit(solution)/shard_map/ppermute | solution.py:425
  4.9 18.7 %all-to-all-start = ((bf16[16,64,256]{2,1,0:T(8,128)(2,1)}), bf16[16,64,256]{2,1,0:T(8,128)(2,1)S(1)}, u32[]{:S(2)}, u32[]{:S(2)}) async-start(bf16[16,64,256]{2,1,0:T(8,128)(2,1)} %shard_map.127), calls=%async_computation | async-start | bytes 1048576 | tf_op jit(solution)/shard_map/all_to_all | solution.py:429
  60.9 36.8 %all-to-all-start.2 = ((bf16[8,320,256]{2,1,0:T(8,128)(2,1)}), bf16[8,320,256]{2,1,0:T(8,128)(2,1)S(1)}, u32[]{:S(2)}, u32[]{:S(2)}) async-start(bf16[8,320,256]{2,1,0:T(8,128)(2,1)} %shard_map.130), calls=%async_computation.2 | async-start | bytes 2621440 | tf_op jit(solution)/shard_map/all_to_all | solution.py:449
  65.7 17.1 %collective-permute-start.1 = (bf16[1024,256]{1,0:T(8,128)(2,1)S(1)}, bf16[1024,256]{1,0:T(8,128)(2,1)S(1)}, u32[]{:S(2)}, u32[]{:S(2)}) collective-permute-start(bf16[1024,256]{1,0:T(8,128)(2,1)S(1)} %get-tuple-element.19), channel_id=1, source_target_pairs={{0,4},{4,8},{8,12},{12,0},{1,5},{5,9},{9,13},{13,1},{2,6},{6,10},{... | collective-permute-start | bytes 1572872 | tf_op jit(solution)/shard_map/ppermute | solution.py:395
  68.9 28.9 %copy-start = (bf16[1,4096,128]{2,1,0:T(8,128)(2,1)S(1)}, bf16[1,4096,128]{2,1,0:T(8,128)(2,1)}, u32[]{:S(2)}) copy-start(bf16[1,4096,128]{2,1,0:T(8,128)(2,1)} %param.23) | copy-start | bytes 3145732
  68.9 28.9 %copy-start.1 = (bf16[1,4096,128]{2,1,0:T(8,128)(2,1)S(1)}, bf16[1,4096,128]{2,1,0:T(8,128)(2,1)}, u32[]{:S(2)}) copy-start(bf16[1,4096,128]{2,1,0:T(8,128)(2,1)} %param.24) | copy-start | bytes 3145732
  68.9 28.9 %copy-start.5 = (bf16[4096]{0:T(1024)(128)(2,1)S(1)}, bf16[4096]{0:T(1024)(128)(2,1)}, u32[]{:S(2)}) copy-start(bf16[4096]{0:T(1024)(128)(2,1)} %param.20) | copy-start | bytes 24580
  68.9 18.4 %collective-permute-start.2 = (bf16[1024,256]{1,0:T(8,128)(2,1)S(1)}, bf16[1024,256]{1,0:T(8,128)(2,1)S(1)}, u32[]{:S(2)}, u32[]{:S(2)}) collective-permute-start(bf16[1024,256]{1,0:T(8,128)(2,1)S(1)} %get-tuple-element.20), channel_id=1, source_target_pairs={{0,8},{4,12},{8,0},{12,4},{1,9},{5,13},{9,1},{13,5},{2,10},{6,14},... | collective-permute-start | bytes 1572872 | tf_op jit(solution)/shard_map/ppermute | solution.py:395
  75.3 22.5 %collective-permute-start.3 = (bf16[1024,256]{1,0:T(8,128)(2,1)S(1)}, bf16[1024,256]{1,0:T(8,128)(2,1)}, u32[]{:S(2)}, u32[]{:S(2)}) collective-permute-start(bf16[1024,256]{1,0:T(8,128)(2,1)S(1)} %shard_map.132), channel_id=1, source_target_pairs={{0,12},{4,0},{8,4},{12,8},{1,13},{5,1},{9,5},{13,9},{2,14},{6,2},{... | collective-permute-start | bytes 1572872 | tf_op jit(solution)/shard_map/ppermute | solution.py:395
  82.8 4.5 %copy-start.7 = (bf16[1024,256]{1,0:T(8,128)(2,1)}, bf16[1024,256]{1,0:T(8,128)(2,1)S(1)}, u32[]{:S(2)}) copy-start(bf16[1024,256]{1,0:T(8,128)(2,1)S(1)} %collective-permute-done.1.rest_0_) | copy-start | bytes 1572868
  87.3 0.8 copy-start.8
  122.9 6.1 %copy-start.2 = (bf16[1,2048,256]{2,1,0:T(8,128)(2,1)S(1)}, bf16[1,2048,256]{2,1,0:T(8,128)(2,1)}, u32[]{:S(2)}) copy-start(bf16[1,2048,256]{2,1,0:T(8,128)(2,1)} %param.25) | copy-start | bytes 3145732
  124.1 24.7 %all-to-all-start.4 = ((bf16[4,640,128]{2,1,0:T(8,128)(2,1)}), bf16[4,640,128]{2,1,0:T(8,128)(2,1)S(1)}, u32[]{:S(2)}, u32[]{:S(2)}) async-start(bf16[4,640,128]{2,1,0:T(8,128)(2,1)} %shard_map.133), calls=%async_computation.4 | async-start | bytes 1310720 | tf_op jit(solution)/shard_map/all_to_all | solution.py:453
  129.1 11.5 %collective-permute-start.4 = (bf16[4,128,256]{2,1,0:T(8,128)(2,1)S(1)}, bf16[4,128,256]{2,1,0:T(8,128)(2,1)S(1)}, u32[]{:S(2)}, u32[]{:S(2)}) collective-permute-start(bf16[4,128,256]{2,1,0:T(8,128)(2,1)S(1)} %get-tuple-element.27), channel_id=1, source_target_pairs={{0,1},{1,2},{2,3},{3,0},{4,5},{5,6},{6,7},{7,4},{8,9},{9,10},{10,1... | collective-permute-start | bytes 786440 | tf_op jit(solution)/shard_map/ppermute | solution.py:395
  132.7 12.8 %collective-permute-start.5 = (bf16[4,128,256]{2,1,0:T(8,128)(2,1)S(1)}, bf16[4,128,256]{2,1,0:T(8,128)(2,1)S(1)}, u32[]{:S(2)}, u32[]{:S(2)}) collective-permute-start(bf16[4,128,256]{2,1,0:T(8,128)(2,1)S(1)} %get-tuple-element.26), channel_id=1, source_target_pairs={{0,2},{1,3},{2,0},{3,1},{4,6},{5,7},{6,4},{7,5},{8,10},{9,11},{10,... | collective-permute-start | bytes 786440 | tf_op jit(solution)/shard_map/ppermute | solution.py:395
  137.3 9.7 %collective-permute-start.6 = (bf16[4,128,256]{2,1,0:T(8,128)(2,1)S(1)}, bf16[4,128,256]{2,1,0:T(8,128)(2,1)S(1)}, u32[]{:S(2)}, u32[]{:S(2)}) collective-permute-start(bf16[4,128,256]{2,1,0:T(8,128)(2,1)S(1)} %get-tuple-element.25), channel_id=1, source_target_pairs={{0,3},{1,0},{2,1},{3,2},{4,7},{5,4},{6,5},{7,6},{8,11},{9,8},{10,9... | collective-permute-start | bytes 786440 | tf_op jit(solution)/shard_map/ppermute | solution.py:395
  140.6 6.3 %copy-start.9 = (bf16[4,128,256]{2,1,0:T(8,128)(2,1)}, bf16[4,128,256]{2,1,0:T(8,128)(2,1)S(1)}, u32[]{:S(2)}) copy-start(bf16[4,128,256]{2,1,0:T(8,128)(2,1)S(1)} %collective-permute-done.4.refs_0_) | copy-start | bytes 786436
  145.4 1.5 copy-start.10
  147.0 0.7 copy-start.11
  171.9 27.8 %copy-start.6 = (f32[256,2]{0,1:T(2,128)S(1)}, f32[256,2]{0,1:T(2,128)}, u32[]{:S(2)}) copy-start(f32[256,2]{0,1:T(2,128)} %param.22) | copy-start | bytes 6148

commit v7 on v6

--- a/solution.py
+++ b/solution.py
@@ -194,30 +194,38 @@
     feats = dim // n_ty
 
     def body(wg_ref, wu_ref, *rest):
-        out_refs, sems = rest[:-1], rest[-1]
+        count = len(steps)
+        out_refs, held, sems = rest[:count], rest[count], rest[count + 1]
         ty = lax.axis_index("ty")
-        moves = []
+        reads, writes = [], []
         for k, d in enumerate(steps):
             to = lax.rem(ty + d, n_ty)
             rows = pl.ds(pl.multiple_of(to * feats, feats), feats)
             for j, w_ref in enumerate((wg_ref, wu_ref)):
                 lanes = pl.ds(j * hid, hid)
-                moves.append(
-                    pltpu.make_async_copy(
-                        w_ref.at[rows, :], out_refs[k].at[:, lanes], sems.at[2 * k + j]
-                    )
+                move = pltpu.make_async_copy(
+                    w_ref.at[rows, :], held.at[k, :, lanes], sems.at[3 * k + j]
                 )
-        for move in moves:
+                move.start()
+                reads.append(move)
+        for k in range(count):
+            reads[2 * k].wait()
+            reads[2 * k + 1].wait()
+            move = pltpu.make_async_copy(held.at[k], out_refs[k], sems.at[3 * k + 2])
             move.start()
-        for move in moves:
+            writes.append(move)
+        for move in writes:
             move.wait()
 
     return pl.pallas_call(
         body,
         out_shape=tuple(jax.ShapeDtypeStruct((feats, 2 * hid), BF16) for d in steps),
         in_specs=[pl.BlockSpec(memory_space=pltpu.HBM)] * 2,
-        out_specs=tuple(pl.BlockSpec(memory_space=pltpu.VMEM) for d in steps),
-        scratch_shapes=[pltpu.SemaphoreType.DMA((2 * len(steps),))],
+        out_specs=tuple(pl.BlockSpec(memory_space=pl.ANY) for d in steps),
+        scratch_shapes=[
+            pltpu.VMEM((len(steps), feats, 2 * hid), BF16),
+            pltpu.SemaphoreType.DMA((3 * len(steps),)),
+        ],
         compiler_params=pltpu.CompilerParams(vmem_limit_bytes=12 << 20),
     )(*[pltpu.with_memory_space_constraint(w, pltpu.HBM) for w in (w_gate, w_up)])
 

time: 202 us -> 202 us (level)
  no operation moved by 1% of the time
where the time goes in v7:
time: 202 us; the launch traced here: 201 us
  blocking collectives  107 us (53%)
  starting transfers between devices  41 us (20%)
  waiting for transfers between devices  35.1 us (17%)
  Pallas kernels  14.8 us (7%)
    all_to_all x1, blocking collectives, local(): lax.all_to_all(outgoing.reshape(n_z, 2 * cap, width), 'z', 0, 0, tiled=True)  35.3 us
    all_to_all x1, blocking collectives, local(): lax.all_to_all(join_rows(outs, cap).reshape(n_z, 2 * cap, width), 'z', 0,...  27.4 us
    ppermute x6, waiting for transfers between devices, shifted(): lax.ppermute(value, axis, [(i, (i + steps) % count) for i in range(count)])  25.8 us
    all_to_all x1, blocking collectives, local(): parts = lax.all_to_all(parts, 'ty', 0, 0, tiled=True)  22.3 us
    all_to_all x1, blocking collectives, local(): lax.all_to_all(down(hidden, w_down4, stage(down_pieces)), ('core', 'tx'),...  22.2 us
    ppermute x6, starting transfers between devices, shifted(): lax.ppermute(value, axis, [(i, (i + steps) % count) for i in range(count)])  22 us
    all_to_all x1, waiting for transfers between devices, local(): conv_all = lax.all_to_all(conv_copies, TP, 0, 0, tiled=True)  9.33 us
    all_to_all x1, starting transfers between devices, local(): conv_all = lax.all_to_all(conv_copies, TP, 0, 0, tiled=True)  8.72 us
  transfers between devices with their start and end apart: 10, of which 6 were waited for; matrix products, arithmetic and copies ran while one was open for 0% of the time, Pallas kernels for 3%

profile of v7, /device:TPU:8, one launch (start us, length us, event | category | flops | bytes accessed | tf_op | source)
XLA Modules:
  0.0 200.9 jit_solution(11760730939406104439)
XLA Ops:
  0.0 0.0 copy-start.12
  0.0 0.0 copy-start.3
  0.0 0.9 multiply_convert_fusion
  0.9 1.7 collective-permute-start
  2.6 1.2 convolve_head.1
  3.8 0.0 collective-permute-done
  3.8 1.0 shard_map.127
  4.9 8.7 %all-to-all-start = ((bf16[16,64,256]{2,1,0:T(8,128)(2,1)}), bf16[16,64,256]{2,1,0:T(8,128)(2,1)S(1)}, u32[]{:S(2)}, u32[]{:S(2)}) async-start(bf16[16,64,256]{2,1,0:T(8,128)(2,1)} %shard_map.127), calls=%async_computation | async-start | bytes 1048576 | tf_op jit(solution)/shard_map/all_to_all | solution.py:437
  13.6 0.0 copy-done.12
  13.6 0.1 copy.17.pick_ref
  13.7 0.5 shard_map.128.slot_ref
  14.3 9.3 %all-to-all-done = bf16[16,64,256]{2,1,0:T(8,128)(2,1)S(1)} async-done(((bf16[16,64,256]{2,1,0:T(8,128)(2,1)}), bf16[16,64,256]{2,1,0:T(8,128)(2,1)S(1)}, u32[]{:S(2)}, u32[]{:S(2)}) %all-to-all-start) | async-done | bytes 524320 | tf_op jit(solution)/shard_map/all_to_all | solution.py:437
  23.6 0.0 copy-done.3
  23.6 0.0 copy-done.4
  23.6 0.7 shard_map.129
  24.3 35.3 %all_to_all.35 = bf16[16,40,256]{2,1,0:T(8,128)(2,1)S(1)} all-to-all(bf16[16,40,256]{2,1,0:T(8,128)(2,1)S(1)} %bitcast.33), channel_id=1, replica_groups=mesh['z'=16,'core'=2,'ty'=4,'tx'=4] {'z'}, dimensions={0} | all-to-all | bytes 655360 | tf_op jit(solution)/shard_map/all_to_all | solution.py:453
  59.6 1.3 shard_map.130
  60.9 3.6 %all-to-all-start.2 = ((bf16[8,320,256]{2,1,0:T(8,128)(2,1)}), bf16[8,320,256]{2,1,0:T(8,128)(2,1)S(1)}, u32[]{:S(2)}, u32[]{:S(2)}) async-start(bf16[8,320,256]{2,1,0:T(8,128)(2,1)} %shard_map.130), calls=%async_computation.2 | async-start | bytes 2621440 | tf_op jit(solution)/shard_map/all_to_all | solution.py:457
  64.5 1.3 shard_map.131
  65.8 3.1 %collective-permute-start.1 = (bf16[1024,256]{1,0:T(8,128)(2,1)S(1)}, bf16[1024,256]{1,0:T(8,128)(2,1)S(1)}, u32[]{:S(2)}, u32[]{:S(2)}) collective-permute-start(bf16[1024,256]{1,0:T(8,128)(2,1)S(1)} %get-tuple-element.19), channel_id=1, source_target_pairs={{0,4},{4,8},{8,12},{12,0},{1,5},{5,9},{9,13},{13,1},{2,6},{6,10},{... | collective-permute-start | bytes 1572872 | tf_op jit(solution)/shard_map/ppermute | solution.py:403
  68.9 0.0 copy-start
  68.9 0.0 copy-start.1
  68.9 0.0 copy-start.5
  69.0 5.3 %collective-permute-start.2 = (bf16[1024,256]{1,0:T(8,128)(2,1)S(1)}, bf16[1024,256]{1,0:T(8,128)(2,1)S(1)}, u32[]{:S(2)}, u32[]{:S(2)}) collective-permute-start(bf16[1024,256]{1,0:T(8,128)(2,1)S(1)} %get-tuple-element.20), channel_id=1, source_target_pairs={{0,8},{4,12},{8,0},{12,4},{1,9},{5,13},{9,1},{13,5},{2,10},{6,14},... | collective-permute-start | bytes 1572872 | tf_op jit(solution)/shard_map/ppermute | solution.py:403
  74.3 1.1 shard_map.132
  75.4 2.1 %collective-permute-start.3 = (bf16[1024,256]{1,0:T(8,128)(2,1)S(1)}, bf16[1024,256]{1,0:T(8,128)(2,1)}, u32[]{:S(2)}, u32[]{:S(2)}) collective-permute-start(bf16[1024,256]{1,0:T(8,128)(2,1)S(1)} %shard_map.132), channel_id=1, source_target_pairs={{0,12},{4,0},{8,4},{12,8},{1,13},{5,1},{9,5},{13,9},{2,14},{6,2},{... | collective-permute-start | bytes 1572872 | tf_op jit(solution)/shard_map/ppermute | solution.py:403
  77.5 5.3 %collective-permute-done.1.rest_0_ = bf16[1024,256]{1,0:T(8,128)(2,1)S(1)} collective-permute-done((bf16[1024,256]{1,0:T(8,128)(2,1)S(1)}, bf16[1024,256]{1,0:T(8,128)(2,1)S(1)}, u32[]{:S(2)}, u32[]{:S(2)}) %collective-permute-start.1) | collective-permute-done | bytes 524320 | tf_op jit(solution)/shard_map/ppermute | solution.py:403
  82.9 0.0 copy-start.7
  82.9 4.5 %collective-permute-done.2.rest_1_ = bf16[1024,256]{1,0:T(8,128)(2,1)S(1)} collective-permute-done((bf16[1024,256]{1,0:T(8,128)(2,1)S(1)}, bf16[1024,256]{1,0:T(8,128)(2,1)S(1)}, u32[]{:S(2)}, u32[]{:S(2)}) %collective-permute-start.2) | collective-permute-done | bytes 524320 | tf_op jit(solution)/shard_map/ppermute | solution.py:403
  87.3 0.0 copy-done.7
  87.3 0.0 copy-start.8
  87.3 0.8 copy-done.8
  88.1 9.7 %collective-permute-done.3.rest_2_ = bf16[1024,256]{1,0:T(8,128)(2,1)} collective-permute-done((bf16[1024,256]{1,0:T(8,128)(2,1)S(1)}, bf16[1024,256]{1,0:T(8,128)(2,1)}, u32[]{:S(2)}, u32[]{:S(2)}) %collective-permute-start.3) | collective-permute-done | bytes 524320 | tf_op jit(solution)/shard_map/ppermute | solution.py:403
  97.8 0.0 all-to-all-done.2.x_ref
  97.8 0.0 copy-done
  97.8 0.0 copy-done.1
  97.8 0.0 copy-done.5
  97.8 2.9 %gate_up.1 = bf16[4,648,256]{2,1,0:T(8,128)(2,1)S(1)} custom-call(bf16[8,320,256]{2,1,0:T(8,128)(2,1)S(1)} %all-to-all-done.2.x_ref, bf16[32,128]{1,0:T(8,128)(2,1)S(1)} %bitcast.35, bf16[4096,128]{1,0:T(8,128)(2,1)S(1)} %bitcast.23, bf16[4096,128]{1,0:T(8,128)(2,1)S(1)} %bitcast.26, bf16[1024,256]{1,0:T(8,128)(2,1)} %copy-done.7, ...), custom_call_target="tpu_custom_call" | custom-call | tf_op jit(solution)/shard_map/gate_up/pallas_call | solution.py:280
  100.7 22.3 %all_to_all.36.p_ref = bf16[4,648,256]{2,1,0:T(8,128)(2,1)S(1)} all-to-all(bf16[4,648,256]{2,1,0:T(8,128)(2,1)S(1)} %gate_up.1), channel_id=1, replica_groups=mesh['z'=16,'core'=2,'ty'=4,'tx'=4] {'ty'}, dimensions={0} | all-to-all | bytes 2654208 | tf_op jit(solution)/shard_map/all_to_all | solution.py:459
  123.0 0.0 copy-start.2
  123.0 1.2 shard_map.133
  124.2 4.9 %all-to-all-start.4 = ((bf16[4,640,128]{2,1,0:T(8,128)(2,1)}), bf16[4,640,128]{2,1,0:T(8,128)(2,1)S(1)}, u32[]{:S(2)}, u32[]{:S(2)}) async-start(bf16[4,640,128]{2,1,0:T(8,128)(2,1)} %shard_map.133), calls=%async_computation.4 | async-start | bytes 1310720 | tf_op jit(solution)/shard_map/all_to_all | solution.py:461
  129.1 0.0 copy-done.2
  129.1 0.1 dynamic-slice_bitcast_fusion
  129.2 3.5 %collective-permute-start.4 = (bf16[4,128,256]{2,1,0:T(8,128)(2,1)S(1)}, bf16[4,128,256]{2,1,0:T(8,128)(2,1)S(1)}, u32[]{:S(2)}, u32[]{:S(2)}) collective-permute-start(bf16[4,128,256]{2,1,0:T(8,128)(2,1)S(1)} %get-tuple-element.27), channel_id=1, source_target_pairs={{0,1},{1,2},{2,3},{3,0},{4,5},{5,6},{6,7},{7,4},{8,9},{9,10},{10,1... | collective-permute-start | bytes 786440 | tf_op jit(solution)/shard_map/ppermute | solution.py:403
  132.7 4.6 %collective-permute-start.5 = (bf16[4,128,256]{2,1,0:T(8,128)(2,1)S(1)}, bf16[4,128,256]{2,1,0:T(8,128)(2,1)S(1)}, u32[]{:S(2)}, u32[]{:S(2)}) collective-permute-start(bf16[4,128,256]{2,1,0:T(8,128)(2,1)S(1)} %get-tuple-element.26), channel_id=1, source_target_pairs={{0,2},{1,3},{2,0},{3,1},{4,6},{5,7},{6,4},{7,5},{8,10},{9,11},{10,... | collective-permute-start | bytes 786440 | tf_op jit(solution)/shard_map/ppermute | solution.py:403
  137.3 3.4 %collective-permute-start.6 = (bf16[4,128,256]{2,1,0:T(8,128)(2,1)S(1)}, bf16[4,128,256]{2,1,0:T(8,128)(2,1)S(1)}, u32[]{:S(2)}, u32[]{:S(2)}) collective-permute-start(bf16[4,128,256]{2,1,0:T(8,128)(2,1)S(1)} %get-tuple-element.25), channel_id=1, source_target_pairs={{0,3},{1,0},{2,1},{3,2},{4,7},{5,4},{6,5},{7,6},{8,11},{9,8},{10,9... | collective-permute-start | bytes 786440 | tf_op jit(solution)/shard_map/ppermute | solution.py:403
  140.7 0.0 collective-permute-done.4.refs_0_
  140.7 0.0 copy-start.9
  140.7 4.8 %collective-permute-done.5.refs_1_ = bf16[4,128,256]{2,1,0:T(8,128)(2,1)S(1)} collective-permute-done((bf16[4,128,256]{2,1,0:T(8,128)(2,1)S(1)}, bf16[4,128,256]{2,1,0:T(8,128)(2,1)S(1)}, u32[]{:S(2)}, u32[]{:S(2)}) %collective-permute-start.5) | collective-permute-done | bytes 262176 | tf_op jit(solution)/shard_map/ppermute | solution.py:403
  145.5 0.0 copy-start.10
  145.5 1.5 collective-permute-done.6.refs_2_
  147.0 0.0 copy-done.9
  147.0 0.0 copy-done.10
  147.0 0.0 copy-start.11
  147.0 0.7 copy-done.11
  147.7 1.1 stage.1
  148.9 0.0 all-to-all-done.4.h_ref
  148.9 0.8 shard_map.134
  149.7 22.2 %all_to_all.37.p_ref = bf16[8,320,256]{2,1,0:T(8,128)(2,1)S(1)} all-to-all(bf16[8,320,256]{2,1,0:T(8,128)(2,1)S(1)} %shard_map.134), channel_id=1, replica_groups=mesh['z'=16,'core'=2,'ty'=4,'tx'=4] {'core','tx'}, dimensions={0} | all-to-all | bytes 2621440 | tf_op jit(solution)/shard_map/all_to_all | solution.py:462
  171.9 0.4 shard_map.135
  172.3 27.4 %all_to_all.38 = bf16[16,40,256]{2,1,0:T(8,128)(2,1)S(1)} all-to-all(bf16[16,40,256]{2,1,0:T(8,128)(2,1)S(1)} %bitcast.32), channel_id=1, replica_groups=mesh['z'=16,'core'=2,'ty'=4,'tx'=4] {'z'}, dimensions={0} | all-to-all | bytes 655360 | tf_op jit(solution)/shard_map/all_to_all | solution.py:465
  199.7 0.0 copy-done.6
  199.7 1.2 shard_map.136
  (2 shorter events, 0.0 us)
Async XLA Ops:
  0.0 13.6 %copy-start.12 = (s32[256,2]{0,1:T(2,128)S(1)}, s32[256,2]{0,1:T(2,128)}, u32[]{:S(2)}) copy-start(s32[256,2]{0,1:T(2,128)} %param.21) | copy-start | bytes 6148
  0.0 23.6 %copy-start.3 = (bf16[1024,256]{1,0:T(8,128)(2,1)S(1)}, bf16[1024,256]{1,0:T(8,128)(2,1)}, u32[]{:S(2)}) copy-start(bf16[1024,256]{1,0:T(8,128)(2,1)} %w_ref.1) | copy-start | bytes 1572868
  0.0 23.6 %copy-start.4 = (bf16[256,256]{1,0:T(8,128)(2,1)S(1)}, bf16[256,256]{1,0:T(8,128)(2,1)}, u32[]{:S(2)}) copy-start(bf16[256,256]{1,0:T(8,128)(2,1)} %res_ref.1) | copy-start | bytes 393220
  0.9 2.9 %collective-permute-start = (bf16[2,64]{0,1:T(8,128)(2,1)S(1)}, bf16[2,64]{0,1:T(8,128)(2,1)S(1)}, u32[]{:S(2)}, u32[]{:S(2)}) collective-permute-start(bf16[2,64]{0,1:T(8,128)(2,1)S(1)} %multiply_convert_fusion), channel_id=1, source_target_pairs={{0,16},{16,32},{32,48},{48,64},{64,80},{80,96},{96,112},{112,128},... | collective-permute-start | bytes 776 | tf_op jit(solution)/shard_map/ppermute | solution.py:433
  4.9 18.7 %all-to-all-start = ((bf16[16,64,256]{2,1,0:T(8,128)(2,1)}), bf16[16,64,256]{2,1,0:T(8,128)(2,1)S(1)}, u32[]{:S(2)}, u32[]{:S(2)}) async-start(bf16[16,64,256]{2,1,0:T(8,128)(2,1)} %shard_map.127), calls=%async_computation | async-start | bytes 1048576 | tf_op jit(solution)/shard_map/all_to_all | solution.py:437
  60.9 36.9 %all-to-all-start.2 = ((bf16[8,320,256]{2,1,0:T(8,128)(2,1)}), bf16[8,320,256]{2,1,0:T(8,128)(2,1)S(1)}, u32[]{:S(2)}, u32[]{:S(2)}) async-start(bf16[8,320,256]{2,1,0:T(8,128)(2,1)} %shard_map.130), calls=%async_computation.2 | async-start | bytes 2621440 | tf_op jit(solution)/shard_map/all_to_all | solution.py:457
  65.8 17.1 %collective-permute-start.1 = (bf16[1024,256]{1,0:T(8,128)(2,1)S(1)}, bf16[1024,256]{1,0:T(8,128)(2,1)S(1)}, u32[]{:S(2)}, u32[]{:S(2)}) collective-permute-start(bf16[1024,256]{1,0:T(8,128)(2,1)S(1)} %get-tuple-element.19), channel_id=1, source_target_pairs={{0,4},{4,8},{8,12},{12,0},{1,5},{5,9},{9,13},{13,1},{2,6},{6,10},{... | collective-permute-start | bytes 1572872 | tf_op jit(solution)/shard_map/ppermute | solution.py:403
  68.9 28.9 %copy-start = (bf16[1,4096,128]{2,1,0:T(8,128)(2,1)S(1)}, bf16[1,4096,128]{2,1,0:T(8,128)(2,1)}, u32[]{:S(2)}) copy-start(bf16[1,4096,128]{2,1,0:T(8,128)(2,1)} %param.23) | copy-start | bytes 3145732
  68.9 28.9 %copy-start.1 = (bf16[1,4096,128]{2,1,0:T(8,128)(2,1)S(1)}, bf16[1,4096,128]{2,1,0:T(8,128)(2,1)}, u32[]{:S(2)}) copy-start(bf16[1,4096,128]{2,1,0:T(8,128)(2,1)} %param.24) | copy-start | bytes 3145732
  68.9 28.9 %copy-start.5 = (bf16[4096]{0:T(1024)(128)(2,1)S(1)}, bf16[4096]{0:T(1024)(128)(2,1)}, u32[]{:S(2)}) copy-start(bf16[4096]{0:T(1024)(128)(2,1)} %param.20) | copy-start | bytes 24580
  69.0 18.4 %collective-permute-start.2 = (bf16[1024,256]{1,0:T(8,128)(2,1)S(1)}, bf16[1024,256]{1,0:T(8,128)(2,1)S(1)}, u32[]{:S(2)}, u32[]{:S(2)}) collective-permute-start(bf16[1024,256]{1,0:T(8,128)(2,1)S(1)} %get-tuple-element.20), channel_id=1, source_target_pairs={{0,8},{4,12},{8,0},{12,4},{1,9},{5,13},{9,1},{13,5},{2,10},{6,14},... | collective-permute-start | bytes 1572872 | tf_op jit(solution)/shard_map/ppermute | solution.py:403
  75.4 22.4 %collective-permute-start.3 = (bf16[1024,256]{1,0:T(8,128)(2,1)S(1)}, bf16[1024,256]{1,0:T(8,128)(2,1)}, u32[]{:S(2)}, u32[]{:S(2)}) collective-permute-start(bf16[1024,256]{1,0:T(8,128)(2,1)S(1)} %shard_map.132), channel_id=1, source_target_pairs={{0,12},{4,0},{8,4},{12,8},{1,13},{5,1},{9,5},{13,9},{2,14},{6,2},{... | collective-permute-start | bytes 1572872 | tf_op jit(solution)/shard_map/ppermute | solution.py:403
  82.9 4.5 %copy-start.7 = (bf16[1024,256]{1,0:T(8,128)(2,1)}, bf16[1024,256]{1,0:T(8,128)(2,1)S(1)}, u32[]{:S(2)}) copy-start(bf16[1024,256]{1,0:T(8,128)(2,1)S(1)} %collective-permute-done.1.rest_0_) | copy-start | bytes 1572868
  87.3 0.8 copy-start.8
  123.0 6.1 %copy-start.2 = (bf16[1,2048,256]{2,1,0:T(8,128)(2,1)S(1)}, bf16[1,2048,256]{2,1,0:T(8,128)(2,1)}, u32[]{:S(2)}) copy-start(bf16[1,2048,256]{2,1,0:T(8,128)(2,1)} %param.25) | copy-start | bytes 3145732
  124.2 24.7 %all-to-all-start.4 = ((bf16[4,640,128]{2,1,0:T(8,128)(2,1)}), bf16[4,640,128]{2,1,0:T(8,128)(2,1)S(1)}, u32[]{:S(2)}, u32[]{:S(2)}) async-start(bf16[4,640,128]{2,1,0:T(8,128)(2,1)} %shard_map.133), calls=%async_computation.4 | async-start | bytes 1310720 | tf_op jit(solution)/shard_map/all_to_all | solution.py:461
  129.2 11.5 %collective-permute-start.4 = (bf16[4,128,256]{2,1,0:T(8,128)(2,1)S(1)}, bf16[4,128,256]{2,1,0:T(8,128)(2,1)S(1)}, u32[]{:S(2)}, u32[]{:S(2)}) collective-permute-start(bf16[4,128,256]{2,1,0:T(8,128)(2,1)S(1)} %get-tuple-element.27), channel_id=1, source_target_pairs={{0,1},{1,2},{2,3},{3,0},{4,5},{5,6},{6,7},{7,4},{8,9},{9,10},{10,1... | collective-permute-start | bytes 786440 | tf_op jit(solution)/shard_map/ppermute | solution.py:403
  132.7 12.8 %collective-permute-start.5 = (bf16[4,128,256]{2,1,0:T(8,128)(2,1)S(1)}, bf16[4,128,256]{2,1,0:T(8,128)(2,1)S(1)}, u32[]{:S(2)}, u32[]{:S(2)}) collective-permute-start(bf16[4,128,256]{2,1,0:T(8,128)(2,1)S(1)} %get-tuple-element.26), channel_id=1, source_target_pairs={{0,2},{1,3},{2,0},{3,1},{4,6},{5,7},{6,4},{7,5},{8,10},{9,11},{10,... | collective-permute-start | bytes 786440 | tf_op jit(solution)/shard_map/ppermute | solution.py:403
  137.3 9.7 %collective-permute-start.6 = (bf16[4,128,256]{2,1,0:T(8,128)(2,1)S(1)}, bf16[4,128,256]{2,1,0:T(8,128)(2,1)S(1)}, u32[]{:S(2)}, u32[]{:S(2)}) collective-permute-start(bf16[4,128,256]{2,1,0:T(8,128)(2,1)S(1)} %get-tuple-element.25), channel_id=1, source_target_pairs={{0,3},{1,0},{2,1},{3,2},{4,7},{5,4},{6,5},{7,6},{8,11},{9,8},{10,9... | collective-permute-start | bytes 786440 | tf_op jit(solution)/shard_map/ppermute | solution.py:403
  140.7 6.3 %copy-start.9 = (bf16[4,128,256]{2,1,0:T(8,128)(2,1)}, bf16[4,128,256]{2,1,0:T(8,128)(2,1)S(1)}, u32[]{:S(2)}) copy-start(bf16[4,128,256]{2,1,0:T(8,128)(2,1)S(1)} %collective-permute-done.4.refs_0_) | copy-start | bytes 786436
  145.5 1.5 copy-start.10
  147.0 0.7 copy-start.11
  171.9 27.7 %copy-start.6 = (f32[256,2]{0,1:T(2,128)S(1)}, f32[256,2]{0,1:T(2,128)}, u32[]{:S(2)}) copy-start(f32[256,2]{0,1:T(2,128)} %param.22) | copy-start | bytes 6148
